TPU v7x, 512 devices: a whole 4x4x16 slice. The times are simulated.
512 devices in a mesh: sp: 32 (over z, core), tp: 16 (over y, x).
Axes of the slice: x: 4, y: 4, z: 16, core: 2. Of those that a mesh axis runs over, the one named last changes fastest.
Arguments:
- queries: bfloat16 [8192, 2048], P('sp', 'tp'), may hold values from -8 to 8
- key_rows: bfloat16 [8192, 1024], P('sp', 'tp'), may hold values from -8 to 8
- values: bfloat16 [8192, 1024], P('sp', 'tp'), may hold values from -6 to 6
- sink_logits: float32 [32], P('tp'), may hold values from 2 to 6
- residual: bfloat16 [8192, 2048], P(('sp', 'tp')), may hold values from -6 to 6
- out_weight: bfloat16 [2048, 2048], P('tp'), may hold values from -0.125 to 0.125
- norm_gain: float32 [2048], replicated, may hold values from 0.1 to 1.9
- expert_ids: int32 [8192, 2], P('sp'), may hold values from 0 to 31, as said below
- route_weight: float32 [8192, 2], P('sp'), may hold values from 0.2 to 1
- gate_proj: bfloat16 [32, 2048, 4096], P('sp', None, 'tp'), may hold values from -0.125 to 0.125
- up_proj: bfloat16 [32, 2048, 4096], P('sp', None, 'tp'), may hold values from -0.125 to 0.125
- down_proj: bfloat16 [32, 4096, 2048], P('sp', 'tp'), may hold values from -0.09375 to 0.09375
Outputs:
- mixed_out: bfloat16 [8192, 2048], P(('sp', 'tp'))
Inputs may be any that keep to these rules, and one draw needn't show every extreme that they name: `expert_ids`: the two entries of a row are different experts of one group: experts g * 8 to g * 8 + 7 for a group g below 4. In each aligned block of 16 rows (the rows of one device) no expert is named more than 2 times, and one expert is named exactly 2 times in every block.
All inputs are finite; a program needn't handle non-finite values.
Results may differ from a plain program's by a relative error of at most 0.014.
Values may be sent and summed in bfloat16 or wider, within the bound.
No kernel may reach another device: no remote copies, remote signals or barrier semaphores. Data moves between devices by JAX's collectives and lax.ppermute only.
A program may use at most 64 MiB of HBM per device.

v0:
```python
import jax
import jax.numpy as jnp
from jax import lax
from jax.sharding import PartitionSpec as P

HEAD = 64
WINDOW = 128


norm_epsilon = 1e-06


def from_behind(block, axis, distance):
    devices = range(lax.axis_size(axis))
    route = [(i - distance, i) for i in devices if i - distance in devices]
    return lax.ppermute(block, axis, route)


def split_up(array, dim, size):
    before, after = (array.shape[:dim], array.shape[dim + 1 :])
    return jnp.moveaxis(array.reshape(*before, size, -1, *after), dim, 0)


def sum_at_owner(array, axis, dim):
    size = lax.axis_size(axis)
    pieces = lax.all_to_all(split_up(array, dim, size), axis, 0, 0, tiled=True)
    return jnp.sum(pieces.astype(jnp.float32), axis=0)


def rotary(values_in, positions, head_count):
    halfway = HEAD // 2
    frequency = 10000.0 ** (-jnp.arange(halfway, dtype=jnp.float32) * 2.0 / HEAD)
    angles = positions.astype(jnp.float32)[:, None] * frequency[None, :]
    cosine = jnp.cos(angles)[:, None, :]
    sine_part = jnp.sin(angles)[:, None, :]
    reshaped = values_in.astype(jnp.float32).reshape(values_in.shape[0], head_count, HEAD)
    front_part = reshaped[..., :halfway]
    back_part = reshaped[..., halfway:]
    turned = jnp.concatenate(
        [front_part * cosine - back_part * sine_part, back_part * cosine + front_part * sine_part],
        -1,
    )
    return turned.astype(jnp.bfloat16)


def attend(query_blocks, key_pairs, value_pairs, sink_grid, key_start):
    block_count = query_blocks.shape[0]
    window_len = query_blocks.shape[1]
    scores = jnp.einsum(
        "bqkgd,bskd->bkgqs", query_blocks, key_pairs, preferred_element_type=jnp.float32
    ) * HEAD ** (-0.5)
    row_idx = jnp.arange(window_len)[:, None]
    col_idx = jnp.arange(2 * window_len)[None, :]
    distance = row_idx - col_idx + window_len
    key_pos = key_start + jnp.arange(block_count)[:, None, None] * window_len + col_idx[None]
    allowed = (distance >= 0)[None] & (distance < window_len)[None] & (key_pos >= 0)
    scores = jnp.where(allowed[:, None, None], scores, -jnp.inf)
    sink_full = sink_grid[None, :, :, None]
    highest = jnp.maximum(jnp.max(scores, -1), sink_full)
    exp_scores = jnp.exp(scores - highest[..., None])
    denominator = jnp.sum(exp_scores, -1) + jnp.exp(sink_full - highest)
    weighted = jnp.einsum(
        "bkgqs,bskd->bkgqd",
        exp_scores.astype(jnp.bfloat16),
        value_pairs,
        preferred_element_type=jnp.float32,
    )
    normalized = weighted / denominator[..., None]
    return (
        jnp.transpose(normalized, (0, 3, 1, 2, 4))
        .astype(jnp.bfloat16)
        .reshape(block_count * window_len, -1)
    )


def slot_select(picks_in, expert_count, capacity):
    flattened = picks_in.reshape(-1)
    onehot = (flattened[:, None] == jnp.arange(expert_count, dtype=jnp.int32)[None, :]).astype(
        jnp.int32
    )
    rank_of = jnp.sum(jnp.cumsum(onehot, 0) * onehot, 1) - 1
    slot_of = flattened * capacity + rank_of
    chosen = jnp.arange(expert_count * capacity, dtype=jnp.int32)[:, None] == slot_of[None, :]
    return chosen.astype(jnp.bfloat16)


def expert_part(rows_in, gate_proj, up_proj, down_proj):
    in_shape = rows_in.shape
    flattened = rows_in.reshape(-1, in_shape[-1])
    gate_val = jnp.dot(flattened, gate_proj[0], preferred_element_type=jnp.float32)
    up_val = jnp.dot(flattened, up_proj[0], preferred_element_type=jnp.float32)
    hidden = (jax.nn.silu(gate_val) * up_val).astype(jnp.bfloat16)
    return (
        jnp.dot(hidden, down_proj[0], preferred_element_type=jnp.float32)
        .astype(jnp.bfloat16)
        .reshape(in_shape)
    )


def per_device(
    queries,
    key_rows,
    values,
    sink_logits,
    residual,
    out_weight,
    norm_gain,
    expert_ids,
    route_weight,
    gate_proj,
    up_proj,
    down_proj,
):
    local_len = queries.shape[0]
    q_heads = sink_logits.shape[0]
    kv_heads = key_rows.shape[1] // HEAD
    group_size = q_heads // kv_heads
    window_len = WINDOW
    seq_start = lax.axis_index("sp") * local_len
    rim_pair = jnp.stack([key_rows[local_len - window_len :], values[local_len - window_len :]])
    rim_pair = from_behind(rim_pair, "sp", 1)
    key_ext = jnp.concatenate([rim_pair[0], key_rows], 0)
    val_ext = jnp.concatenate([rim_pair[1], values], 0)
    positions = seq_start + jnp.arange(local_len, dtype=jnp.int32)
    ext_positions = seq_start - window_len + jnp.arange(local_len + window_len, dtype=jnp.int32)
    rot_query = rotary(queries, positions, q_heads)
    rot_key = rotary(key_ext, ext_positions, kv_heads)
    block_count = local_len // window_len
    query_blocks = rot_query.reshape(block_count, window_len, kv_heads, group_size, HEAD)
    key_blocks = rot_key.reshape(block_count + 1, window_len, kv_heads, HEAD)
    value_blocks = val_ext.reshape(block_count + 1, window_len, kv_heads, HEAD)
    key_pairs = jnp.concatenate([key_blocks[:-1], key_blocks[1:]], 1)
    value_pairs = jnp.concatenate([value_blocks[:-1], value_blocks[1:]], 1)
    sink_grid = sink_logits.reshape(kv_heads, group_size)
    attended = attend(query_blocks, key_pairs, value_pairs, sink_grid, seq_start - window_len)
    tok_rows = residual.shape[0]
    tp_count = lax.axis_size("tp")
    tp_index = lax.axis_index("tp")
    projected = sum_at_owner(
        jnp.dot(attended, out_weight, preferred_element_type=jnp.float32).astype(jnp.bfloat16),
        "tp",
        0,
    )
    middle = (residual.astype(jnp.float32) + projected).astype(jnp.bfloat16)
    middle_f = middle.astype(jnp.float32)
    normed = (
        middle_f
        * lax.rsqrt(jnp.mean(middle_f * middle_f, -1, keepdims=True) + norm_epsilon)
        * norm_gain
    ).astype(jnp.bfloat16)
    expert_count = lax.axis_size("sp")
    capacity = 2 * max(1, 2 * tok_rows // expert_count)
    model_width = normed.shape[1]
    own_ids = lax.dynamic_slice_in_dim(expert_ids, tp_index * tok_rows, tok_rows, 0)
    own_weights = lax.dynamic_slice_in_dim(route_weight, tp_index * tok_rows, tok_rows, 0)
    select = slot_select(own_ids, expert_count, capacity)
    token_select = jnp.sum(select.reshape(expert_count * capacity, tok_rows, 2), -1)
    outbound = jnp.dot(token_select, normed, preferred_element_type=jnp.float32).astype(
        jnp.bfloat16
    )
    outbound = outbound.reshape(expert_count, capacity, model_width)
    arrived = lax.all_to_all(outbound, "sp", split_axis=0, concat_axis=0, tiled=True)
    partial_out = expert_part(
        lax.all_gather(arrived, "tp", axis=0, tiled=True), gate_proj, up_proj, down_proj
    )
    partial_out = partial_out.reshape(tp_count, expert_count * capacity, model_width)
    width_parts = lax.all_to_all(partial_out, "tp", split_axis=0, concat_axis=0, tiled=True)
    summed = jnp.sum(width_parts.astype(jnp.float32), 0).reshape(
        expert_count, capacity, model_width
    )
    returned = (
        lax.all_to_all(summed.astype(jnp.bfloat16), "sp", split_axis=0, concat_axis=0, tiled=True)
        .astype(summed.dtype)
        .reshape(expert_count * capacity, model_width)
    )
    picked = jnp.dot(
        select.astype(jnp.float32).T,
        returned,
        precision=lax.Precision.HIGHEST,
        preferred_element_type=jnp.float32,
    )
    routed = jnp.sum(picked.reshape(tok_rows, 2, model_width) * own_weights[..., None], 1)
    return (middle_f + routed).astype(jnp.bfloat16)


def solution(mesh):
    return jax.shard_map(
        per_device,
        mesh=mesh,
        in_specs=(
            P("sp", "tp"),
            P("sp", "tp"),
            P("sp", "tp"),
            P("tp"),
            P(("sp", "tp"), None),
            P("tp", None),
            P(),
            P("sp", None),
            P("sp", None),
            P("sp", None, "tp"),
            P("sp", None, "tp"),
            P("sp", "tp", None),
        ),
        out_specs=P(("sp", "tp"), None),
        check_vma=False,
    )
```

profile of v0, /device:TPU:1, one launch (start us, length us, event | category | flops | bytes accessed | tf_op | source)
XLA Modules:
  0.0 260.5 jit_solution(3781551424925160539)
XLA Ops:
  6.5 0.9 slice_bitcast_fusion.2
  7.4 4.9 %collective-permute-start = (bf16[2,128,64]{1,2,0:T(8,128)(2,1)S(1)}, bf16[2,128,64]{1,2,0:T(8,128)(2,1)S(1)}, u32[]{:S(2)}, u32[]{:S(2)}) collective-permute-start(bf16[2,128,64]{1,2,0:T(8,128)(2,1)S(1)} %pad_maximum_fusion.2), channel_id=1, source_target_pairs={{0,16},{16,32},{32,48},{48,64},{64,80},{80,96},{96,112},{112,128},... | collective-permute-start | bytes 98312 | tf_op jit(solution)/shard_map/ppermute | solution.py:16
  12.4 0.9 copy.39
  13.4 0.1 add_compare_fusion
  13.5 0.2 multiply_cosine_fusion.1
  13.7 0.1 broadcast_and_fusion
  13.9 0.8 slice.60
  14.7 1.5 collective-permute-done
  16.2 0.8 maximum_convert_fusion
  17.0 0.3 fusion.46
  17.3 0.3 fusion.61
  17.6 0.7 broadcast_maximum_fusion
  18.3 0.1 fusion.17
  18.4 0.7 exponential_add_fusion
  19.2 0.7 pad_maximum_fusion.1
  19.9 0.2 fusion.5
  20.1 0.1 copy.45
  20.2 1.4 convolution_convert_fusion.1
  21.7 5.3 %all-to-all-start = ((bf16[16,16,2048]{2,1,0:T(8,128)(2,1)}), bf16[16,16,2048]{2,1,0:T(8,128)(2,1)S(1)}, u32[]{:S(2)}, u32[]{:S(2)}) async-start(bf16[16,16,2048]{2,1,0:T(8,128)(2,1)} %bitcast.18), calls=%async_computation | async-start | bytes 2097152 | tf_op jit(solution)/shard_map/all_to_all | solution.py:26
  27.0 0.1 constant_dynamic-slice_fusion.1
  27.1 0.1 copy.52
  27.2 0.1 reshape.404
  27.3 0.1 fusion.54
  27.3 0.1 reduce_window_sum.11
  27.4 0.2 select_reduce_fusion
  27.6 0.1 sub.63
  27.7 0.1 copy.47
  27.8 0.1 fusion.57
  27.8 17.7 %all-to-all-done = bf16[16,16,2048]{2,1,0:T(8,128)(2,1)S(1)} async-done(((bf16[16,16,2048]{2,1,0:T(8,128)(2,1)}), bf16[16,16,2048]{2,1,0:T(8,128)(2,1)S(1)}, u32[]{:S(2)}, u32[]{:S(2)}) %all-to-all-start) | async-done | bytes 1048608 | tf_op jit(solution)/shard_map/all_to_all | solution.py:26
  45.5 0.1 convert_reduce_fusion
  45.7 0.1 fusion.22
  45.9 0.3 convolution_convert_fusion.2
  46.1 0.2 reshape.405
  46.3 36.3 %all_to_all.20 = bf16[32,2,2048]{2,1,0:T(2,128)(2,1)} all-to-all(bf16[32,2,2048]{2,1,0:T(2,128)(2,1)S(1)} %reshape.405), channel_id=1, replica_groups=mesh['sp'=32,'tp'=16] {'sp'}, dimensions={0} | all-to-all | bytes 524288 | tf_op jit(solution)/shard_map/all_to_all | solution.py:162
  82.6 53.9 %all-gather.2.cloned.1.call-done = bf16[512,2,2048]{2,1,0:T(2,128)(2,1)} async-done(((bf16[32,2,2048]{2,1,0:T(2,128)(2,1)}), bf16[512,2,2048]{2,1,0:T(2,128)(2,1)}) %all-gather.2.cloned.1.call-update) | async-done | bytes 4194320 | tf_op jit(solution)/shard_map/all_gather | solution.py:164
  136.6 7.2 %reshape.406 = bf16[1024,2048]{1,0:T(8,128)(2,1)} reshape(bf16[512,2,2048]{2,1,0:T(2,128)(2,1)} %all-gather.2.cloned.1.call-done) | data formatting | bytes 8388608 | tf_op jit(solution)/shard_map/reshape | solution.py:89
  143.8 4.5 %fusion.9 = f32[1024,256]{1,0:T(8,128)} fusion(bf16[1024,2048]{1,0:T(8,128)(2,1)} %reshape.406, bf16[1,2048,256]{2,1,0:T(8,128)(2,1)S(1)} %copy-done.6), kind=kOutput, calls=%fused_computation.16 | convolution fusion | flops 1073741824 | bytes 6291456 | tf_op jit(solution)/shard_map/dot_general | solution.py:90
  148.3 9.1 %convolution_convert_fusion = bf16[1024,2048]{1,0:T(8,128)(2,1)} fusion(bf16[1024,2048]{1,0:T(8,128)(2,1)} %reshape.406, bf16[1,256,2048]{2,1,0:T(8,128)(2,1)S(1)} %copy-done, bf16[1,2048,256]{2,1,0:T(8,128)(2,1)} %param.22, f32[1024,256]{1,0:T(8,128)} %fusion.9), kind=kOutput, calls=%fused_computation | convolution fusion | flops 2151153664 | bytes 11534336 | tf_op jit(solution)/shard_map/dot_general | solution.py:94
  157.4 55.0 %all_to_all.21 = bf16[16,64,2048]{2,1,0:T(8,128)(2,1)} all-to-all(bf16[16,64,2048]{2,1,0:T(8,128)(2,1)} %bitcast.84), channel_id=1, replica_groups=mesh['sp'=32,'tp'=16] {'tp'}, dimensions={0} | all-to-all | bytes 8388608 | tf_op jit(solution)/shard_map/all_to_all | solution.py:167
  212.4 3.0 %reduce_sum.74 = bf16[64,2048]{1,0:T(8,128)(2,1)S(1)} reduce(bf16[16,64,2048]{2,1,0:T(8,128)(2,1)} %all_to_all.21, bf16[]{:T(256)} %constant.52.clone.1), dimensions={0}, to_apply=%region_7.8 | reduce | flops 1966080 | bytes 4456450 | tf_op jit(solution)/shard_map/reduce_sum | solution.py:168
  215.4 0.9 convert_element_type.113
  216.2 14.3 %all-to-all-start.3 = ((bf16[32,2,2048]{2,1,0:T(2,128)(2,1)}), bf16[32,2,2048]{2,1,0:T(2,128)(2,1)S(1)}, u32[]{:S(2)}, u32[]{:S(2)}) async-start(bf16[32,2,2048]{2,1,0:T(2,128)(2,1)} %convert_element_type.113), calls=%async_computation.3 | async-start | bytes 524288 | tf_op jit(solution)/shard_map/all_to_all | solution.py:172
  230.5 0.1 iota_compare_fusion.2
  230.6 0.1 constant_dynamic-slice_fusion
  230.7 22.1 %all-to-all-done.3 = bf16[32,2,2048]{2,1,0:T(2,128)(2,1)S(1)} async-done(((bf16[32,2,2048]{2,1,0:T(2,128)(2,1)}), bf16[32,2,2048]{2,1,0:T(2,128)(2,1)S(1)}, u32[]{:S(2)}, u32[]{:S(2)}) %all-to-all-start.3) | async-done | bytes 262176 | tf_op jit(solution)/shard_map/all_to_all | solution.py:172
  252.8 0.1 reshape.412
  252.9 0.2 fusion.3
  253.0 0.6 fusion.25
  (36 shorter events, 0.3 us)
Async XLA Ops:
  6.5 141.8 %copy-start = (bf16[1,256,2048]{2,1,0:T(8,128)(2,1)S(1)}, bf16[1,256,2048]{2,1,0:T(8,128)(2,1)}, u32[]{:S(2)}) copy-start(bf16[1,256,2048]{2,1,0:T(8,128)(2,1)} %param.23) | copy-start | bytes 3145732
  6.5 13.7 %copy-start.1 = (bf16[128,2048]{1,0:T(8,128)(2,1)S(1)}, bf16[128,2048]{1,0:T(8,128)(2,1)}, u32[]{:S(2)}) copy-start(bf16[128,2048]{1,0:T(8,128)(2,1)} %param.17) | copy-start | bytes 1572868
  6.5 20.5 %copy-start.4 = (s32[256,2]{0,1:T(2,128)S(1)}, s32[256,2]{0,1:T(2,128)}, u32[]{:S(2)}) copy-start(s32[256,2]{0,1:T(2,128)} %param.19) | copy-start | bytes 6148
  7.4 8.8 %collective-permute-start = (bf16[2,128,64]{1,2,0:T(8,128)(2,1)S(1)}, bf16[2,128,64]{1,2,0:T(8,128)(2,1)S(1)}, u32[]{:S(2)}, u32[]{:S(2)}) collective-permute-start(bf16[2,128,64]{1,2,0:T(8,128)(2,1)S(1)} %pad_maximum_fusion.2), channel_id=1, source_target_pairs={{0,16},{16,32},{32,48},{48,64},{64,80},{80,96},{96,112},{112,128},... | collective-permute-start | bytes 98312 | tf_op jit(solution)/shard_map/ppermute | solution.py:16
  13.9 31.8 %copy-start.2 = (bf16[16,2048]{1,0:T(8,128)(2,1)S(1)}, bf16[16,2048]{1,0:T(8,128)(2,1)}, u32[]{:S(2)}) copy-start(bf16[16,2048]{1,0:T(8,128)(2,1)} %param.16) | copy-start | bytes 196612
  16.2 29.6 %copy-start.3 = (f32[2048]{0:T(1024)S(1)}, f32[2048]{0:T(1024)}, u32[]{:S(2)}) copy-start(f32[2048]{0:T(1024)} %param.18) | copy-start | bytes 24580
  21.7 23.9 %all-to-all-start = ((bf16[16,16,2048]{2,1,0:T(8,128)(2,1)}), bf16[16,16,2048]{2,1,0:T(8,128)(2,1)S(1)}, u32[]{:S(2)}, u32[]{:S(2)}) async-start(bf16[16,16,2048]{2,1,0:T(8,128)(2,1)} %bitcast.18), calls=%async_computation | async-start | bytes 2097152 | tf_op jit(solution)/shard_map/all_to_all | solution.py:26
  27.0 109.6 %all-gather.2.cloned.1.call-start = ((), (), s32[]{:S(2)}) async-start(), calls=%async_computation.4 | async-start | bytes 4456448 | tf_op jit(solution)/shard_map/all_gather | solution.py:164
  82.6 61.2 %copy-start.6 = (bf16[1,2048,256]{2,1,0:T(8,128)(2,1)S(1)}, bf16[1,2048,256]{2,1,0:T(8,128)(2,1)}, u32[]{:S(2)}) copy-start(bf16[1,2048,256]{2,1,0:T(8,128)(2,1)} %param.21) | copy-start | bytes 3145732
  212.4 18.2 %copy-start.5 = (f32[256,2]{0,1:T(2,128)S(1)}, f32[256,2]{0,1:T(2,128)}, u32[]{:S(2)}) copy-start(f32[256,2]{0,1:T(2,128)} %param.20) | copy-start | bytes 6148
  216.2 36.5 %all-to-all-start.3 = ((bf16[32,2,2048]{2,1,0:T(2,128)(2,1)}), bf16[32,2,2048]{2,1,0:T(2,128)(2,1)S(1)}, u32[]{:S(2)}, u32[]{:S(2)}) async-start(bf16[32,2,2048]{2,1,0:T(2,128)(2,1)} %convert_element_type.113), calls=%async_computation.3 | async-start | bytes 524288 | tf_op jit(solution)/shard_map/all_to_all | solution.py:172
Sparse Core Ops, SparseCore 0:
  82.7 53.7 all-gather.1
where the time goes:
time: 261 us
  waiting for transfers between devices  95.2 us (36%)
  blocking collectives  91.2 us (35%)
  starting transfers between devices  24.5 us (9%)
  matrix products  16 us (6%)
  between operations  13.7 us (5%)
  local copies, waits for them, and re-layouts  11.6 us (4%)
  other arithmetic  8.26 us (3%)
    all_to_all x1, blocking collectives, per_device(): lax.all_to_all(partial_out, 'tp', split_axis=0, concat_axis=0, tiled=True)  55 us
    all_gather x1, waiting for transfers between devices, per_device(): lax.all_gather(arrived, 'tp', axis=0, tiled=True)  53.9 us
    all_to_all x1, blocking collectives, per_device(): lax.all_to_all(outbound, 'sp', split_axis=0, concat_axis=0, tiled=True)  36.3 us
    all_to_all x1, waiting for transfers between devices, per_device(): lax.all_to_all(summed.astype(jnp.bfloat16), 'sp', split_axis=0, concat_ax...  22.1 us
    all_to_all x1, waiting for transfers between devices, sum_at_owner(): pieces = lax.all_to_all(split_up(array, dim, size), axis, 0, 0, tiled=True)  17.7 us
    all_to_all x1, starting transfers between devices, per_device(): lax.all_to_all(summed.astype(jnp.bfloat16), 'sp', split_axis=0, concat_ax...  14.3 us
    dot_general x1, matrix products, expert_part(): jnp.dot(hidden, down_proj[0], preferred_element_type=jnp.float32)  9.1 us
    reshape x1, local copies, waits for them, and re-layouts, expert_part(): flattened = rows_in.reshape(-1, in_shape[-1])  7.21 us
  transfers between devices with their start and end apart: 4, of which 4 were waited for; matrix products, arithmetic and copies ran while one was open for 1% of the time, Pallas kernels for 0%

commit v1 on v0

v1 whole, which is shorter than its diff:
```python
import jax
import jax.numpy as jnp
from jax import lax
from jax.sharding import PartitionSpec as P

HEAD = 64
WINDOW = 128


norm_epsilon = 1e-06


SP = ("zg", "zl", "core")
TP = ("y", "xh", "xl")
SIZES = (4, 4, 2, 4, 2, 2)
ROUTE = ("zg", "zl", "core", "xl")
TEAM = ("y", "xh")


def from_behind(block, axis, distance):
    devices = range(lax.axis_size(axis))
    route = [(i - distance, i) for i in devices if i - distance in devices]
    return lax.ppermute(block, axis, route)


def exchange(blocks, axis):
    return lax.all_to_all(blocks, axis, 0, 0, tiled=True)


def sum_at_owner(array, axis):
    size = lax.axis_size(axis)
    pieces = exchange(array.reshape(size, -1, array.shape[-1]), axis)
    return jnp.sum(pieces.astype(jnp.float32), axis=0)


def to_team(weight):
    return lax.ppermute(weight, ("core", "xl"), [(0, 0), (1, 2), (2, 1), (3, 3)])


def across(block):
    return lax.ppermute(block, "core", [(0, 1), (1, 0)])


def rotary(values_in, positions, head_count):
    halfway = HEAD // 2
    frequency = 10000.0 ** (-jnp.arange(halfway, dtype=jnp.float32) * 2.0 / HEAD)
    angles = positions.astype(jnp.float32)[:, None] * frequency[None, :]
    cosine = jnp.cos(angles)[:, None, :]
    sine_part = jnp.sin(angles)[:, None, :]
    reshaped = values_in.astype(jnp.float32).reshape(values_in.shape[0], head_count, HEAD)
    front_part = reshaped[..., :halfway]
    back_part = reshaped[..., halfway:]
    turned = jnp.concatenate(
        [front_part * cosine - back_part * sine_part, back_part * cosine + front_part * sine_part],
        -1,
    )
    return turned.astype(jnp.bfloat16)


def attend(query_blocks, key_pairs, value_pairs, sink_grid, key_start):
    block_count = query_blocks.shape[0]
    window_len = query_blocks.shape[1]
    scores = jnp.einsum(
        "bqkgd,bskd->bkgqs", query_blocks, key_pairs, preferred_element_type=jnp.float32
    ) * HEAD ** (-0.5)
    row_idx = jnp.arange(window_len)[:, None]
    col_idx = jnp.arange(2 * window_len)[None, :]
    distance = row_idx - col_idx + window_len
    key_pos = key_start + jnp.arange(block_count)[:, None, None] * window_len + col_idx[None]
    allowed = (distance >= 0)[None] & (distance < window_len)[None] & (key_pos >= 0)
    scores = jnp.where(allowed[:, None, None], scores, -jnp.inf)
    sink_full = sink_grid[None, :, :, None]
    highest = jnp.maximum(jnp.max(scores, -1), sink_full)
    exp_scores = jnp.exp(scores - highest[..., None])
    denominator = jnp.sum(exp_scores, -1) + jnp.exp(sink_full - highest)
    weighted = jnp.einsum(
        "bkgqs,bskd->bkgqd",
        exp_scores.astype(jnp.bfloat16),
        value_pairs,
        preferred_element_type=jnp.float32,
    )
    normalized = weighted / denominator[..., None]
    return (
        jnp.transpose(normalized, (0, 3, 1, 2, 4))
        .astype(jnp.bfloat16)
        .reshape(block_count * window_len, -1)
    )


def slots(ids):
    rows = ids.shape[0]
    earlier = (jnp.arange(rows)[:, None] > jnp.arange(rows)[None, :])[:, None, :, None]
    same = ids[:, :, None, None] == ids[None, None]
    rank = jnp.sum((same & earlier).astype(jnp.int32), (2, 3))
    return (ids // 2) * 4 + rank * 2 + ids % 2


def expert_part(rows_in, weights):
    total = 0.0
    for gate, up, down in weights:
        gate_val = jnp.dot(rows_in, gate, preferred_element_type=jnp.float32)
        up_val = jnp.dot(rows_in, up, preferred_element_type=jnp.float32)
        hidden = (jax.nn.silu(gate_val) * up_val).astype(jnp.bfloat16)
        total = total + jnp.dot(hidden, down, preferred_element_type=jnp.float32)
    return total.astype(jnp.bfloat16)


def per_device(
    queries,
    key_rows,
    values,
    sink_logits,
    residual,
    out_weight,
    norm_gain,
    expert_ids,
    route_weight,
    gate_proj,
    up_proj,
    down_proj,
):
    local_len = queries.shape[0]
    q_heads = sink_logits.shape[0]
    kv_heads = key_rows.shape[1] // HEAD
    group_size = q_heads // kv_heads
    window_len = WINDOW
    seq_start = lax.axis_index(SP) * local_len
    rim_pair = jnp.stack([key_rows[local_len - window_len :], values[local_len - window_len :]])
    rim_pair = from_behind(rim_pair, SP, 1)
    gate = to_team(gate_proj[0])
    key_ext = jnp.concatenate([rim_pair[0], key_rows], 0)
    val_ext = jnp.concatenate([rim_pair[1], values], 0)
    positions = seq_start + jnp.arange(local_len, dtype=jnp.int32)
    ext_positions = seq_start - window_len + jnp.arange(local_len + window_len, dtype=jnp.int32)
    rot_query = rotary(queries, positions, q_heads)
    rot_key = rotary(key_ext, ext_positions, kv_heads)
    block_count = local_len // window_len
    query_blocks = rot_query.reshape(block_count, window_len, kv_heads, group_size, HEAD)
    key_blocks = rot_key.reshape(block_count + 1, window_len, kv_heads, HEAD)
    value_blocks = val_ext.reshape(block_count + 1, window_len, kv_heads, HEAD)
    key_pairs = jnp.concatenate([key_blocks[:-1], key_blocks[1:]], 1)
    value_pairs = jnp.concatenate([value_blocks[:-1], value_blocks[1:]], 1)
    sink_grid = sink_logits.reshape(kv_heads, group_size)
    attended = attend(query_blocks, key_pairs, value_pairs, sink_grid, seq_start - window_len)
    tok_rows, width = residual.shape
    shares = jnp.dot(attended, out_weight, preferred_element_type=jnp.float32).astype(jnp.bfloat16)
    shares, up_proj, down_proj = lax.optimization_barrier((shares, up_proj, down_proj))
    projected = sum_at_owner(shares, TP)
    up = to_team(up_proj[0])
    down = to_team(down_proj[0])
    middle = (residual.astype(jnp.float32) + projected).astype(jnp.bfloat16)
    middle_f = middle.astype(jnp.float32)
    normed = (
        middle_f
        * lax.rsqrt(jnp.mean(middle_f * middle_f, -1, keepdims=True) + norm_epsilon)
        * norm_gain
    ).astype(jnp.bfloat16)

    routes = 64
    first = lax.axis_index(TP) * tok_rows
    own_ids = lax.dynamic_slice_in_dim(expert_ids, first, tok_rows, 0)
    own_weights = lax.dynamic_slice_in_dim(route_weight, first, tok_rows, 0)
    slot = slots(own_ids)
    chosen = jnp.arange(routes, dtype=jnp.int32)[:, None, None] == slot[None]
    outbound = jnp.dot(
        jnp.any(chosen, -1).astype(jnp.bfloat16), normed, preferred_element_type=jnp.float32
    ).astype(jnp.bfloat16)
    arrived = exchange(outbound.reshape(routes, 16, width // 16), ROUTE).reshape(routes, width)

    team = 8
    gathered = exchange(jnp.broadcast_to(arrived[None], (team, routes, width)), TEAM)
    mine = (gate, up, down)
    others = tuple(across(w) for w in mine)
    partial_out = expert_part(gathered.reshape(team * routes, width), (mine, others))
    summed = sum_at_owner(partial_out, TEAM).astype(jnp.bfloat16)
    returned = exchange(summed.reshape(routes, 16, width // 16), ROUTE).reshape(routes, width)

    routed = 0.0
    for k in range(2):
        picked = jnp.dot(
            (slot[:, k, None] == jnp.arange(routes, dtype=jnp.int32)).astype(jnp.bfloat16),
            returned,
            preferred_element_type=jnp.float32,
        )
        routed = routed + picked * own_weights[:, k, None]
    return (middle_f + routed).astype(jnp.bfloat16)


def solution(mesh):
    fine = jax.sharding.Mesh(mesh.devices.reshape(SIZES), SP + TP)
    return jax.shard_map(
        per_device,
        mesh=fine,
        in_specs=(
            P(SP, TP),
            P(SP, TP),
            P(SP, TP),
            P(TP),
            P(SP + TP, None),
            P(TP, None),
            P(),
            P(SP, None),
            P(SP, None),
            P(SP, None, TP),
            P(SP, None, TP),
            P(SP, TP, None),
        ),
        out_specs=P(SP + TP, None),
        check_vma=False,
    )
```

time: 261 us -> 224 us (0.86)
  blocking collectives: 91.2 us -> 71 us
  between operations: 13.7 us -> 0.37 us
  starting transfers between devices: 24.5 us -> 35.6 us
  waiting for transfers between devices: 95.2 us -> 85.5 us
  local copies, waits for them, and re-layouts: 11.6 us -> 5.3 us
  other arithmetic: 8.26 us -> 2.83 us
  matrix products: 16 us -> 20.4 us
    all_gather x1 -> x0, waiting for transfers between devices: 53.9 us -> none  [per_device(): lax.all_gather(arrived, 'tp', axis=0, tiled=True)]
    ppermute x0 -> x6, waiting for transfers between devices: none -> 44.7 us  [the longest x3 44.7 us: to_team(): lax.ppermute(weight, ('core', 'xl'), [(0, 0), (1, 2), (2, 1), (3, 3)])]
    all_to_all x2, blocking collectives: 91.2 us -> 71 us  [exchange(): return lax.all_to_all(blocks, axis, 0, 0, tiled=True)]
    ppermute x0 -> x6, starting transfers between devices: none -> 15.7 us  [the longest x3 10 us: to_team(): lax.ppermute(weight, ('core', 'xl'), [(0, 0), (1, 2), (2, 1), (3, 3)])]
    reshape x4 -> x0, local copies, waits for them, and re-layouts: 7.58 us -> none  [the longest x1 7.21 us: expert_part(): flattened = rows_in.reshape(-1, in_shape[-1])]
    all_to_all x2 -> x3, starting transfers between devices: 19.5 us -> 14.9 us  [exchange(): return lax.all_to_all(blocks, axis, 0, 0, tiled=True)]
    dot_general x4 -> x7, matrix products: 14 us -> 18.5 us  [the longest x2 12.4 us: expert_part(): total = total + jnp.dot(hidden, down, preferred_element_type=jnp.float32)]
    reduce_sum x3 -> x1, other arithmetic: 3.25 us -> 0.19 us  [slots(): rank = jnp.sum((same & earlier).astype(jnp.int32), (2, 3))]
  transfers between devices with their start and end apart: 4 -> 10, of which waited for: 4 -> 6; matrix products, arithmetic and copies ran while one was open for 1% -> 6% of each run, Pallas kernels for 0% -> 0%
where the time goes in v1:
time: 224 us; the launch traced here: 221 us
  waiting for transfers between devices  85.5 us (38%)
  blocking collectives  71 us (32%)
  starting transfers between devices  35.6 us (16%)
  matrix products  20.4 us (9%)
  local copies, waits for them, and re-layouts  5.3 us (2%)
  other arithmetic  2.83 us (1%)
    all_to_all x2, blocking collectives, exchange(): return lax.all_to_all(blocks, axis, 0, 0, tiled=True)  71 us
    ppermute x3, waiting for transfers between devices, to_team(): lax.ppermute(weight, ('core', 'xl'), [(0, 0), (1, 2), (2, 1), (3, 3)])  44.7 us
    all_to_all x3, waiting for transfers between devices, exchange(): return lax.all_to_all(blocks, axis, 0, 0, tiled=True)  39.2 us
    all_to_all x3, starting transfers between devices, exchange(): return lax.all_to_all(blocks, axis, 0, 0, tiled=True)  14.9 us
    dot_general x2, matrix products, expert_part(): total = total + jnp.dot(hidden, down, preferred_element_type=jnp.float32)  12.4 us
    ppermute x3, starting transfers between devices, to_team(): lax.ppermute(weight, ('core', 'xl'), [(0, 0), (1, 2), (2, 1), (3, 3)])  10 us
    ppermute x3, starting transfers between devices, across(): return lax.ppermute(block, 'core', [(0, 1), (1, 0)])  5.73 us
    ppermute x1, starting transfers between devices, from_behind(): return lax.ppermute(block, axis, route)  4.92 us
  transfers between devices with their start and end apart: 10, of which 6 were waited for; matrix products, arithmetic and copies ran while one was open for 6% of the time, Pallas kernels for 0%

profile of v1, /device:TPU:1, one launch (start us, length us, event | category | flops | bytes accessed | tf_op | source)
XLA Modules:
  0.0 221.0 jit_solution(4831564267710439237)
XLA Ops:
  0.0 0.8 slice_bitcast_fusion.2
  0.8 4.9 %collective-permute-start = (bf16[2,128,64]{1,2,0:T(8,128)(2,1)S(1)}, bf16[2,128,64]{1,2,0:T(8,128)(2,1)S(1)}, u32[]{:S(2)}, u32[]{:S(2)}) collective-permute-start(bf16[2,128,64]{1,2,0:T(8,128)(2,1)S(1)} %pad_maximum_fusion.2), channel_id=1, source_target_pairs={{0,16},{16,32},{32,48},{48,64},{64,80},{80,96},{96,112},{112,128},... | collective-permute-start | bytes 98312 | tf_op jit(solution)/shard_map/ppermute | solution.py:23
  5.8 0.9 copy.31
  6.8 0.1 add_compare_fusion
  6.9 0.2 multiply_cosine_fusion.1
  7.1 0.1 broadcast_and_fusion
  7.3 0.8 slice.72
  8.1 1.5 collective-permute-done
  9.6 0.8 maximum_convert_fusion
  10.4 0.3 fusion.43
  10.7 0.3 fusion.59
  11.1 0.1 fusion.8
  11.2 0.1 exponential_add_fusion
  11.3 0.2 fusion.7
  11.6 1.4 convolution_convert_fusion
  13.1 5.4 %all-to-all-start = ((bf16[16,16,2048]{2,1,0:T(8,128)(2,1)}), bf16[16,16,2048]{2,1,0:T(8,128)(2,1)S(1)}, u32[]{:S(2)}, u32[]{:S(2)}) async-start(bf16[16,16,2048]{2,1,0:T(8,128)(2,1)} %bitcast.18), calls=%async_computation | async-start | bytes 2097152 | tf_op jit(solution)/shard_map/all_to_all | solution.py:27
  18.5 0.1 constant_dynamic-slice_fusion.1
  18.6 0.2 convert_reduce_fusion.1
  18.7 0.1 fusion.54
  18.8 0.1 fusion.51
  18.9 18.1 %all-to-all-done = bf16[16,16,2048]{2,1,0:T(8,128)(2,1)S(1)} async-done(((bf16[16,16,2048]{2,1,0:T(8,128)(2,1)}), bf16[16,16,2048]{2,1,0:T(8,128)(2,1)S(1)}, u32[]{:S(2)}, u32[]{:S(2)}) %all-to-all-start) | async-done | bytes 1048608 | tf_op jit(solution)/shard_map/all_to_all | solution.py:27
  37.1 0.1 convert_reduce_fusion
  37.2 0.1 fusion.20
  37.4 0.3 fusion.5
  37.7 35.7 %all_to_all.25 = bf16[64,16,128]{2,1,0:T(8,128)(2,1)S(1)} all-to-all(bf16[64,16,128]{2,1,0:T(8,128)(2,1)S(1)} %bitcast.117), channel_id=1, replica_groups=mesh['zg'=4,'zl'=4,'core'=2,'y'=4,'xh'=2,'xl'=2] {'zg','zl','core','xl'}, dimensions={0} | all-to-all | bytes 524288 | tf_op jit(solution)/shard_map/all_to_all | solution.py:27
  73.5 1.6 broadcast_in_dim.15
  75.1 3.6 %all-to-all-start.2 = ((bf16[8,64,2048]{2,1,0:T(8,128)(2,1)}), bf16[8,64,2048]{2,1,0:T(8,128)(2,1)S(1)}, u32[]{:S(2)}, u32[]{:S(2)}) async-start(bf16[8,64,2048]{2,1,0:T(8,128)(2,1)} %broadcast_in_dim.15), calls=%async_computation.2 | async-start | bytes 4194304 | tf_op jit(solution)/shard_map/all_to_all | solution.py:27
  78.7 4.4 %collective-permute-start.1 = (bf16[2048,256]{1,0:T(8,128)(2,1)}, bf16[2048,256]{1,0:T(8,128)(2,1)}, u32[]{:S(2)}, u32[]{:S(2)}) collective-permute-start(bf16[2048,256]{1,0:T(8,128)(2,1)} %bitcast.124), channel_id=1, source_target_pairs={{0,0},{1,16},{16,1},{17,17},{2,2},{3,18},{18,3},{19,19},{4,4},{5,2... | collective-permute-start | bytes 3145736 | tf_op jit(solution)/shard_map/ppermute | solution.py:37
  83.1 1.9 collective-permute-start.2
  85.0 3.6 %collective-permute-start.3 = (bf16[256,2048]{1,0:T(8,128)(2,1)}, bf16[256,2048]{1,0:T(8,128)(2,1)}, u32[]{:S(2)}, u32[]{:S(2)}) collective-permute-start(bf16[256,2048]{1,0:T(8,128)(2,1)} %bitcast.126), channel_id=1, source_target_pairs={{0,0},{1,16},{16,1},{17,17},{2,2},{3,18},{18,3},{19,19},{4,4},{5,2... | collective-permute-start | bytes 3145736 | tf_op jit(solution)/shard_map/ppermute | solution.py:37
  88.7 26.1 %collective-permute-done.1 = bf16[2048,256]{1,0:T(8,128)(2,1)} collective-permute-done((bf16[2048,256]{1,0:T(8,128)(2,1)}, bf16[2048,256]{1,0:T(8,128)(2,1)}, u32[]{:S(2)}, u32[]{:S(2)}) %collective-permute-start.1) | collective-permute-done | bytes 1048608 | tf_op jit(solution)/shard_map/ppermute | solution.py:37
  114.8 1.9 collective-permute-start.4
  116.7 9.3 %collective-permute-done.2 = bf16[2048,256]{1,0:T(8,128)(2,1)} collective-permute-done((bf16[2048,256]{1,0:T(8,128)(2,1)}, bf16[2048,256]{1,0:T(8,128)(2,1)}, u32[]{:S(2)}, u32[]{:S(2)}) %collective-permute-start.2) | collective-permute-done | bytes 1048608 | tf_op jit(solution)/shard_map/ppermute | solution.py:37
  126.0 1.9 collective-permute-start.5
  128.0 9.3 %collective-permute-done.3 = bf16[256,2048]{1,0:T(8,128)(2,1)} collective-permute-done((bf16[256,2048]{1,0:T(8,128)(2,1)}, bf16[256,2048]{1,0:T(8,128)(2,1)}, u32[]{:S(2)}, u32[]{:S(2)}) %collective-permute-start.3) | collective-permute-done | bytes 1048608 | tf_op jit(solution)/shard_map/ppermute | solution.py:37
  137.3 1.9 collective-permute-start.6
  139.2 1.9 fusion.64
  141.2 2.8 %fusion.65 = f32[512,256]{1,0:T(8,128)} fusion(bf16[512,2048]{1,0:T(8,128)(2,1)S(1)} %bitcast.109, bf16[2048,256]{1,0:T(8,128)(2,1)} %collective-permute-done.4), kind=kOutput, calls=%fused_computation.124 | convolution fusion | flops 536870912 | bytes 3670016 | tf_op jit(solution)/shard_map/dot_general | solution.py:101
  143.9 5.8 %fusion.12 = f32[512,2048]{1,0:T(8,128)} fusion(bf16[256,2048]{1,0:T(8,128)(2,1)} %collective-permute-done.3, f32[512,256]{1,0:T(8,128)S(1)} %fusion.64, bf16[512,2048]{1,0:T(8,128)(2,1)S(1)} %bitcast.110, bf16[2048,256]{1,0:T(8,128)(2,1)} %collective-permute-done.2), kind=kOutput, calls=%fused_computation.22 | convolution fusion | flops 1074528256 | bytes 8912896 | tf_op jit(solution)/shard_map/dot_general | solution.py:104
  149.7 6.6 %add_convert_fusion = bf16[512,2048]{1,0:T(8,128)(2,1)} fusion(f32[512,2048]{1,0:T(8,128)} %fusion.12, bf16[256,2048]{1,0:T(8,128)(2,1)} %collective-permute-done.6, f32[512,256]{1,0:T(8,128)} %fusion.65, bf16[512,2048]{1,0:T(8,128)(2,1)S(1)} %bitcast.111, bf16[2048,256]{1,0:T(8,128)(2,1)} %collective-permute-done.5), kind=kOutput, calls=%fused_computation | convolution fusion | flops 1076625408 | bytes 11010048 | tf_op jit(solution)/shard_map/dot_general | solution.py:104
  156.4 35.3 %all_to_all.26 = bf16[8,64,2048]{2,1,0:T(8,128)(2,1)S(1)} all-to-all(bf16[8,64,2048]{2,1,0:T(8,128)(2,1)} %bitcast.112), channel_id=1, replica_groups=mesh['zg'=4,'zl'=4,'core'=2,'y'=4,'xh'=2,'xl'=2] {'y','xh'}, dimensions={0} | all-to-all | bytes 4194304 | tf_op jit(solution)/shard_map/all_to_all | solution.py:27
  191.7 0.4 reduce_sum.52
  192.0 0.8 copy.48
  192.8 6.0 %all-to-all-start.4 = ((bf16[64,16,128]{2,1,0:T(8,128)(2,1)}), bf16[64,16,128]{2,1,0:T(8,128)(2,1)S(1)}, u32[]{:S(2)}, u32[]{:S(2)}) async-start(bf16[64,16,128]{2,1,0:T(8,128)(2,1)} %bitcast.52), calls=%async_computation.4 | async-start | bytes 524288 | tf_op jit(solution)/shard_map/all_to_all | solution.py:27
  198.8 0.1 constant_dynamic-slice_fusion
  198.9 21.0 %all-to-all-done.4 = bf16[64,16,128]{2,1,0:T(8,128)(2,1)S(1)} async-done(((bf16[64,16,128]{2,1,0:T(8,128)(2,1)}), bf16[64,16,128]{2,1,0:T(8,128)(2,1)S(1)}, u32[]{:S(2)}, u32[]{:S(2)}) %all-to-all-start.4) | async-done | bytes 262176 | tf_op jit(solution)/shard_map/all_to_all | solution.py:27
  219.9 0.2 convolution_multiply_fusion.1
  220.1 0.9 fusion.2
  (43 shorter events, 0.5 us)
Async XLA Ops:
  0.0 11.6 %copy-start = (bf16[128,2048]{1,0:T(8,128)(2,1)S(1)}, bf16[128,2048]{1,0:T(8,128)(2,1)}, u32[]{:S(2)}) copy-start(bf16[128,2048]{1,0:T(8,128)(2,1)} %param.17) | copy-start | bytes 1572868
  0.0 11.3 %copy-start.1 = (bf16[256,64]{0,1:T(8,128)(2,1)S(1)}, bf16[256,64]{0,1:T(8,128)(2,1)}, u32[]{:S(2)}) copy-start(bf16[256,64]{0,1:T(8,128)(2,1)} %param.14) | copy-start | bytes 98308
  0.0 11.0 %copy-start.5 = (f32[2]{0:T(128)S(1)}, f32[2]{0:T(128)}, u32[]{:S(2)}) copy-start(f32[2]{0:T(128)} %param.15) | copy-start | bytes 28
  0.8 8.8 %collective-permute-start = (bf16[2,128,64]{1,2,0:T(8,128)(2,1)S(1)}, bf16[2,128,64]{1,2,0:T(8,128)(2,1)S(1)}, u32[]{:S(2)}, u32[]{:S(2)}) collective-permute-start(bf16[2,128,64]{1,2,0:T(8,128)(2,1)S(1)} %pad_maximum_fusion.2), channel_id=1, source_target_pairs={{0,16},{16,32},{32,48},{48,64},{64,80},{80,96},{96,112},{112,128},... | collective-permute-start | bytes 98312 | tf_op jit(solution)/shard_map/ppermute | solution.py:23
  11.5 6.9 %copy-start.4 = (s32[256,2]{0,1:T(2,128)S(1)}, s32[256,2]{0,1:T(2,128)}, u32[]{:S(2)}) copy-start(s32[256,2]{0,1:T(2,128)} %param.19) | copy-start | bytes 6148
  11.6 25.6 %copy-start.2 = (bf16[16,2048]{1,0:T(8,128)(2,1)S(1)}, bf16[16,2048]{1,0:T(8,128)(2,1)}, u32[]{:S(2)}) copy-start(bf16[16,2048]{1,0:T(8,128)(2,1)} %param.16) | copy-start | bytes 196612
  13.1 24.3 %copy-start.3 = (f32[2048]{0:T(1024)S(1)}, f32[2048]{0:T(1024)}, u32[]{:S(2)}) copy-start(f32[2048]{0:T(1024)} %param.18) | copy-start | bytes 24580
  13.1 24.0 %all-to-all-start = ((bf16[16,16,2048]{2,1,0:T(8,128)(2,1)}), bf16[16,16,2048]{2,1,0:T(8,128)(2,1)S(1)}, u32[]{:S(2)}, u32[]{:S(2)}) async-start(bf16[16,16,2048]{2,1,0:T(8,128)(2,1)} %bitcast.18), calls=%async_computation | async-start | bytes 2097152 | tf_op jit(solution)/shard_map/all_to_all | solution.py:27
  75.1 64.1 %all-to-all-start.2 = ((bf16[8,64,2048]{2,1,0:T(8,128)(2,1)}), bf16[8,64,2048]{2,1,0:T(8,128)(2,1)S(1)}, u32[]{:S(2)}, u32[]{:S(2)}) async-start(bf16[8,64,2048]{2,1,0:T(8,128)(2,1)} %broadcast_in_dim.15), calls=%async_computation.2 | async-start | bytes 4194304 | tf_op jit(solution)/shard_map/all_to_all | solution.py:27
  78.7 36.1 %collective-permute-start.1 = (bf16[2048,256]{1,0:T(8,128)(2,1)}, bf16[2048,256]{1,0:T(8,128)(2,1)}, u32[]{:S(2)}, u32[]{:S(2)}) collective-permute-start(bf16[2048,256]{1,0:T(8,128)(2,1)} %bitcast.124), channel_id=1, source_target_pairs={{0,0},{1,16},{16,1},{17,17},{2,2},{3,18},{18,3},{19,19},{4,4},{5,2... | collective-permute-start | bytes 3145736 | tf_op jit(solution)/shard_map/ppermute | solution.py:37
  83.1 42.9 %collective-permute-start.2 = (bf16[2048,256]{1,0:T(8,128)(2,1)}, bf16[2048,256]{1,0:T(8,128)(2,1)}, u32[]{:S(2)}, u32[]{:S(2)}) collective-permute-start(bf16[2048,256]{1,0:T(8,128)(2,1)} %bitcast.125), channel_id=1, source_target_pairs={{0,0},{1,16},{16,1},{17,17},{2,2},{3,18},{18,3},{19,19},{4,4},{5,2... | collective-permute-start | bytes 3145736 | tf_op jit(solution)/shard_map/ppermute | solution.py:37
  85.0 52.2 %collective-permute-start.3 = (bf16[256,2048]{1,0:T(8,128)(2,1)}, bf16[256,2048]{1,0:T(8,128)(2,1)}, u32[]{:S(2)}, u32[]{:S(2)}) collective-permute-start(bf16[256,2048]{1,0:T(8,128)(2,1)} %bitcast.126), channel_id=1, source_target_pairs={{0,0},{1,16},{16,1},{17,17},{2,2},{3,18},{18,3},{19,19},{4,4},{5,2... | collective-permute-start | bytes 3145736 | tf_op jit(solution)/shard_map/ppermute | solution.py:37
  114.8 26.3 %collective-permute-start.4 = (bf16[2048,256]{1,0:T(8,128)(2,1)}, bf16[2048,256]{1,0:T(8,128)(2,1)}, u32[]{:S(2)}, u32[]{:S(2)}) collective-permute-start(bf16[2048,256]{1,0:T(8,128)(2,1)} %collective-permute-done.1), channel_id=1, source_target_pairs={{0,16},{16,0},{1,17},{17,1},{2,18},{18,2},{3,19},{19,3},{4,20},{20... | collective-permute-start | bytes 3145736 | tf_op jit(solution)/shard_map/ppermute | solution.py:41
  126.0 23.7 %collective-permute-start.5 = (bf16[2048,256]{1,0:T(8,128)(2,1)}, bf16[2048,256]{1,0:T(8,128)(2,1)}, u32[]{:S(2)}, u32[]{:S(2)}) collective-permute-start(bf16[2048,256]{1,0:T(8,128)(2,1)} %collective-permute-done.2), channel_id=1, source_target_pairs={{0,16},{16,0},{1,17},{17,1},{2,18},{18,2},{3,19},{19,3},{4,20},{20... | collective-permute-start | bytes 3145736 | tf_op jit(solution)/shard_map/ppermute | solution.py:41
  137.3 12.5 %collective-permute-start.6 = (bf16[256,2048]{1,0:T(8,128)(2,1)}, bf16[256,2048]{1,0:T(8,128)(2,1)}, u32[]{:S(2)}, u32[]{:S(2)}) collective-permute-start(bf16[256,2048]{1,0:T(8,128)(2,1)} %collective-permute-done.3), channel_id=1, source_target_pairs={{0,16},{16,0},{1,17},{17,1},{2,18},{18,2},{3,19},{19,3},{4,20},{20... | collective-permute-start | bytes 3145736 | tf_op jit(solution)/shard_map/ppermute | solution.py:41
  191.7 7.1 %copy-start.6 = (f32[256,2]{0,1:T(2,128)S(1)}, f32[256,2]{0,1:T(2,128)}, u32[]{:S(2)}) copy-start(f32[256,2]{0,1:T(2,128)} %param.20) | copy-start | bytes 6148
  192.8 27.1 %all-to-all-start.4 = ((bf16[64,16,128]{2,1,0:T(8,128)(2,1)}), bf16[64,16,128]{2,1,0:T(8,128)(2,1)S(1)}, u32[]{:S(2)}, u32[]{:S(2)}) async-start(bf16[64,16,128]{2,1,0:T(8,128)(2,1)} %bitcast.52), calls=%async_computation.4 | async-start | bytes 524288 | tf_op jit(solution)/shard_map/all_to_all | solution.py:27

commit v2 on v1

--- a/solution.py
+++ b/solution.py
@@ -1,7 +1,10 @@
 import jax
 import jax.numpy as jnp
 from jax import lax
+from jax.experimental import pallas as pl
+from jax.experimental.pallas import tpu as pltpu
 from jax.sharding import PartitionSpec as P
+
 
 HEAD = 64
 WINDOW = 128
@@ -33,12 +36,12 @@
     return jnp.sum(pieces.astype(jnp.float32), axis=0)
 
 
-def to_team(weight):
-    return lax.ppermute(weight, ("core", "xl"), [(0, 0), (1, 2), (2, 1), (3, 3)])
-
-
-def across(block):
-    return lax.ppermute(block, "core", [(0, 1), (1, 0)])
+def turn(weight):
+    return lax.ppermute(weight, ("core", "xl"), [(0, 2), (2, 3), (3, 1), (1, 0)])
+
+
+def pass_on(weight):
+    return lax.ppermute(weight, ("core", "xl"), [(0, 2), (3, 1)])
 
 
 def rotary(values_in, positions, head_count):
@@ -87,22 +90,98 @@
     )
 
 
-def slots(ids):
-    rows = ids.shape[0]
-    earlier = (jnp.arange(rows)[:, None] > jnp.arange(rows)[None, :])[:, None, :, None]
-    same = ids[:, :, None, None] == ids[None, None]
-    rank = jnp.sum((same & earlier).astype(jnp.int32), (2, 3))
-    return (ids // 2) * 4 + rank * 2 + ids % 2
-
-
-def expert_part(rows_in, weights):
-    total = 0.0
-    for gate, up, down in weights:
-        gate_val = jnp.dot(rows_in, gate, preferred_element_type=jnp.float32)
-        up_val = jnp.dot(rows_in, up, preferred_element_type=jnp.float32)
-        hidden = (jax.nn.silu(gate_val) * up_val).astype(jnp.bfloat16)
-        total = total + jnp.dot(hidden, down, preferred_element_type=jnp.float32)
-    return total.astype(jnp.bfloat16)
+IN_VMEM = pl.BlockSpec(memory_space=pltpu.VMEM)
+
+
+def plan_kernel(ids_ref, ids_row_ref, spread_ref, collect_ref):
+    rows, picks = ids_ref.shape
+    routes = spread_ref.shape[0]
+    down = lax.broadcasted_iota(jnp.int32, (rows, rows), 0)
+    right = lax.broadcasted_iota(jnp.int32, (rows, rows), 1)
+    spread = jnp.zeros((routes, rows), jnp.float32)
+    for k in range(picks):
+        col, row = ids_ref[:, k : k + 1], ids_row_ref[k : k + 1, :]
+        rank_col = jnp.zeros((rows, 1), jnp.int32)
+        rank_row = jnp.zeros((1, rows), jnp.int32)
+        for j in range(picks):
+            other_col, other_row = ids_ref[:, j : j + 1], ids_row_ref[j : j + 1, :]
+            before = jnp.where((col == other_row) & (right < down), 1, 0)
+            rank_col = rank_col + jnp.sum(before, 1, keepdims=True)
+            before = jnp.where((other_col == row) & (down < right), 1, 0)
+            rank_row = rank_row + jnp.sum(before, 0, keepdims=True)
+        slot_col = (col >> 1) * 4 + rank_col * 2 + (col & 1)
+        slot_row = (row >> 1) * 4 + rank_row * 2 + (row & 1)
+        collect_ref[k * rows : (k + 1) * rows, :] = jnp.where(
+            lax.broadcasted_iota(jnp.int32, (rows, routes), 1) == slot_col, 1.0, 0.0
+        ).astype(jnp.bfloat16)
+        spread = spread + jnp.where(
+            lax.broadcasted_iota(jnp.int32, (routes, rows), 0) == slot_row, 1.0, 0.0
+        )
+    spread_ref[...] = spread.astype(jnp.bfloat16)
+
+
+def plan(ids, routes):
+    rows, picks = ids.shape
+    return pl.pallas_call(
+        plan_kernel,
+        out_shape=(
+            jax.ShapeDtypeStruct((routes, rows), jnp.bfloat16),
+            jax.ShapeDtypeStruct((picks * rows, routes), jnp.bfloat16),
+        ),
+        in_specs=[IN_VMEM] * 2,
+        out_specs=[IN_VMEM] * 2,
+        cost_estimate=pl.CostEstimate(flops=10**6, bytes_accessed=8192, transcendentals=0),
+    )(ids, ids.T)
+
+
+def hold_kernel(in_ref, out_ref):
+    out_ref[...] = in_ref[...]
+
+
+def hold(array):
+    return pl.pallas_call(
+        hold_kernel,
+        out_shape=jax.ShapeDtypeStruct(array.shape, array.dtype),
+        in_specs=[IN_VMEM],
+        out_specs=IN_VMEM,
+        cost_estimate=pl.CostEstimate(flops=10**6, bytes_accessed=8192, transcendentals=0),
+    )(array)
+
+
+def expert_kernel(rows_ref, *refs):
+    *weights, out_ref = refs
+    rows = rows_ref[...]
+    parts = []
+    for gate, up, down in zip(*[iter(weights)] * 3, strict=True):
+        gate_val = jnp.dot(rows, gate[...], preferred_element_type=jnp.float32)
+        up_val = jnp.dot(rows, up[...], preferred_element_type=jnp.float32)
+        hidden = gate_val / (1.0 + jnp.exp(-gate_val)) * up_val
+        parts.append((hidden.astype(jnp.bfloat16), down))
+    chunk = 512
+    for at in range(0, out_ref.shape[1], chunk):
+        total = jnp.zeros((rows.shape[0], chunk), jnp.float32)
+        for hidden, down in parts:
+            total += jnp.dot(
+                hidden, down[:, at : at + chunk], preferred_element_type=jnp.float32
+            )
+        out_ref[:, at : at + chunk] = total.astype(jnp.bfloat16)
+
+
+def expert_part(rows, *weights):
+    count, width = rows.shape
+    units = sum(w.shape[1] for w in weights[::3])
+    return pl.pallas_call(
+        expert_kernel,
+        out_shape=jax.ShapeDtypeStruct((count, width), jnp.bfloat16),
+        in_specs=[IN_VMEM] * (1 + len(weights)),
+        out_specs=IN_VMEM,
+        compiler_params=pltpu.CompilerParams(vmem_limit_bytes=40 * 2**20),
+        cost_estimate=pl.CostEstimate(
+            flops=6 * count * units * width,
+            bytes_accessed=4 * count * width + 6 * units * width,
+            transcendentals=count * units,
+        ),
+    )(rows, *weights)
 
 
 def per_device(
@@ -127,7 +206,8 @@
     seq_start = lax.axis_index(SP) * local_len
     rim_pair = jnp.stack([key_rows[local_len - window_len :], values[local_len - window_len :]])
     rim_pair = from_behind(rim_pair, SP, 1)
-    gate = to_team(gate_proj[0])
+    own = (gate_proj[0], up_proj[0], down_proj[0])
+    gate = turn(own[0])
     key_ext = jnp.concatenate([rim_pair[0], key_rows], 0)
     val_ext = jnp.concatenate([rim_pair[1], values], 0)
     positions = seq_start + jnp.arange(local_len, dtype=jnp.int32)
@@ -143,11 +223,15 @@
     sink_grid = sink_logits.reshape(kv_heads, group_size)
     attended = attend(query_blocks, key_pairs, value_pairs, sink_grid, seq_start - window_len)
     tok_rows, width = residual.shape
+    first = lax.axis_index(TP) * tok_rows
+    own_ids = lax.dynamic_slice_in_dim(expert_ids, first, tok_rows, 0)
+    own_weights = lax.dynamic_slice_in_dim(route_weight, first, tok_rows, 0)
     shares = jnp.dot(attended, out_weight, preferred_element_type=jnp.float32).astype(jnp.bfloat16)
-    shares, up_proj, down_proj = lax.optimization_barrier((shares, up_proj, down_proj))
     projected = sum_at_owner(shares, TP)
-    up = to_team(up_proj[0])
-    down = to_team(down_proj[0])
+    up = turn(own[1])
+    down = turn(own[2])
+    routes = 64
+    spread, collect = plan(own_ids, routes)
     middle = (residual.astype(jnp.float32) + projected).astype(jnp.bfloat16)
     middle_f = middle.astype(jnp.float32)
     normed = (
@@ -156,33 +240,30 @@
         * norm_gain
     ).astype(jnp.bfloat16)
 
-    routes = 64
-    first = lax.axis_index(TP) * tok_rows
-    own_ids = lax.dynamic_slice_in_dim(expert_ids, first, tok_rows, 0)
-    own_weights = lax.dynamic_slice_in_dim(route_weight, first, tok_rows, 0)
-    slot = slots(own_ids)
-    chosen = jnp.arange(routes, dtype=jnp.int32)[:, None, None] == slot[None]
-    outbound = jnp.dot(
-        jnp.any(chosen, -1).astype(jnp.bfloat16), normed, preferred_element_type=jnp.float32
-    ).astype(jnp.bfloat16)
+    outbound = jnp.dot(spread, normed, preferred_element_type=jnp.float32).astype(jnp.bfloat16)
     arrived = exchange(outbound.reshape(routes, 16, width // 16), ROUTE).reshape(routes, width)
+    gate_too = pass_on(gate)
+    up_too = pass_on(up)
+    own_weights = hold(own_weights)
 
     team = 8
-    gathered = exchange(jnp.broadcast_to(arrived[None], (team, routes, width)), TEAM)
-    mine = (gate, up, down)
-    others = tuple(across(w) for w in mine)
-    partial_out = expert_part(gathered.reshape(team * routes, width), (mine, others))
+    spread_out = jnp.broadcast_to(arrived[None], (team, routes, width))
+    gathered = exchange(spread_out, TEAM)
+    down_too = pass_on(down)
+    kept = lax.axis_index("core") == lax.axis_index("xl")
+    second = [
+        jnp.where(kept, mine, passed)
+        for mine, passed in zip(own, (gate_too, up_too, down_too), strict=True)
+    ]
+    partial_out = expert_part(
+        gathered.reshape(team * routes, width), gate, up, down, *second
+    )
     summed = sum_at_owner(partial_out, TEAM).astype(jnp.bfloat16)
     returned = exchange(summed.reshape(routes, 16, width // 16), ROUTE).reshape(routes, width)
 
-    routed = 0.0
-    for k in range(2):
-        picked = jnp.dot(
-            (slot[:, k, None] == jnp.arange(routes, dtype=jnp.int32)).astype(jnp.bfloat16),
-            returned,
-            preferred_element_type=jnp.float32,
-        )
-        routed = routed + picked * own_weights[:, k, None]
+    picked = jnp.dot(collect, returned, preferred_element_type=jnp.float32)
+    picked = picked.reshape(2, tok_rows, width)
+    routed = picked[0] * own_weights[:, :1] + picked[1] * own_weights[:, 1:]
     return (middle_f + routed).astype(jnp.bfloat16)
 
 

time: 224 us -> 182 us (0.81)
  blocking collectives: 71 us -> 31.6 us
  waiting for transfers between devices: 85.5 us -> 64.9 us
  matrix products: 20.4 us -> 3.1 us
  starting transfers between devices: 35.6 us -> 49.4 us
  Pallas kernels: 0 us -> 8.1 us
  local copies, waits for them, and re-layouts: 5.3 us -> 12.7 us
  other arithmetic: 2.83 us -> 10.2 us
    ppermute x6, waiting for transfers between devices: 44.7 us -> 0.02 us  [the longest x3 0.01 us: turn(): lax.ppermute(weight, ('core', 'xl'), [(0, 2), (2, 3), (3, 1), (1, 0)])]
    all_to_all x2 -> x1, blocking collectives: 71 us -> 31.6 us  [exchange(): return lax.all_to_all(blocks, axis, 0, 0, tiled=True)]
    all_to_all x3 -> x4, waiting for transfers between devices: 39.2 us -> 63.3 us  [exchange(): return lax.all_to_all(blocks, axis, 0, 0, tiled=True)]
    dot_general x7 -> x2, matrix products: 18.5 us -> 1.15 us  [the longest x1 0.99 us: per_device(): jnp.dot(spread, normed, preferred_element_type=jnp.float32)]
    all_to_all x3 -> x4, starting transfers between devices: 14.9 us -> 31.8 us  [exchange(): return lax.all_to_all(blocks, axis, 0, 0, tiled=True)]
    pallas_call x0 -> x3, Pallas kernels: none -> 8.1 us  [the longest x1 5.28 us: expert_part(): pl.pallas_call(expert_kernel, out_shape=jax.ShapeDtypeStruct((count, widt...]
    select_n x0 -> x3, other arithmetic: none -> 6.26 us  [per_device(): jnp.where(kept, mine, passed)]
    unnamed x18 -> x31, local copies, waits for them, and re-layouts: 1.83 us -> 6.95 us
  transfers between devices with their start and end apart: 10 -> 11, of which waited for: 6 -> 5; matrix products, arithmetic and copies ran while one was open for 6% -> 9% of each run, Pallas kernels for 0% -> 2%
where the time goes in v2:
time: 182 us; the launch traced here: 180 us
  waiting for transfers between devices  64.9 us (36%)
  starting transfers between devices  49.4 us (27%)
  blocking collectives  31.6 us (17%)
  local copies, waits for them, and re-layouts  12.7 us (7%)
  other arithmetic  10.2 us (6%)
  Pallas kernels  8.1 us (4%)
  matrix products  3.1 us (2%)
    all_to_all x4, waiting for transfers between devices, exchange(): return lax.all_to_all(blocks, axis, 0, 0, tiled=True)  63.3 us
    all_to_all x4, starting transfers between devices, exchange(): return lax.all_to_all(blocks, axis, 0, 0, tiled=True)  31.8 us
    all_to_all x1, blocking collectives, exchange(): return lax.all_to_all(blocks, axis, 0, 0, tiled=True)  31.6 us
    ppermute x3, starting transfers between devices, turn(): lax.ppermute(weight, ('core', 'xl'), [(0, 2), (2, 3), (3, 1), (1, 0)])  8.71 us
    unnamed x31, local copies, waits for them, and re-layouts  6.95 us
    select_n x3, other arithmetic, per_device(): jnp.where(kept, mine, passed)  6.26 us
    pallas_call x1, Pallas kernels, expert_part(): pl.pallas_call(expert_kernel, out_shape=jax.ShapeDtypeStruct((count, widt...  5.28 us
    ppermute x1, starting transfers between devices, from_behind(): return lax.ppermute(block, axis, route)  4.92 us
  transfers between devices with their start and end apart: 11, of which 5 were waited for; matrix products, arithmetic and copies ran while one was open for 9% of the time, Pallas kernels for 2%

profile of v2, /device:TPU:1, one launch (start us, length us, event | category | flops | bytes accessed | tf_op | source)
XLA Modules:
  0.0 180.4 jit_solution(6767923482883502330)
XLA Ops:
  0.0 0.8 slice_bitcast_fusion.2
  0.8 4.9 %collective-permute-start = (bf16[2,128,64]{1,2,0:T(8,128)(2,1)S(1)}, bf16[2,128,64]{1,2,0:T(8,128)(2,1)S(1)}, u32[]{:S(2)}, u32[]{:S(2)}) collective-permute-start(bf16[2,128,64]{1,2,0:T(8,128)(2,1)S(1)} %pad_maximum_fusion.2), channel_id=1, source_target_pairs={{0,16},{16,32},{32,48},{48,64},{64,80},{80,96},{96,112},{112,128},... | collective-permute-start | bytes 98312 | tf_op jit(solution)/shard_map/ppermute | solution.py:26
  5.8 0.9 copy.18
  6.9 0.2 multiply_cosine_fusion.1
  7.3 0.8 slice.74
  8.1 1.5 collective-permute-done
  9.6 0.8 maximum_convert_fusion
  10.4 0.3 fusion.38
  10.7 0.7 pad_maximum_fusion.1
  11.5 0.3 fusion.48
  12.0 0.2 fusion.4
  12.4 1.4 convolution_convert_fusion
  13.8 5.4 %all-to-all-start = ((bf16[16,16,2048]{2,1,0:T(8,128)(2,1)}), bf16[16,16,2048]{2,1,0:T(8,128)(2,1)S(1)}, u32[]{:S(2)}, u32[]{:S(2)}) async-start(bf16[16,16,2048]{2,1,0:T(8,128)(2,1)} %bitcast.18), calls=%async_computation | async-start | bytes 2097152 | tf_op jit(solution)/shard_map/all_to_all | solution.py:30
  19.2 3.3 %collective-permute-start.1 = (bf16[2048,256]{1,0:T(8,128)(2,1)S(1)}, bf16[2048,256]{1,0:T(8,128)(2,1)}, u32[]{:S(2)}, u32[]{:S(2)}) collective-permute-start(bf16[2048,256]{1,0:T(8,128)(2,1)S(1)} %bitcast.98), channel_id=1, source_target_pairs={{0,16},{16,17},{17,1},{1,0},{2,18},{18,19},{19,3},{3,2},{4,20},{20... | collective-permute-start | bytes 3145736 | tf_op jit(solution)/shard_map/ppermute | solution.py:40
  22.5 2.2 %collective-permute-start.2 = (bf16[2048,256]{1,0:T(8,128)(2,1)}, bf16[2048,256]{1,0:T(8,128)(2,1)}, u32[]{:S(2)}, u32[]{:S(2)}) collective-permute-start(bf16[2048,256]{1,0:T(8,128)(2,1)} %bitcast.99), channel_id=1, source_target_pairs={{0,16},{16,17},{17,1},{1,0},{2,18},{18,19},{19,3},{3,2},{4,20},{20... | collective-permute-start | bytes 3145736 | tf_op jit(solution)/shard_map/ppermute | solution.py:40
  24.7 0.7 copy.25.ids_ref
  25.4 0.6 fusion.52.ids_row_ref
  26.1 1.5 shard_map.118
  27.6 10.2 %all-to-all-done = bf16[16,16,2048]{2,1,0:T(8,128)(2,1)S(1)} async-done(((bf16[16,16,2048]{2,1,0:T(8,128)(2,1)}), bf16[16,16,2048]{2,1,0:T(8,128)(2,1)S(1)}, u32[]{:S(2)}, u32[]{:S(2)}) %all-to-all-start) | async-done | bytes 1048608 | tf_op jit(solution)/shard_map/all_to_all | solution.py:30
  37.8 0.1 convert_reduce_fusion
  38.1 1.0 fusion.2
  39.1 0.8 copy.36
  39.9 16.5 %all-to-all-start.1 = ((bf16[64,16,128]{2,1,0:T(8,128)(2,1)}), bf16[64,16,128]{2,1,0:T(8,128)(2,1)S(1)}, u32[]{:S(2)}, u32[]{:S(2)}) async-start(bf16[64,16,128]{2,1,0:T(8,128)(2,1)} %bitcast.45), calls=%async_computation.1 | async-start | bytes 524288 | tf_op jit(solution)/shard_map/all_to_all | solution.py:30
  56.4 3.3 %collective-permute-start.3 = (bf16[256,2048]{1,0:T(8,128)(2,1)}, bf16[256,2048]{1,0:T(8,128)(2,1)}, u32[]{:S(2)}, u32[]{:S(2)}) collective-permute-start(bf16[256,2048]{1,0:T(8,128)(2,1)} %bitcast.100), channel_id=1, source_target_pairs={{0,16},{16,17},{17,1},{1,0},{2,18},{18,19},{19,3},{3,2},{4,20},{20... | collective-permute-start | bytes 3145736 | tf_op jit(solution)/shard_map/ppermute | solution.py:40
  59.6 1.3 collective-permute-start.4
  60.9 1.3 collective-permute-start.5
  62.2 15.5 %all-to-all-done.1 = bf16[64,16,128]{2,1,0:T(8,128)(2,1)S(1)} async-done(((bf16[64,16,128]{2,1,0:T(8,128)(2,1)}), bf16[64,16,128]{2,1,0:T(8,128)(2,1)S(1)}, u32[]{:S(2)}, u32[]{:S(2)}) %all-to-all-start.1) | async-done | bytes 262176 | tf_op jit(solution)/shard_map/all_to_all | solution.py:30
  77.9 1.6 broadcast_in_dim.15
  79.5 3.6 %all-to-all-start.2 = ((bf16[8,64,2048]{2,1,0:T(8,128)(2,1)}), bf16[8,64,2048]{2,1,0:T(8,128)(2,1)S(1)}, u32[]{:S(2)}, u32[]{:S(2)}) async-start(bf16[8,64,2048]{2,1,0:T(8,128)(2,1)} %broadcast_in_dim.15), calls=%async_computation.2 | async-start | bytes 4194304 | tf_op jit(solution)/shard_map/all_to_all | solution.py:30
  83.1 1.4 collective-permute-start.6
  84.5 2.7 %broadcast_select_fusion.2.refs_3_ = bf16[2048,256]{1,0:T(8,128)(2,1)} fusion(bf16[2048,256]{1,0:T(8,128)(2,1)} %collective-permute-done.4, pred[]{:T(512)S(6)} %eq.3, bf16[1,2048,256]{2,1,0:T(8,128)(2,1)} %param.21), kind=kLoop, calls=%fused_computation.12 | loop fusion | flops 524288 | bytes 3145729 | tf_op jit(solution)/shard_map/jit(_where)/select_n | solution.py:255
  87.2 2.5 %broadcast_select_fusion.1.refs_4_ = bf16[2048,256]{1,0:T(8,128)(2,1)} fusion(bf16[2048,256]{1,0:T(8,128)(2,1)} %collective-permute-done.5, pred[]{:T(512)S(6)} %eq.3, bf16[1,2048,256]{2,1,0:T(8,128)(2,1)S(1)} %copy-done.5), kind=kLoop, calls=%fused_computation.11 | loop fusion | flops 524288 | bytes 3145729 | tf_op jit(solution)/shard_map/jit(_where)/select_n | solution.py:255
  89.7 1.1 broadcast_select_fusion.refs_5_
  90.8 19.2 %all-to-all-done.2 = bf16[8,64,2048]{2,1,0:T(8,128)(2,1)S(1)} async-done(((bf16[8,64,2048]{2,1,0:T(8,128)(2,1)}), bf16[8,64,2048]{2,1,0:T(8,128)(2,1)S(1)}, u32[]{:S(2)}, u32[]{:S(2)}) %all-to-all-start.2) | async-done | bytes 2097184 | tf_op jit(solution)/shard_map/all_to_all | solution.py:30
  110.0 1.2 copy-done.1
  111.2 1.2 copy-done.2
  112.5 1.2 copy-done.3
  113.7 5.3 %shard_map.119 = bf16[512,2048]{1,0:T(8,128)(2,1)S(1)} custom-call(bf16[512,2048]{1,0:T(8,128)(2,1)S(1)} %bitcast.94, bf16[2048,256]{1,0:T(8,128)(2,1)} %collective-permute-done.1.refs_0_, bf16[2048,256]{1,0:T(8,128)(2,1)} %collective-permute-done.2.refs_1_, bf16[256,2048]{1,0:T(8,128)(2,1)} %collective-permute-done.3.refs_2_, ...), custom_call_target="tpu_custom_call" | custom-call | flops 3221225472 | bytes 10485760 | tf_op jit(solution)/shard_map/pallas_call | solution.py:173
  119.0 31.6 %all_to_all.25 = bf16[8,64,2048]{2,1,0:T(8,128)(2,1)S(1)} all-to-all(bf16[8,64,2048]{2,1,0:T(8,128)(2,1)S(1)} %bitcast.95), channel_id=1, replica_groups=mesh['zg'=4,'zl'=4,'core'=2,'y'=4,'xh'=2,'xl'=2] {'y','xh'}, dimensions={0} | all-to-all | bytes 4194304 | tf_op jit(solution)/shard_map/all_to_all | solution.py:30
  150.6 0.4 reduce_sum.42
  150.9 0.8 copy.38
  151.7 6.4 %all-to-all-start.4 = ((bf16[64,16,128]{2,1,0:T(8,128)(2,1)}), bf16[64,16,128]{2,1,0:T(8,128)(2,1)S(1)}, u32[]{:S(2)}, u32[]{:S(2)}) async-start(bf16[64,16,128]{2,1,0:T(8,128)(2,1)} %bitcast.49), calls=%async_computation.4 | async-start | bytes 524288 | tf_op jit(solution)/shard_map/all_to_all | solution.py:30
  158.1 0.7 copy.30.in_ref
  158.8 1.3 shard_map.120
  160.1 1.0 slice_reduce_fusion.1
  161.1 18.4 %all-to-all-done.4 = bf16[64,16,128]{2,1,0:T(8,128)(2,1)S(1)} async-done(((bf16[64,16,128]{2,1,0:T(8,128)(2,1)}), bf16[64,16,128]{2,1,0:T(8,128)(2,1)S(1)}, u32[]{:S(2)}, u32[]{:S(2)}) %all-to-all-start.4) | async-done | bytes 262176 | tf_op jit(solution)/shard_map/all_to_all | solution.py:30
  179.5 0.2 fusion.9
  179.7 0.7 fusion.16
  (56 shorter events, 1.1 us)
Async XLA Ops:
  0.0 12.3 %copy-start = (bf16[128,2048]{1,0:T(8,128)(2,1)S(1)}, bf16[128,2048]{1,0:T(8,128)(2,1)}, u32[]{:S(2)}) copy-start(bf16[128,2048]{1,0:T(8,128)(2,1)} %param.17) | copy-start | bytes 1572868
  0.0 11.8 %copy-start.11 = (f32[2]{0:T(128)S(1)}, f32[2]{0:T(128)}, u32[]{:S(2)}) copy-start(f32[2]{0:T(128)} %param.15) | copy-start | bytes 28
  0.8 8.8 %collective-permute-start = (bf16[2,128,64]{1,2,0:T(8,128)(2,1)S(1)}, bf16[2,128,64]{1,2,0:T(8,128)(2,1)S(1)}, u32[]{:S(2)}, u32[]{:S(2)}) collective-permute-start(bf16[2,128,64]{1,2,0:T(8,128)(2,1)S(1)} %pad_maximum_fusion.2), channel_id=1, source_target_pairs={{0,16},{16,32},{32,48},{48,64},{64,80},{80,96},{96,112},{112,128},... | collective-permute-start | bytes 98312 | tf_op jit(solution)/shard_map/ppermute | solution.py:26
  12.2 6.9 %copy-start.4 = (bf16[1,2048,256]{2,1,0:T(8,128)(2,1)S(1)}, bf16[1,2048,256]{2,1,0:T(8,128)(2,1)}, u32[]{:S(2)}) copy-start(bf16[1,2048,256]{2,1,0:T(8,128)(2,1)} %param.21) | copy-start | bytes 3145732
  12.2 12.4 %copy-start.10 = (s32[256,2]{0,1:T(2,128)S(1)}, s32[256,2]{0,1:T(2,128)}, u32[]{:S(2)}) copy-start(s32[256,2]{0,1:T(2,128)} %param.19) | copy-start | bytes 6148
  12.3 25.6 %copy-start.7 = (bf16[16,2048]{1,0:T(8,128)(2,1)S(1)}, bf16[16,2048]{1,0:T(8,128)(2,1)}, u32[]{:S(2)}) copy-start(bf16[16,2048]{1,0:T(8,128)(2,1)} %param.16) | copy-start | bytes 196612
  13.8 24.3 %copy-start.9 = (f32[2048]{0:T(1024)S(1)}, f32[2048]{0:T(1024)}, u32[]{:S(2)}) copy-start(f32[2048]{0:T(1024)} %param.18) | copy-start | bytes 24580
  13.8 24.0 %all-to-all-start = ((bf16[16,16,2048]{2,1,0:T(8,128)(2,1)}), bf16[16,16,2048]{2,1,0:T(8,128)(2,1)S(1)}, u32[]{:S(2)}, u32[]{:S(2)}) async-start(bf16[16,16,2048]{2,1,0:T(8,128)(2,1)} %bitcast.18), calls=%async_computation | async-start | bytes 2097152 | tf_op jit(solution)/shard_map/all_to_all | solution.py:30
  19.2 40.4 %collective-permute-start.1 = (bf16[2048,256]{1,0:T(8,128)(2,1)S(1)}, bf16[2048,256]{1,0:T(8,128)(2,1)}, u32[]{:S(2)}, u32[]{:S(2)}) collective-permute-start(bf16[2048,256]{1,0:T(8,128)(2,1)S(1)} %bitcast.98), channel_id=1, source_target_pairs={{0,16},{16,17},{17,1},{1,0},{2,18},{18,19},{19,3},{3,2},{4,20},{20... | collective-permute-start | bytes 3145736 | tf_op jit(solution)/shard_map/ppermute | solution.py:40
  22.5 38.5 %collective-permute-start.2 = (bf16[2048,256]{1,0:T(8,128)(2,1)}, bf16[2048,256]{1,0:T(8,128)(2,1)}, u32[]{:S(2)}, u32[]{:S(2)}) collective-permute-start(bf16[2048,256]{1,0:T(8,128)(2,1)} %bitcast.99), channel_id=1, source_target_pairs={{0,16},{16,17},{17,1},{1,0},{2,18},{18,19},{19,3},{3,2},{4,20},{20... | collective-permute-start | bytes 3145736 | tf_op jit(solution)/shard_map/ppermute | solution.py:40
  39.9 37.9 %all-to-all-start.1 = ((bf16[64,16,128]{2,1,0:T(8,128)(2,1)}), bf16[64,16,128]{2,1,0:T(8,128)(2,1)S(1)}, u32[]{:S(2)}, u32[]{:S(2)}) async-start(bf16[64,16,128]{2,1,0:T(8,128)(2,1)} %bitcast.45), calls=%async_computation.1 | async-start | bytes 524288 | tf_op jit(solution)/shard_map/all_to_all | solution.py:30
  56.4 26.7 %collective-permute-start.3 = (bf16[256,2048]{1,0:T(8,128)(2,1)}, bf16[256,2048]{1,0:T(8,128)(2,1)}, u32[]{:S(2)}, u32[]{:S(2)}) collective-permute-start(bf16[256,2048]{1,0:T(8,128)(2,1)} %bitcast.100), channel_id=1, source_target_pairs={{0,16},{16,17},{17,1},{1,0},{2,18},{18,19},{19,3},{3,2},{4,20},{20... | collective-permute-start | bytes 3145736 | tf_op jit(solution)/shard_map/ppermute | solution.py:40
  59.6 24.9 %collective-permute-start.4 = (bf16[2048,256]{1,0:T(8,128)(2,1)}, bf16[2048,256]{1,0:T(8,128)(2,1)}, u32[]{:S(2)}, u32[]{:S(2)}) collective-permute-start(bf16[2048,256]{1,0:T(8,128)(2,1)} %collective-permute-done.1.refs_0_), channel_id=1, source_target_pairs={{0,16},{17,1},{2,18},{19,3},{4,20},{21,5},{6,22},{23,7},{8,24},{25... | collective-permute-start | bytes 3145736 | tf_op jit(solution)/shard_map/ppermute | solution.py:44
  60.9 26.3 %collective-permute-start.5 = (bf16[2048,256]{1,0:T(8,128)(2,1)}, bf16[2048,256]{1,0:T(8,128)(2,1)}, u32[]{:S(2)}, u32[]{:S(2)}) collective-permute-start(bf16[2048,256]{1,0:T(8,128)(2,1)} %collective-permute-done.2.refs_1_), channel_id=1, source_target_pairs={{0,16},{17,1},{2,18},{19,3},{4,20},{21,5},{6,22},{23,7},{8,24},{25... | collective-permute-start | bytes 3145736 | tf_op jit(solution)/shard_map/ppermute | solution.py:44
  79.5 30.5 %all-to-all-start.2 = ((bf16[8,64,2048]{2,1,0:T(8,128)(2,1)}), bf16[8,64,2048]{2,1,0:T(8,128)(2,1)S(1)}, u32[]{:S(2)}, u32[]{:S(2)}) async-start(bf16[8,64,2048]{2,1,0:T(8,128)(2,1)} %broadcast_in_dim.15), calls=%async_computation.2 | async-start | bytes 4194304 | tf_op jit(solution)/shard_map/all_to_all | solution.py:30
  83.1 4.1 %copy-start.5 = (bf16[1,2048,256]{2,1,0:T(8,128)(2,1)S(1)}, bf16[1,2048,256]{2,1,0:T(8,128)(2,1)}, u32[]{:S(2)}) copy-start(bf16[1,2048,256]{2,1,0:T(8,128)(2,1)} %param.22) | copy-start | bytes 3145732
  83.1 6.6 %collective-permute-start.6 = (bf16[256,2048]{1,0:T(8,128)(2,1)}, bf16[256,2048]{1,0:T(8,128)(2,1)S(1)}, u32[]{:S(2)}, u32[]{:S(2)}) collective-permute-start(bf16[256,2048]{1,0:T(8,128)(2,1)} %collective-permute-done.3.refs_2_), channel_id=1, source_target_pairs={{0,16},{17,1},{2,18},{19,3},{4,20},{21,5},{6,22},{23,7},{8,24},{25... | collective-permute-start | bytes 3145736 | tf_op jit(solution)/shard_map/ppermute | solution.py:44
  87.2 2.5 %copy-start.6 = (bf16[1,256,2048]{2,1,0:T(8,128)(2,1)S(1)}, bf16[1,256,2048]{2,1,0:T(8,128)(2,1)}, u32[]{:S(2)}) copy-start(bf16[1,256,2048]{2,1,0:T(8,128)(2,1)} %param.23) | copy-start | bytes 3145732
  110.0 1.2 copy-start.1
  111.2 1.2 copy-start.2
  112.5 1.2 copy-start.3
  150.6 7.5 %copy-start.12 = (f32[256,2]{0,1:T(2,128)S(1)}, f32[256,2]{0,1:T(2,128)}, u32[]{:S(2)}) copy-start(f32[256,2]{0,1:T(2,128)} %param.20) | copy-start | bytes 6148
  150.6 28.9 %copy-start.8 = (bf16[32,64]{1,0:T(8,128)(2,1)S(1)}, bf16[32,64]{1,0:T(8,128)(2,1)}, u32[]{:S(2)}) copy-start(bf16[32,64]{1,0:T(8,128)(2,1)} %get-tuple-element.7) | copy-start | bytes 12292
  151.7 27.8 %all-to-all-start.4 = ((bf16[64,16,128]{2,1,0:T(8,128)(2,1)}), bf16[64,16,128]{2,1,0:T(8,128)(2,1)S(1)}, u32[]{:S(2)}, u32[]{:S(2)}) async-start(bf16[64,16,128]{2,1,0:T(8,128)(2,1)} %bitcast.49), calls=%async_computation.4 | async-start | bytes 524288 | tf_op jit(solution)/shard_map/all_to_all | solution.py:30

commit v3 on v2

v3 whole, which is shorter than its diff:
```python
import jax
import jax.numpy as jnp
from jax import lax
from jax.experimental import pallas as pl
from jax.experimental.pallas import tpu as pltpu
from jax.sharding import PartitionSpec as P


HEAD = 64
WINDOW = 128


norm_epsilon = 1e-06


SP = ("zg", "zl", "core")
TP = ("y", "xh", "xl")
SIZES = (4, 4, 2, 4, 2, 2)
ROUTE = ("zg", "zl")


def from_behind(block, axis, distance):
    devices = range(lax.axis_size(axis))
    route = [(i - distance, i) for i in devices if i - distance in devices]
    return lax.ppermute(block, axis, route)


def exchange(blocks, axis):
    return lax.all_to_all(blocks, axis, 0, 0, tiled=True)


def turn(pack, side):
    columns = 4
    route = []
    for x in range(columns):
        here = x % 2
        beside = (x + side * (1 - 2 * here)) % columns
        route += [
            (here * columns + x, (1 - here) * columns + x),
            ((1 - here) * columns + x, (1 - here) * columns + beside),
        ]
    return lax.ppermute(pack, ("core", "xh", "xl"), route)


def pass_on(pack):
    return lax.ppermute(pack, ("core", "xl"), [(0, 2), (3, 1)])


IN_VMEM = pl.BlockSpec(memory_space=pltpu.VMEM)
IN_SMEM = pl.BlockSpec(memory_space=pltpu.SMEM)
IN_HBM = pl.BlockSpec(memory_space=pltpu.HBM)

LINES = 8
SLOTS = 4
PLANES = 16
PAIR = 2
RANKS = 2
DEPTH = 4


def near(array):
    return pltpu.with_memory_space_constraint(array, pltpu.VMEM)


def iota(shape, dim):
    return lax.broadcasted_iota(jnp.int32, shape, dim)


def one_hot(mask):
    return jnp.where(mask, 1.0, 0.0).astype(jnp.bfloat16)


def dot(left, right):
    return jnp.dot(left, right, preferred_element_type=jnp.float32)


def room(mib):
    return pltpu.CompilerParams(vmem_limit_bytes=mib * 2**20)


def price(flops, nbytes):
    return pl.CostEstimate(flops=flops, bytes_accessed=nbytes, transcendentals=0)


def turned(array, cosine, sine):
    half = HEAD // 2
    front, back = array[:half], array[half:]
    return jnp.concatenate(
        [front * cosine - back * sine, back * cosine + front * sine], 0
    ).astype(jnp.bfloat16)


def over_rows(left, right):
    return lax.dot_general(left, right, (((0,), (0,)), ((), ())), preferred_element_type=jnp.float32)


def attend_kernel(
    edge_ref, sink_ref, query_ref, key_ref, value_ref, rim_ref, *refs
):
    count = query_ref.shape[0]
    cosine_ref, sine_ref, weight_ref, out_ref = refs
    cosine, sine = cosine_ref[...], sine_ref[...]
    keys = jnp.concatenate([rim_ref[:HEAD], key_ref[...]], 1).astype(jnp.float32)
    keys = turned(keys, cosine, sine)
    values = jnp.concatenate([rim_ref[HEAD:], value_ref[...]], 1)
    queries = query_ref[...].astype(jnp.float32).T
    cosine, sine = cosine[:, WINDOW:], sine[:, WINDOW:]
    queries = [turned(queries[at : at + HEAD], cosine, sine) for at in (0, HEAD)]
    shape = (2 * WINDOW, 2 * WINDOW)
    key_at = lax.broadcasted_iota(jnp.int32, shape, 0)
    query_at = lax.broadcasted_iota(jnp.int32, shape, 1) & (WINDOW - 1)
    seen = (key_at > query_at) & (key_at <= query_at + WINDOW)
    first_head = lax.broadcasted_iota(jnp.int32, (1, 2 * WINDOW), 1) < WINDOW
    sink = jnp.where(first_head, sink_ref[0], sink_ref[1])
    for at in range(0, count, WINDOW):
        here = jnp.concatenate([q[:, at : at + WINDOW] for q in queries], 1)
        scores = over_rows(keys[:, at : at + 2 * WINDOW], here) * HEAD ** (-0.5)
        allowed = seen
        if at == 0:
            allowed = allowed & (key_at >= edge_ref[0])
        scores = jnp.where(allowed, scores, -jnp.inf)
        highest = jnp.maximum(jnp.max(scores, 0, keepdims=True), sink)
        raised = jnp.exp(scores - highest)
        denominator = jnp.sum(raised, 0, keepdims=True) + jnp.exp(sink - highest)
        weighted = jnp.dot(
            values[:, at : at + 2 * WINDOW],
            raised.astype(jnp.bfloat16),
            preferred_element_type=jnp.float32,
        )
        attended = (weighted / denominator).astype(jnp.bfloat16)
        attended = jnp.concatenate([attended[:, :WINDOW], attended[:, WINDOW:]], 0)
        out_ref[at : at + WINDOW] = over_rows(attended, weight_ref[...]).astype(jnp.bfloat16)


def attention_share(edge, sinks, queries, keys_t, values_t, rim, angles, weight):
    count, width = queries.shape[0], weight.shape[1]
    return pl.pallas_call(
        attend_kernel,
        out_shape=jax.ShapeDtypeStruct((count, width), jnp.bfloat16),
        in_specs=[IN_SMEM] * 2 + [IN_VMEM] * 7,
        out_specs=IN_VMEM,
        cost_estimate=pl.CostEstimate(
            flops=2 * count * 128 * (width + 1024),
            bytes_accessed=2 * (count + 128) * width,
            transcendentals=2 * count * 256,
        ),
    )(edge, sinks, queries, keys_t, values_t, *map(near, (rim, *angles)), weight)


def plan_kernel(ids_ref, ids_row_ref, spread_ref, collect_ref):
    rows, picks = ids_ref.shape
    lines = collect_ref.shape[2]
    below, right = iota((rows, rows), 0), iota((rows, rows), 1)
    spread = [jnp.zeros((lines, rows), jnp.float32)] * 2
    for k in range(picks):
        col, row = ids_ref[:, k : k + 1], ids_row_ref[k : k + 1, :]
        rank_col = jnp.zeros((rows, 1), jnp.int32)
        rank_row = jnp.zeros((1, rows), jnp.int32)
        for j in range(picks):
            other_col, other_row = ids_ref[:, j : j + 1], ids_row_ref[j : j + 1, :]
            before = jnp.where((col == other_row) & (right < below), 1, 0)
            rank_col = rank_col + jnp.sum(before, 1, keepdims=True)
            before = jnp.where((other_col == row) & (below < right), 1, 0)
            rank_row = rank_row + jnp.sum(before, 0, keepdims=True)
        for half in range(2):
            line_col = (col >> 1) * LINES + half * SLOTS + (col & 1) * RANKS + rank_col
            line_row = (row >> 1) * LINES + half * SLOTS + (row & 1) * RANKS + rank_row
            collect_ref[half, k * rows : (k + 1) * rows, :] = one_hot(
                iota((rows, lines), 1) == line_col
            )
            spread[half] = spread[half] + jnp.where(
                iota((lines, rows), 0) == line_row, 1.0, 0.0
            )
    for half in range(2):
        spread_ref[half] = spread[half].astype(jnp.bfloat16)


def plan(ids):
    rows, picks = ids.shape
    lines = PLANES * LINES
    return pl.pallas_call(
        plan_kernel,
        out_shape=(
            jax.ShapeDtypeStruct((2, lines, rows), jnp.bfloat16),
            jax.ShapeDtypeStruct((2, picks * rows, lines), jnp.bfloat16),
        ),
        in_specs=[IN_VMEM] * 2,
        out_specs=[IN_VMEM] * 2,
        compiler_params=room(16),
        cost_estimate=price(10**6, 2**14),
    )(ids, ids.T)


def pack_kernel(gate_ref, up_ref, down_ref, *refs):
    *out_refs, sems = refs
    copies = []
    for half, out_ref in enumerate(out_refs):
        lanes = pl.ds(half * 128, 128)
        pieces = [
            (gate_ref.at[:, :, lanes], out_ref.at[0]),
            (up_ref.at[:, :, lanes], out_ref.at[1]),
        ]
        for j in range(out_ref.shape[1]):
            pieces.append((down_ref.at[lanes, pl.ds(j * 128, 128)], out_ref.at[2, j]))
        for k, (source, target) in enumerate(pieces):
            copies.append(pltpu.make_async_copy(source, target, sems.at[half, k]))
    for copy in copies:
        copy.start()
    for copy in copies:
        copy.wait()


def pack(gate, up, down):
    units, width = down.shape
    blocks = width // 128
    shape = jax.ShapeDtypeStruct((3, blocks, 128, units // 2), jnp.bfloat16)
    return pl.pallas_call(
        pack_kernel,
        out_shape=(shape, shape),
        in_specs=[IN_HBM] * 3,
        out_specs=[IN_VMEM] * 2,
        scratch_shapes=[pltpu.SemaphoreType.DMA((2, 2 + blocks))],
        compiler_params=room(16),
        cost_estimate=price(10**6, 12 * units * width),
    )(gate.reshape(blocks, 128, units), up.reshape(blocks, 128, units), down)


def hold_kernel(in_ref, out_ref):
    out_ref[...] = in_ref[...]


def hold(array):
    return pl.pallas_call(
        hold_kernel,
        out_shape=jax.ShapeDtypeStruct(array.shape, array.dtype),
        in_specs=[IN_VMEM],
        out_specs=IN_VMEM,
        compiler_params=room(4),
        cost_estimate=price(10**6, 2**13),
    )(array)


def settle_kernel(shares_ref, residual_ref, gain_ref, spread_ref, middle_ref, out_ref):
    projected = jnp.sum(shares_ref[...].astype(jnp.float32), 0)
    middle = (residual_ref[...].astype(jnp.float32) + projected).astype(jnp.bfloat16)
    middle_ref[...] = middle
    middle = middle.astype(jnp.float32)
    square = jnp.mean(middle * middle, -1, keepdims=True)
    normed = (middle * lax.rsqrt(square + norm_epsilon) * gain_ref[...]).astype(jnp.bfloat16)
    half = normed.shape[1] // 2
    lines = dot(spread_ref[0], normed[:, :half]) + dot(spread_ref[1], normed[:, half:])
    out_ref[...] = lines.astype(jnp.bfloat16)


def settle(shares, residual, gain, spread):
    rows, width = residual.shape
    lines = spread.shape[1]
    return pl.pallas_call(
        settle_kernel,
        out_shape=(
            jax.ShapeDtypeStruct((rows, width), jnp.bfloat16),
            jax.ShapeDtypeStruct((lines, width // 2), jnp.bfloat16),
        ),
        in_specs=[IN_VMEM] * 4,
        out_specs=[IN_VMEM] * 2,
        compiler_params=room(16),
        cost_estimate=price(2 * lines * rows * width, 2 * shares.size),
    )(near(shares), residual, gain, near(spread))


def lines_of(half):
    shape = (PAIR * PLANES * RANKS, PLANES * LINES)
    row = iota(shape, 0)
    per_expert = PLANES * RANKS
    plane, slot = (row % per_expert) // RANKS, row // per_expert * RANKS + row % RANKS
    return iota(shape, 1) == plane * LINES + half * SLOTS + slot


def fan_kernel(lines_ref, out_ref):
    half = lines_ref.shape[1]
    for h in range(2):
        rows = dot(one_hot(lines_of(h)), lines_ref[...]).astype(jnp.bfloat16)
        for to in range(out_ref.shape[0]):
            out_ref[to, :, h * half : (h + 1) * half] = rows


def fan(lines, team):
    rows, width = PAIR * PLANES * RANKS, 2 * lines.shape[1]
    return pl.pallas_call(
        fan_kernel,
        out_shape=pltpu.VMEM((team, rows, width), jnp.bfloat16),
        in_specs=[IN_VMEM],
        out_specs=IN_VMEM,
        compiler_params=room(16),
        cost_estimate=price(2 * rows * lines.size * 2, 2 * team * rows * width),
    )(near(lines))


def fold_kernel(parts_ref, out_ref):
    half = out_ref.shape[1]
    rows = jnp.sum(parts_ref[...].astype(jnp.float32), 0).astype(jnp.bfloat16)
    lines = 0.0
    for h in range(2):
        take = one_hot(lines_of(h))
        lines = lines + lax.dot_general(
            take,
            rows[:, h * half : (h + 1) * half],
            (((0,), (0,)), ((), ())),
            preferred_element_type=jnp.float32,
        )
    out_ref[...] = lines.astype(jnp.bfloat16)


def fold(parts):
    width = parts.shape[2]
    lines = PLANES * LINES
    return pl.pallas_call(
        fold_kernel,
        out_shape=jax.ShapeDtypeStruct((lines, width // 2), jnp.bfloat16),
        in_specs=[IN_VMEM],
        out_specs=IN_VMEM,
        compiler_params=room(24),
        cost_estimate=price(2 * lines * parts.shape[1] * width, 2 * parts.size),
    )(near(parts))


def finish_kernel(lines_ref, collect_ref, share_ref, middle_ref, out_ref):
    rows = middle_ref.shape[0]
    half = lines_ref.shape[1]
    for h in range(2):
        at = slice(h * half, (h + 1) * half)
        picked = dot(collect_ref[h], lines_ref[...])
        routed = picked[:rows] * share_ref[:, :1] + picked[rows:] * share_ref[:, 1:]
        out_ref[:, at] = (middle_ref[:, at].astype(jnp.float32) + routed).astype(jnp.bfloat16)


def finish(lines, collect, shares, middle):
    return pl.pallas_call(
        finish_kernel,
        out_shape=jax.ShapeDtypeStruct(middle.shape, middle.dtype),
        in_specs=[IN_VMEM] * 4,
        out_specs=IN_VMEM,
        compiler_params=room(16),
        cost_estimate=price(4 * collect.size * lines.shape[1], 4 * lines.size),
    )(*map(near, (lines, collect)), shares, near(middle))


def expert_kernel(kept_ref, rows_ref, *refs):
    own, turned, passed = refs[0:2], refs[2:4], refs[4:6]
    out_ref, *slots, sems = refs[6:]
    gates, ups, downs = slots
    kept = kept_ref[0] == 1
    halves = range(len(own))

    def copy(source, slot, kind, half):
        units = pl.ds(half * 128, 128)
        place = (slot, slice(None), units) if kind == 2 else (slot, slice(None), slice(None), units)
        target = slots[kind].at[place]
        return pltpu.make_async_copy(source[half].at[kind], target, sems.at[slot, kind, half])

    def fetch(slot, kind):
        if slot == 0:
            for half in halves:
                copy(turned, slot, kind, half).start()
            return

        @pl.when(kept)
        def _():
            for half in halves:
                copy(own, slot, kind, half).start()

        @pl.when(jnp.logical_not(kept))
        def _():
            for half in halves:
                copy(passed, slot, kind, half).start()

    order = [(0, 0), (0, 1), (1, 0), (1, 1), (0, 2), (1, 2)]

    def ready(at):
        for half in halves:
            copy(turned, *order[at], half).wait()
        if at + DEPTH < len(order):
            fetch(*order[at + DEPTH])

    for at in range(DEPTH):
        fetch(*order[at])
    rows = rows_ref[...]
    hidden = []
    for slot in range(2):
        ready(2 * slot)
        gate_val = dot(rows, gates[slot].reshape(rows.shape[1], -1))
        ready(2 * slot + 1)
        up_val = dot(rows, ups[slot].reshape(rows.shape[1], -1))
        hidden.append((gate_val / (1.0 + jnp.exp(-gate_val)) * up_val).astype(jnp.bfloat16))
    ready(4)
    ready(5)
    chunk = 512
    for at in range(0, out_ref.shape[1], chunk):
        total = 0.0
        for slot in range(2):
            blocks = [downs[slot, j] for j in range(at // 128, (at + chunk) // 128)]
            total = total + dot(hidden[slot], jnp.concatenate(blocks, 1))
        out_ref[:, at : at + chunk] = total.astype(jnp.bfloat16)


def expert_part(kept, rows, own, turned, passed):
    count, width = rows.shape
    _, blocks, lanes, half = own[0].shape
    return pl.pallas_call(
        expert_kernel,
        out_shape=pltpu.VMEM((count, width), jnp.bfloat16),
        in_specs=[IN_SMEM, IN_VMEM] + [IN_HBM] * 6,
        out_specs=IN_VMEM,
        scratch_shapes=[
            pltpu.VMEM((2, blocks, lanes, 2 * half), jnp.bfloat16),
            pltpu.VMEM((2, blocks, lanes, 2 * half), jnp.bfloat16),
            pltpu.VMEM((2, blocks, 2 * half, lanes), jnp.bfloat16),
            pltpu.SemaphoreType.DMA((2, 3, 2)),
        ],
        compiler_params=room(32),
        cost_estimate=pl.CostEstimate(
            flops=24 * count * half * width,
            bytes_accessed=4 * count * width + 24 * half * width,
            transcendentals=4 * count * half,
        ),
    )(kept, near(rows), *own, *turned, *passed)


def per_device(
    queries,
    key_rows,
    values,
    sink_logits,
    residual,
    out_weight,
    norm_gain,
    expert_ids,
    route_weight,
    gate_proj,
    up_proj,
    down_proj,
):
    local_len = queries.shape[0]
    span = lax.axis_index(SP)
    keys_t, values_t = key_rows.T, values.T
    rim = jnp.concatenate([keys_t[:, -WINDOW:], values_t[:, -WINDOW:]], 0)
    rim = from_behind(rim, SP, 1)
    half = HEAD // 2
    frequency = 10000.0 ** (-jnp.arange(half, dtype=jnp.float32) * 2.0 / HEAD)
    positions = span * local_len - WINDOW + jnp.arange(local_len + WINDOW, dtype=jnp.int32)
    angles = positions.astype(jnp.float32)[None, :] * frequency[:, None]
    angles = (jnp.cos(angles), jnp.sin(angles))
    edge = jnp.where(span == 0, WINDOW, 0).astype(jnp.int32).reshape(1)
    shares = attention_share(edge, sink_logits, queries, keys_t, values_t, rim, angles, out_weight)
    tok_rows, width = residual.shape
    first = lax.axis_index(TP) * tok_rows
    own_ids = lax.dynamic_slice_in_dim(expert_ids, first, tok_rows, 0)
    own_weights = lax.dynamic_slice_in_dim(route_weight, first, tok_rows, 0)
    shares = exchange(shares.reshape(lax.axis_size(TP), -1, width), TP)
    own = pack(gate_proj[0], up_proj[0], down_proj[0])
    right = turn(own[0], 1)
    left = turn(own[1], -1)
    spread, collect = plan(own_ids)
    middle, lines = settle(shares, residual, norm_gain.reshape(1, -1), spread)
    lines = exchange(lines.reshape(PLANES, LINES, width // 2), ROUTE)
    team = lax.axis_size(TP) // PAIR
    fanned = fan(lines.reshape(PLANES * LINES, width // 2), team)
    gathered = exchange(fanned.reshape(team * PAIR, -1, width), TP)
    right_too = pass_on(right)
    left_too = pass_on(left)
    kept = (lax.axis_index("core") == lax.axis_index("xl")).astype(jnp.int32).reshape(1)
    own_weights = hold(own_weights)
    parts = expert_part(
        kept, gathered.reshape(-1, width), own, (right, left), (right_too, left_too)
    )
    parts = exchange(parts.reshape(team * PAIR, -1, width), TP)
    lines = fold(parts.reshape(team, -1, width))
    lines = exchange(lines.reshape(PLANES, LINES, width // 2), ROUTE)
    return finish(lines.reshape(PLANES * LINES, width // 2), collect, own_weights, middle)


def solution(mesh):
    fine = jax.sharding.Mesh(mesh.devices.reshape(SIZES), SP + TP)
    return jax.shard_map(
        per_device,
        mesh=fine,
        in_specs=(
            P(SP, TP),
            P(SP, TP),
            P(SP, TP),
            P(TP),
            P(SP + TP, None),
            P(TP, None),
            P(),
            P(SP, None),
            P(SP, None),
            P(SP, None, TP),
            P(SP, None, TP),
            P(SP, TP, None),
        ),
        out_specs=P(SP + TP, None),
        check_vma=False,
    )
```

time: 182 us -> 170 us (0.934)
  the two profiles are of different devices: /device:TPU:1 before, /device:TPU:32 now
where the time goes in v3:
time: 170 us
  blocking collectives  62.6 us (37%)
  waiting for transfers between devices  52.2 us (31%)
  starting transfers between devices  33 us (19%)
  Pallas kernels  18.4 us (11%)
  local copies, waits for them, and re-layouts  3.09 us (2%)
    all_to_all x2, blocking collectives, exchange(): return lax.all_to_all(blocks, axis, 0, 0, tiled=True)  62.6 us
    all_to_all x3, waiting for transfers between devices, exchange(): return lax.all_to_all(blocks, axis, 0, 0, tiled=True)  47 us
    all_to_all x3, starting transfers between devices, exchange(): return lax.all_to_all(blocks, axis, 0, 0, tiled=True)  21.6 us
    pallas_call x1, Pallas kernels, expert_part(): pl.pallas_call(expert_kernel, out_shape=pltpu.VMEM((count, width), jnp.bf...  7.5 us
    ppermute x2, starting transfers between devices, pass_on(): return lax.ppermute(pack, ('core', 'xl'), [(0, 2), (3, 1)])  4.95 us
    ppermute x2, starting transfers between devices, turn(): return lax.ppermute(pack, ('core', 'xh', 'xl'), route)  4.64 us
    pallas_call x1, Pallas kernels, attention_share(): pl.pallas_call(attend_kernel, out_shape=jax.ShapeDtypeStruct((count, widt...  3.68 us
  transfers between devices with their start and end apart: 8, of which 5 were waited for; matrix products, arithmetic and copies ran while one was open for 0% of the time, Pallas kernels for 3%

profile of v3, /device:TPU:32, one launch (start us, length us, event | category | flops | bytes accessed | tf_op | source)
XLA Modules:
  0.0 169.7 jit_solution(435046040401770149)
XLA Ops:
  0.0 0.0 copy-start
  0.0 0.7 slice.8
  0.7 0.7 slice.9
  1.5 1.9 %collective-permute-start = (bf16[128,128]{1,0:T(8,128)(2,1)S(1)}, bf16[128,128]{1,0:T(8,128)(2,1)S(1)}, u32[]{:S(2)}, u32[]{:S(2)}) collective-permute-start(bf16[128,128]{1,0:T(8,128)(2,1)S(1)} %pad_maximum_fusion), channel_id=1, source_target_pairs={{0,16},{16,32},{32,48},{48,64},{64,80},{80,96},{96,112},{112,128},... | collective-permute-start | bytes 98312 | tf_op jit(solution)/shard_map/ppermute | solution.py:25
  3.4 0.3 multiply_sine_fusion
  3.7 3.0 %collective-permute-done.rim_ref = bf16[128,128]{1,0:T(8,128)(2,1)S(1)} collective-permute-done((bf16[128,128]{1,0:T(8,128)(2,1)S(1)}, bf16[128,128]{1,0:T(8,128)(2,1)S(1)}, u32[]{:S(2)}, u32[]{:S(2)}) %collective-permute-start) | collective-permute-done | bytes 32800 | tf_op jit(solution)/shard_map/ppermute | solution.py:25
  6.7 0.0 copy-start.1
  6.7 0.0 copy-start.2
  6.7 3.7 %shard_map.118 = bf16[256,2048]{1,0:T(8,128)(2,1)} custom-call(s32[1]{0:T(128)} %bitcast.1.edge_ref, f32[2]{0:T(128)} %sink_ref.1, bf16[256,128]{1,0:T(8,128)(2,1)} %query_ref.1, bf16[64,256]{1,0:T(8,128)(2,1)} %bitcast.31, bf16[64,256]{1,0:T(8,128)(2,1)} %bitcast.33, bf16[128,128]{1,0:T(8,128)(2,1)S(1)} %collective-permute-done.rim_ref, ...), custom_call_target="tpu_custom_call" | custom-call | flops 201326592 | bytes 1572864 | tf_op jit(solution)/shard_map/pallas_call | solution.py:137
  10.4 7.0 %all-to-all-start = ((bf16[16,16,2048]{2,1,0:T(8,128)(2,1)}), bf16[16,16,2048]{2,1,0:T(8,128)(2,1)S(1)}, u32[]{:S(2)}, u32[]{:S(2)}) async-start(bf16[16,16,2048]{2,1,0:T(8,128)(2,1)} %bitcast.29), calls=%async_computation | async-start | bytes 2097152 | tf_op jit(solution)/shard_map/all_to_all | solution.py:29
  17.4 0.0 copy-done.1
  17.4 0.0 copy-done.2
  17.4 0.0 copy-start.3
  17.4 1.2 copy-done.3
  18.6 0.0 copy-start.4
  18.6 0.0 copy-start.5
  18.6 2.7 %shard_map.122 = (bf16[3,16,128,128]{3,2,1,0:T(8,128)(2,1)}, bf16[3,16,128,128]{3,2,1,0:T(8,128)(2,1)}) custom-call(bf16[16,128,256]{2,1,0:T(8,128)(2,1)S(1)} %bitcast.22, bf16[16,128,256]{2,1,0:T(8,128)(2,1)S(1)} %bitcast.23, bf16[256,2048]{1,0:T(8,128)(2,1)S(1)} %bitcast.24), custom_call_target="tpu_custom_call" | custom-call | flops 1000000 | bytes 6291456 | tf_op jit(solution)/shard_map/pallas_call | solution.py:217
  21.4 1.9 %collective-permute-start.1 = (bf16[3,16,128,128]{3,2,1,0:T(8,128)(2,1)}, bf16[3,16,128,128]{3,2,1,0:T(8,128)(2,1)}, u32[]{:S(2)}, u32[]{:S(2)}) collective-permute-start(bf16[3,16,128,128]{3,2,1,0:T(8,128)(2,1)} %get-tuple-element.13.refs_0_), channel_id=1, source_target_pairs={{0,16},{16,17},{17,1},{1,0},{2,18},{18,19},{19,3},{3,2},{4,20},{20... | collective-permute-start | bytes 4718600 | tf_op jit(solution)/shard_map/ppermute | solution.py:42
  23.3 2.7 %collective-permute-start.2 = (bf16[3,16,128,128]{3,2,1,0:T(8,128)(2,1)}, bf16[3,16,128,128]{3,2,1,0:T(8,128)(2,1)}, u32[]{:S(2)}, u32[]{:S(2)}) collective-permute-start(bf16[3,16,128,128]{3,2,1,0:T(8,128)(2,1)} %get-tuple-element.14.refs_1_), channel_id=1, source_target_pairs={{0,16},{16,19},{17,1},{1,2},{2,18},{18,17},{19,3},{3,0},{4,20},{20... | collective-permute-start | bytes 4718600 | tf_op jit(solution)/shard_map/ppermute | solution.py:42
  26.0 0.0 copy-done
  26.0 0.1 constant_dynamic-slice_fusion.1
  26.1 0.1 copy.13.ids_ref
  26.2 0.1 fusion.ids_row_ref
  26.3 0.2 shard_map.119
  26.5 9.4 %all-to-all-done.shares_ref = bf16[16,16,2048]{2,1,0:T(8,128)(2,1)S(1)} async-done(((bf16[16,16,2048]{2,1,0:T(8,128)(2,1)}), bf16[16,16,2048]{2,1,0:T(8,128)(2,1)S(1)}, u32[]{:S(2)}, u32[]{:S(2)}) %all-to-all-start) | async-done | bytes 1048608 | tf_op jit(solution)/shard_map/all_to_all | solution.py:29
  35.9 0.0 copy-done.4
  35.9 0.0 copy-done.5
  35.9 0.5 shard_map.120
  36.4 33.6 %all_to_all.25 = bf16[16,8,1024]{2,1,0:T(8,128)(2,1)S(1)} all-to-all(bf16[16,8,1024]{2,1,0:T(8,128)(2,1)S(1)} %bitcast.27), channel_id=1, replica_groups=mesh['zg'=4,'zl'=4,'core'=2,'y'=4,'xh'=2,'xl'=2] {'zg','zl'}, dimensions={0} | all-to-all | bytes 524288 | tf_op jit(solution)/shard_map/all_to_all | solution.py:29
  70.0 1.7 shard_map.121
  71.7 3.7 %all-to-all-start.2 = ((bf16[16,32,2048]{2,1,0:T(8,128)(2,1)}), bf16[16,32,2048]{2,1,0:T(8,128)(2,1)S(1)}, u32[]{:S(2)}, u32[]{:S(2)}) async-start(bf16[16,32,2048]{2,1,0:T(8,128)(2,1)} %bitcast.9), calls=%async_computation.2 | async-start | bytes 4194304 | tf_op jit(solution)/shard_map/all_to_all | solution.py:29
  75.4 0.0 collective-permute-done.1.refs_2_
  75.4 2.5 %collective-permute-start.3 = (bf16[3,16,128,128]{3,2,1,0:T(8,128)(2,1)}, bf16[3,16,128,128]{3,2,1,0:T(8,128)(2,1)}, u32[]{:S(2)}, u32[]{:S(2)}) collective-permute-start(bf16[3,16,128,128]{3,2,1,0:T(8,128)(2,1)} %collective-permute-done.1.refs_2_), channel_id=1, source_target_pairs={{0,16},{17,1},{2,18},{19,3},{4,20},{21,5},{6,22},{23,7},{8,24},{25... | collective-permute-start | bytes 4718600 | tf_op jit(solution)/shard_map/ppermute | solution.py:46
  77.9 0.0 collective-permute-done.2.refs_3_
  77.9 2.4 %collective-permute-start.4 = (bf16[3,16,128,128]{3,2,1,0:T(8,128)(2,1)}, bf16[3,16,128,128]{3,2,1,0:T(8,128)(2,1)}, u32[]{:S(2)}, u32[]{:S(2)}) collective-permute-start(bf16[3,16,128,128]{3,2,1,0:T(8,128)(2,1)} %collective-permute-done.2.refs_3_), channel_id=1, source_target_pairs={{0,16},{17,1},{2,18},{19,3},{4,20},{21,5},{6,22},{23,7},{8,24},{25... | collective-permute-start | bytes 4718600 | tf_op jit(solution)/shard_map/ppermute | solution.py:46
  80.4 0.0 collective-permute-done.3.refs_4_
  80.4 2.2 %collective-permute-done.4.refs_5_ = bf16[3,16,128,128]{3,2,1,0:T(8,128)(2,1)} collective-permute-done((bf16[3,16,128,128]{3,2,1,0:T(8,128)(2,1)}, bf16[3,16,128,128]{3,2,1,0:T(8,128)(2,1)}, u32[]{:S(2)}, u32[]{:S(2)}) %collective-permute-start.4) | collective-permute-done | bytes 1572896 | tf_op jit(solution)/shard_map/ppermute | solution.py:46
  82.6 20.2 %all-to-all-done.2 = bf16[16,32,2048]{2,1,0:T(8,128)(2,1)S(1)} async-done(((bf16[16,32,2048]{2,1,0:T(8,128)(2,1)}), bf16[16,32,2048]{2,1,0:T(8,128)(2,1)S(1)}, u32[]{:S(2)}, u32[]{:S(2)}) %all-to-all-start.2) | async-done | bytes 2097184 | tf_op jit(solution)/shard_map/all_to_all | solution.py:29
  102.8 7.5 %shard_map.123 = bf16[512,2048]{1,0:T(8,128)(2,1)S(1)} custom-call(s32[1]{0:T(128)} %bitcast.kept_ref, bf16[512,2048]{1,0:T(8,128)(2,1)S(1)} %bitcast.20, bf16[3,16,128,128]{3,2,1,0:T(8,128)(2,1)} %get-tuple-element.13.refs_0_, bf16[3,16,128,128]{3,2,1,0:T(8,128)(2,1)} %get-tuple-element.14.refs_1_, ...), custom_call_target="tpu_custom_call" | custom-call | flops 3221225472 | bytes 10485760 | tf_op jit(solution)/shard_map/pallas_call | solution.py:409
  110.3 29.0 %all_to_all.26 = bf16[16,32,2048]{2,1,0:T(8,128)(2,1)S(1)} all-to-all(bf16[16,32,2048]{2,1,0:T(8,128)(2,1)S(1)} %bitcast.21), channel_id=1, replica_groups=mesh['zg'=4,'zl'=4,'core'=2,'y'=4,'xh'=2,'xl'=2] {'y','xh','xl'}, dimensions={0} | all-to-all | bytes 4194304 | tf_op jit(solution)/shard_map/all_to_all | solution.py:29
  139.2 0.0 copy-start.6
  139.2 1.2 shard_map.124
  140.5 10.8 %all-to-all-start.4 = ((bf16[16,8,1024]{2,1,0:T(8,128)(2,1)}), bf16[16,8,1024]{2,1,0:T(8,128)(2,1)S(1)}, u32[]{:S(2)}, u32[]{:S(2)}) async-start(bf16[16,8,1024]{2,1,0:T(8,128)(2,1)} %bitcast.16), calls=%async_computation.4 | async-start | bytes 524288 | tf_op jit(solution)/shard_map/all_to_all | solution.py:29
  151.3 0.0 copy-done.6
  151.3 0.1 constant_dynamic-slice_fusion
  151.4 0.1 copy.15.in_ref
  151.4 17.4 %all-to-all-done.4 = bf16[16,8,1024]{2,1,0:T(8,128)(2,1)S(1)} async-done(((bf16[16,8,1024]{2,1,0:T(8,128)(2,1)}), bf16[16,8,1024]{2,1,0:T(8,128)(2,1)S(1)}, u32[]{:S(2)}, u32[]{:S(2)}) %all-to-all-start.4) | async-done | bytes 262176 | tf_op jit(solution)/shard_map/all_to_all | solution.py:29
  168.9 0.8 shard_map.126
  (4 shorter events, 0.0 us)
Async XLA Ops:
  0.0 26.0 %copy-start = (s32[256,2]{0,1:T(2,128)S(1)}, s32[256,2]{0,1:T(2,128)}, u32[]{:S(2)}) copy-start(s32[256,2]{0,1:T(2,128)} %param.19) | copy-start | bytes 6148
  1.5 5.2 %collective-permute-start = (bf16[128,128]{1,0:T(8,128)(2,1)S(1)}, bf16[128,128]{1,0:T(8,128)(2,1)S(1)}, u32[]{:S(2)}, u32[]{:S(2)}) collective-permute-start(bf16[128,128]{1,0:T(8,128)(2,1)S(1)} %pad_maximum_fusion), channel_id=1, source_target_pairs={{0,16},{16,32},{32,48},{48,64},{64,80},{80,96},{96,112},{112,128},... | collective-permute-start | bytes 98312 | tf_op jit(solution)/shard_map/ppermute | solution.py:25
  6.7 10.7 %copy-start.1 = (bf16[1,2048,256]{2,1,0:T(8,128)(2,1)S(1)}, bf16[1,2048,256]{2,1,0:T(8,128)(2,1)}, u32[]{:S(2)}) copy-start(bf16[1,2048,256]{2,1,0:T(8,128)(2,1)} %param.21) | copy-start | bytes 3145732
  6.7 10.7 %copy-start.2 = (bf16[1,2048,256]{2,1,0:T(8,128)(2,1)S(1)}, bf16[1,2048,256]{2,1,0:T(8,128)(2,1)}, u32[]{:S(2)}) copy-start(bf16[1,2048,256]{2,1,0:T(8,128)(2,1)} %param.22) | copy-start | bytes 3145732
  10.4 25.5 %all-to-all-start = ((bf16[16,16,2048]{2,1,0:T(8,128)(2,1)}), bf16[16,16,2048]{2,1,0:T(8,128)(2,1)S(1)}, u32[]{:S(2)}, u32[]{:S(2)}) async-start(bf16[16,16,2048]{2,1,0:T(8,128)(2,1)} %bitcast.29), calls=%async_computation | async-start | bytes 2097152 | tf_op jit(solution)/shard_map/all_to_all | solution.py:29
  17.4 1.2 copy-start.3
  18.6 17.3 %copy-start.4 = (bf16[16,2048]{1,0:T(8,128)(2,1)S(1)}, bf16[16,2048]{1,0:T(8,128)(2,1)}, u32[]{:S(2)}) copy-start(bf16[16,2048]{1,0:T(8,128)(2,1)} %residual_ref.1) | copy-start | bytes 196612
  18.6 17.3 %copy-start.5 = (f32[2048]{0:T(1024)S(1)}, f32[2048]{0:T(1024)}, u32[]{:S(2)}) copy-start(f32[2048]{0:T(1024)} %param.18) | copy-start | bytes 24580
  21.4 54.0 %collective-permute-start.1 = (bf16[3,16,128,128]{3,2,1,0:T(8,128)(2,1)}, bf16[3,16,128,128]{3,2,1,0:T(8,128)(2,1)}, u32[]{:S(2)}, u32[]{:S(2)}) collective-permute-start(bf16[3,16,128,128]{3,2,1,0:T(8,128)(2,1)} %get-tuple-element.13.refs_0_), channel_id=1, source_target_pairs={{0,16},{16,17},{17,1},{1,0},{2,18},{18,19},{19,3},{3,2},{4,20},{20... | collective-permute-start | bytes 4718600 | tf_op jit(solution)/shard_map/ppermute | solution.py:42
  23.3 54.6 %collective-permute-start.2 = (bf16[3,16,128,128]{3,2,1,0:T(8,128)(2,1)}, bf16[3,16,128,128]{3,2,1,0:T(8,128)(2,1)}, u32[]{:S(2)}, u32[]{:S(2)}) collective-permute-start(bf16[3,16,128,128]{3,2,1,0:T(8,128)(2,1)} %get-tuple-element.14.refs_1_), channel_id=1, source_target_pairs={{0,16},{16,19},{17,1},{1,2},{2,18},{18,17},{19,3},{3,0},{4,20},{20... | collective-permute-start | bytes 4718600 | tf_op jit(solution)/shard_map/ppermute | solution.py:42
  71.7 31.1 %all-to-all-start.2 = ((bf16[16,32,2048]{2,1,0:T(8,128)(2,1)}), bf16[16,32,2048]{2,1,0:T(8,128)(2,1)S(1)}, u32[]{:S(2)}, u32[]{:S(2)}) async-start(bf16[16,32,2048]{2,1,0:T(8,128)(2,1)} %bitcast.9), calls=%async_computation.2 | async-start | bytes 4194304 | tf_op jit(solution)/shard_map/all_to_all | solution.py:29
  75.4 5.0 %collective-permute-start.3 = (bf16[3,16,128,128]{3,2,1,0:T(8,128)(2,1)}, bf16[3,16,128,128]{3,2,1,0:T(8,128)(2,1)}, u32[]{:S(2)}, u32[]{:S(2)}) collective-permute-start(bf16[3,16,128,128]{3,2,1,0:T(8,128)(2,1)} %collective-permute-done.1.refs_2_), channel_id=1, source_target_pairs={{0,16},{17,1},{2,18},{19,3},{4,20},{21,5},{6,22},{23,7},{8,24},{25... | collective-permute-start | bytes 4718600 | tf_op jit(solution)/shard_map/ppermute | solution.py:46
  77.9 4.6 %collective-permute-start.4 = (bf16[3,16,128,128]{3,2,1,0:T(8,128)(2,1)}, bf16[3,16,128,128]{3,2,1,0:T(8,128)(2,1)}, u32[]{:S(2)}, u32[]{:S(2)}) collective-permute-start(bf16[3,16,128,128]{3,2,1,0:T(8,128)(2,1)} %collective-permute-done.2.refs_3_), channel_id=1, source_target_pairs={{0,16},{17,1},{2,18},{19,3},{4,20},{21,5},{6,22},{23,7},{8,24},{25... | collective-permute-start | bytes 4718600 | tf_op jit(solution)/shard_map/ppermute | solution.py:46
  139.2 12.0 %copy-start.6 = (f32[256,2]{0,1:T(2,128)S(1)}, f32[256,2]{0,1:T(2,128)}, u32[]{:S(2)}) copy-start(f32[256,2]{0,1:T(2,128)} %param.20) | copy-start | bytes 6148
  140.5 28.4 %all-to-all-start.4 = ((bf16[16,8,1024]{2,1,0:T(8,128)(2,1)}), bf16[16,8,1024]{2,1,0:T(8,128)(2,1)S(1)}, u32[]{:S(2)}, u32[]{:S(2)}) async-start(bf16[16,8,1024]{2,1,0:T(8,128)(2,1)} %bitcast.16), calls=%async_computation.4 | async-start | bytes 524288 | tf_op jit(solution)/shard_map/all_to_all | solution.py:29

commit v4 on v3

--- a/solution.py
+++ b/solution.py
@@ -13,10 +13,22 @@
 norm_epsilon = 1e-06
 
 
-SP = ("zg", "zl", "core")
-TP = ("y", "xh", "xl")
-SIZES = (4, 4, 2, 4, 2, 2)
-ROUTE = ("zg", "zl")
+SP = ("z3", "z2", "z1", "z0", "core")
+TP = ("y1", "y0", "x1", "x0")
+ROUTE = ("z3", "z2", "z1", "z0")
+CHIPS = ("x1", "x0", "y1", "y0")
+OWNERS = ("x1", "x0", "y1", "y0")
+
+
+def place(index, axes, order):
+    return sum(
+        ((index >> (len(axes) - 1 - axes.index(name))) & 1) << (len(order) - 1 - at)
+        for at, name in enumerate(order)
+    )
+
+
+def column_parity(block):
+    return place(block, CHIPS, TP) % 2
 
 
 def from_behind(block, axis, distance):
@@ -39,11 +51,11 @@
             (here * columns + x, (1 - here) * columns + x),
             ((1 - here) * columns + x, (1 - here) * columns + beside),
         ]
-    return lax.ppermute(pack, ("core", "xh", "xl"), route)
+    return lax.ppermute(pack, ("core", "x1", "x0"), route)
 
 
 def pass_on(pack):
-    return lax.ppermute(pack, ("core", "xl"), [(0, 2), (3, 1)])
+    return lax.ppermute(pack, ("core", "x0"), [(0, 2), (3, 1)])
 
 
 IN_VMEM = pl.BlockSpec(memory_space=pltpu.VMEM)
@@ -55,7 +67,6 @@
 PLANES = 16
 PAIR = 2
 RANKS = 2
-DEPTH = 4
 
 
 def near(array):
@@ -129,14 +140,18 @@
         )
         attended = (weighted / denominator).astype(jnp.bfloat16)
         attended = jnp.concatenate([attended[:, :WINDOW], attended[:, WINDOW:]], 0)
-        out_ref[at : at + WINDOW] = over_rows(attended, weight_ref[...]).astype(jnp.bfloat16)
-
-
-def attention_share(edge, sinks, queries, keys_t, values_t, rim, angles, weight):
+        share = over_rows(attended, weight_ref[...]).astype(jnp.bfloat16)
+        rows = out_ref.shape[1]
+        for k in range(WINDOW // rows):
+            to = place(at // rows + k, TP, OWNERS)
+            out_ref[to] = share[k * rows : (k + 1) * rows]
+
+
+def attention_share(edge, sinks, queries, keys_t, values_t, rim, angles, weight, chips):
     count, width = queries.shape[0], weight.shape[1]
     return pl.pallas_call(
         attend_kernel,
-        out_shape=jax.ShapeDtypeStruct((count, width), jnp.bfloat16),
+        out_shape=jax.ShapeDtypeStruct((chips, count // chips, width), jnp.bfloat16),
         in_specs=[IN_SMEM] * 2 + [IN_VMEM] * 7,
         out_specs=IN_VMEM,
         cost_estimate=pl.CostEstimate(
@@ -163,8 +178,8 @@
             before = jnp.where((other_col == row) & (below < right), 1, 0)
             rank_row = rank_row + jnp.sum(before, 0, keepdims=True)
         for half in range(2):
-            line_col = (col >> 1) * LINES + half * SLOTS + (col & 1) * RANKS + rank_col
-            line_row = (row >> 1) * LINES + half * SLOTS + (row & 1) * RANKS + rank_row
+            line_col = place(col >> 1, SP[:-1], ROUTE) * LINES + half * SLOTS + (col & 1) * RANKS + rank_col
+            line_row = place(row >> 1, SP[:-1], ROUTE) * LINES + half * SLOTS + (row & 1) * RANKS + rank_row
             collect_ref[half, k * rows : (k + 1) * rows, :] = one_hot(
                 iota((rows, lines), 1) == line_col
             )
@@ -278,41 +293,41 @@
 
 def fan_kernel(lines_ref, out_ref):
     half = lines_ref.shape[1]
+    count = out_ref.shape[1]
     for h in range(2):
         rows = dot(one_hot(lines_of(h)), lines_ref[...]).astype(jnp.bfloat16)
         for to in range(out_ref.shape[0]):
-            out_ref[to, :, h * half : (h + 1) * half] = rows
-
-
-def fan(lines, team):
-    rows, width = PAIR * PLANES * RANKS, 2 * lines.shape[1]
+            at = column_parity(to) * count
+            out_ref[to, :, h * half : (h + 1) * half] = rows[at : at + count]
+
+
+def fan(lines, chips):
+    rows, width = PLANES * RANKS, 2 * lines.shape[1]
     return pl.pallas_call(
         fan_kernel,
-        out_shape=pltpu.VMEM((team, rows, width), jnp.bfloat16),
+        out_shape=pltpu.VMEM((chips, rows, width), jnp.bfloat16),
         in_specs=[IN_VMEM],
         out_specs=IN_VMEM,
         compiler_params=room(16),
-        cost_estimate=price(2 * rows * lines.size * 2, 2 * team * rows * width),
+        cost_estimate=price(8 * rows * lines.size, 2 * chips * rows * width),
     )(near(lines))
 
 
 def fold_kernel(parts_ref, out_ref):
     half = out_ref.shape[1]
-    rows = jnp.sum(parts_ref[...].astype(jnp.float32), 0).astype(jnp.bfloat16)
     lines = 0.0
+    totals = [0.0] * PAIR
+    for chip in range(parts_ref.shape[0]):
+        expert = column_parity(chip)
+        totals[expert] = totals[expert] + parts_ref[chip].astype(jnp.float32)
+    rows = jnp.concatenate(totals, 0).astype(jnp.bfloat16)
     for h in range(2):
-        take = one_hot(lines_of(h))
-        lines = lines + lax.dot_general(
-            take,
-            rows[:, h * half : (h + 1) * half],
-            (((0,), (0,)), ((), ())),
-            preferred_element_type=jnp.float32,
-        )
+        lines = lines + over_rows(one_hot(lines_of(h)), rows[:, h * half : (h + 1) * half])
     out_ref[...] = lines.astype(jnp.bfloat16)
 
 
 def fold(parts):
-    width = parts.shape[2]
+    width = parts.shape[-1]
     lines = PLANES * LINES
     return pl.pallas_call(
         fold_kernel,
@@ -320,7 +335,7 @@
         in_specs=[IN_VMEM],
         out_specs=IN_VMEM,
         compiler_params=room(24),
-        cost_estimate=price(2 * lines * parts.shape[1] * width, 2 * parts.size),
+        cost_estimate=price(2 * lines * PAIR * parts.shape[1] * width, 2 * parts.size),
     )(near(parts))
 
 
@@ -374,26 +389,22 @@
             for half in halves:
                 copy(passed, slot, kind, half).start()
 
-    order = [(0, 0), (0, 1), (1, 0), (1, 1), (0, 2), (1, 2)]
-
-    def ready(at):
-        for half in halves:
-            copy(turned, *order[at], half).wait()
-        if at + DEPTH < len(order):
-            fetch(*order[at + DEPTH])
-
-    for at in range(DEPTH):
-        fetch(*order[at])
+    def ready(slot, kinds):
+        for kind in kinds:
+            for half in halves:
+                copy(turned, slot, kind, half).wait()
+
+    for slot, kind in ((0, 0), (0, 1), (1, 0), (1, 1), (0, 2), (1, 2)):
+        fetch(slot, kind)
     rows = rows_ref[...]
     hidden = []
     for slot in range(2):
-        ready(2 * slot)
+        ready(slot, (0, 1))
         gate_val = dot(rows, gates[slot].reshape(rows.shape[1], -1))
-        ready(2 * slot + 1)
         up_val = dot(rows, ups[slot].reshape(rows.shape[1], -1))
         hidden.append((gate_val / (1.0 + jnp.exp(-gate_val)) * up_val).astype(jnp.bfloat16))
-    ready(4)
-    ready(5)
+    ready(0, (2,))
+    ready(1, (2,))
     chunk = 512
     for at in range(0, out_ref.shape[1], chunk):
         total = 0.0
@@ -442,6 +453,7 @@
 ):
     local_len = queries.shape[0]
     span = lax.axis_index(SP)
+    chips = lax.axis_size(TP)
     keys_t, values_t = key_rows.T, values.T
     rim = jnp.concatenate([keys_t[:, -WINDOW:], values_t[:, -WINDOW:]], 0)
     rim = from_behind(rim, SP, 1)
@@ -451,36 +463,37 @@
     angles = positions.astype(jnp.float32)[None, :] * frequency[:, None]
     angles = (jnp.cos(angles), jnp.sin(angles))
     edge = jnp.where(span == 0, WINDOW, 0).astype(jnp.int32).reshape(1)
-    shares = attention_share(edge, sink_logits, queries, keys_t, values_t, rim, angles, out_weight)
+    shares = attention_share(
+        edge, sink_logits, queries, keys_t, values_t, rim, angles, out_weight, chips
+    )
     tok_rows, width = residual.shape
     first = lax.axis_index(TP) * tok_rows
     own_ids = lax.dynamic_slice_in_dim(expert_ids, first, tok_rows, 0)
     own_weights = lax.dynamic_slice_in_dim(route_weight, first, tok_rows, 0)
-    shares = exchange(shares.reshape(lax.axis_size(TP), -1, width), TP)
+    shares = exchange(shares, OWNERS)
     own = pack(gate_proj[0], up_proj[0], down_proj[0])
     right = turn(own[0], 1)
     left = turn(own[1], -1)
     spread, collect = plan(own_ids)
     middle, lines = settle(shares, residual, norm_gain.reshape(1, -1), spread)
     lines = exchange(lines.reshape(PLANES, LINES, width // 2), ROUTE)
-    team = lax.axis_size(TP) // PAIR
-    fanned = fan(lines.reshape(PLANES * LINES, width // 2), team)
-    gathered = exchange(fanned.reshape(team * PAIR, -1, width), TP)
+    fanned = fan(lines.reshape(PLANES * LINES, width // 2), chips)
+    gathered = exchange(fanned, CHIPS)
     right_too = pass_on(right)
     left_too = pass_on(left)
-    kept = (lax.axis_index("core") == lax.axis_index("xl")).astype(jnp.int32).reshape(1)
+    kept = (lax.axis_index("core") == lax.axis_index("x0")).astype(jnp.int32).reshape(1)
     own_weights = hold(own_weights)
     parts = expert_part(
         kept, gathered.reshape(-1, width), own, (right, left), (right_too, left_too)
     )
-    parts = exchange(parts.reshape(team * PAIR, -1, width), TP)
-    lines = fold(parts.reshape(team, -1, width))
+    parts = exchange(parts.reshape(chips, -1, width), CHIPS)
+    lines = fold(parts)
     lines = exchange(lines.reshape(PLANES, LINES, width // 2), ROUTE)
     return finish(lines.reshape(PLANES * LINES, width // 2), collect, own_weights, middle)
 
 
 def solution(mesh):
-    fine = jax.sharding.Mesh(mesh.devices.reshape(SIZES), SP + TP)
+    fine = jax.sharding.Mesh(mesh.devices.reshape([2] * len(SP + TP)), SP + TP)
     return jax.shard_map(
         per_device,
         mesh=fine,

time: 170 us -> 162 us (0.953)
  the two profiles are of different devices: /device:TPU:32 before, /device:TPU:8 now
where the time goes in v4:
time: 162 us; the launch traced here: 161 us
  blocking collectives  58.6 us (36%)
  starting transfers between devices  41.9 us (26%)
  waiting for transfers between devices  40.9 us (25%)
  Pallas kernels  16.3 us (10%)
  local copies, waits for them, and re-layouts  3.09 us (2%)
    all_to_all x2, blocking collectives, exchange(): return lax.all_to_all(blocks, axis, 0, 0, tiled=True)  58.6 us
    all_to_all x3, waiting for transfers between devices, exchange(): return lax.all_to_all(blocks, axis, 0, 0, tiled=True)  38.1 us
    all_to_all x3, starting transfers between devices, exchange(): return lax.all_to_all(blocks, axis, 0, 0, tiled=True)  29.8 us
    pallas_call x1, Pallas kernels, expert_part(): pl.pallas_call(expert_kernel, out_shape=pltpu.VMEM((count, width), jnp.bf...  5.43 us
    ppermute x2, starting transfers between devices, turn(): return lax.ppermute(pack, ('core', 'x1', 'x0'), route)  5.39 us
    ppermute x2, starting transfers between devices, pass_on(): return lax.ppermute(pack, ('core', 'x0'), [(0, 2), (3, 1)])  4.95 us
    pallas_call x1, Pallas kernels, attention_share(): pl.pallas_call(attend_kernel, out_shape=jax.ShapeDtypeStruct((chips, coun...  3.66 us
  transfers between devices with their start and end apart: 8, of which 5 were waited for; matrix products, arithmetic and copies ran while one was open for 0% of the time, Pallas kernels for 3%

profile of v4, /device:TPU:8, one launch (start us, length us, event | category | flops | bytes accessed | tf_op | source)
XLA Modules:
  0.0 161.2 jit_solution(3103609412741209340)
XLA Ops:
  0.0 0.0 copy-start
  0.0 0.7 slice.8
  0.7 0.7 slice.9
  1.5 1.7 %collective-permute-start = (bf16[128,128]{1,0:T(8,128)(2,1)S(1)}, bf16[128,128]{1,0:T(8,128)(2,1)S(1)}, u32[]{:S(2)}, u32[]{:S(2)}) collective-permute-start(bf16[128,128]{1,0:T(8,128)(2,1)S(1)} %pad_maximum_fusion), channel_id=1, source_target_pairs={{0,16},{16,32},{32,48},{48,64},{64,80},{80,96},{96,112},{112,128},... | collective-permute-start | bytes 98312 | tf_op jit(solution)/shard_map/ppermute | solution.py:37
  3.2 0.3 multiply_sine_fusion
  3.5 0.5 collective-permute-done.rim_ref
  4.0 0.0 copy-start.1
  4.0 0.0 copy-start.2
  4.0 3.7 %shard_map.118 = bf16[16,16,2048]{2,1,0:T(8,128)(2,1)} custom-call(s32[1]{0:T(128)} %bitcast.1.edge_ref, f32[2]{0:T(128)} %sink_ref.1, bf16[256,128]{1,0:T(8,128)(2,1)} %query_ref.1, bf16[64,256]{1,0:T(8,128)(2,1)} %bitcast.26, bf16[64,256]{1,0:T(8,128)(2,1)} %bitcast.28, bf16[128,128]{1,0:T(8,128)(2,1)S(1)} %collective-permute-done.rim_ref, ...), custom_call_target="tpu_custom_call" | custom-call | flops 201326592 | bytes 1572864 | tf_op jit(solution)/shard_map/pallas_call | solution.py:152
  7.7 8.8 %all-to-all-start = ((bf16[16,16,2048]{2,1,0:T(8,128)(2,1)}), bf16[16,16,2048]{2,1,0:T(8,128)(2,1)S(1)}, u32[]{:S(2)}, u32[]{:S(2)}) async-start(bf16[16,16,2048]{2,1,0:T(8,128)(2,1)} %shard_map.118), calls=%async_computation | async-start | bytes 2097152 | tf_op jit(solution)/shard_map/all_to_all | solution.py:41
  16.5 0.0 copy-done.1
  16.5 0.0 copy-done.2
  16.5 0.0 copy-start.3
  16.5 1.2 copy-done.3
  17.8 0.0 copy-start.4
  17.8 0.0 copy-start.5
  17.8 2.7 %shard_map.122 = (bf16[3,16,128,128]{3,2,1,0:T(8,128)(2,1)}, bf16[3,16,128,128]{3,2,1,0:T(8,128)(2,1)}) custom-call(bf16[16,128,256]{2,1,0:T(8,128)(2,1)S(1)} %bitcast.18, bf16[16,128,256]{2,1,0:T(8,128)(2,1)S(1)} %bitcast.19, bf16[256,2048]{1,0:T(8,128)(2,1)S(1)} %bitcast.20), custom_call_target="tpu_custom_call" | custom-call | flops 1000000 | bytes 6291456 | tf_op jit(solution)/shard_map/pallas_call | solution.py:232
  20.5 2.3 %collective-permute-start.1 = (bf16[3,16,128,128]{3,2,1,0:T(8,128)(2,1)}, bf16[3,16,128,128]{3,2,1,0:T(8,128)(2,1)}, u32[]{:S(2)}, u32[]{:S(2)}) collective-permute-start(bf16[3,16,128,128]{3,2,1,0:T(8,128)(2,1)} %get-tuple-element.13.refs_0_), channel_id=1, source_target_pairs={{0,16},{16,17},{17,1},{1,0},{2,18},{18,19},{19,3},{3,2},{4,20},{20... | collective-permute-start | bytes 4718600 | tf_op jit(solution)/shard_map/ppermute | solution.py:54
  22.8 3.1 %collective-permute-start.2 = (bf16[3,16,128,128]{3,2,1,0:T(8,128)(2,1)}, bf16[3,16,128,128]{3,2,1,0:T(8,128)(2,1)}, u32[]{:S(2)}, u32[]{:S(2)}) collective-permute-start(bf16[3,16,128,128]{3,2,1,0:T(8,128)(2,1)} %get-tuple-element.14.refs_1_), channel_id=1, source_target_pairs={{0,16},{16,19},{17,1},{1,2},{2,18},{18,17},{19,3},{3,0},{4,20},{20... | collective-permute-start | bytes 4718600 | tf_op jit(solution)/shard_map/ppermute | solution.py:54
  25.9 0.0 copy-done
  25.9 0.1 constant_dynamic-slice_fusion.1
  26.0 0.1 copy.13.ids_ref
  26.1 0.1 fusion.ids_row_ref
  26.1 0.2 shard_map.119
  26.4 7.9 %all-to-all-done.shares_ref = bf16[16,16,2048]{2,1,0:T(8,128)(2,1)S(1)} async-done(((bf16[16,16,2048]{2,1,0:T(8,128)(2,1)}), bf16[16,16,2048]{2,1,0:T(8,128)(2,1)S(1)}, u32[]{:S(2)}, u32[]{:S(2)}) %all-to-all-start) | async-done | bytes 1048608 | tf_op jit(solution)/shard_map/all_to_all | solution.py:41
  34.3 0.0 copy-done.4
  34.3 0.0 copy-done.5
  34.4 0.5 shard_map.120
  34.9 32.0 %all_to_all.25 = bf16[16,8,1024]{2,1,0:T(8,128)(2,1)S(1)} all-to-all(bf16[16,8,1024]{2,1,0:T(8,128)(2,1)S(1)} %bitcast.23), channel_id=1, replica_groups=mesh['z3'=2,'z2'=2,'z1'=2,'z0'=2,'core'=2,'y1'=2,'y0'=2,'x1'=2,'x0'=2] {..., dimensions={0} | all-to-all | bytes 524288 | tf_op jit(solution)/shard_map/all_to_all | solution.py:41
  66.9 1.7 %shard_map.121 = bf16[16,32,2048]{2,1,0:T(8,128)(2,1)} custom-call(bf16[128,1024]{1,0:T(8,128)(2,1)S(1)} %bitcast.21), custom_call_target="tpu_custom_call" | custom-call | flops 33554432 | bytes 2097152 | tf_op jit(solution)/shard_map/pallas_call | solution.py:306
  68.6 5.0 %all-to-all-start.2 = ((bf16[16,32,2048]{2,1,0:T(8,128)(2,1)}), bf16[16,32,2048]{2,1,0:T(8,128)(2,1)S(1)}, u32[]{:S(2)}, u32[]{:S(2)}) async-start(bf16[16,32,2048]{2,1,0:T(8,128)(2,1)} %shard_map.121), calls=%async_computation.2 | async-start | bytes 4194304 | tf_op jit(solution)/shard_map/all_to_all | solution.py:41
  73.6 0.0 collective-permute-done.1.refs_2_
  73.6 2.5 %collective-permute-start.3 = (bf16[3,16,128,128]{3,2,1,0:T(8,128)(2,1)}, bf16[3,16,128,128]{3,2,1,0:T(8,128)(2,1)}, u32[]{:S(2)}, u32[]{:S(2)}) collective-permute-start(bf16[3,16,128,128]{3,2,1,0:T(8,128)(2,1)} %collective-permute-done.1.refs_2_), channel_id=1, source_target_pairs={{0,16},{17,1},{2,18},{19,3},{4,20},{21,5},{6,22},{23,7},{8,24},{25... | collective-permute-start | bytes 4718600 | tf_op jit(solution)/shard_map/ppermute | solution.py:58
  76.1 0.0 collective-permute-done.2.refs_3_
  76.1 2.4 %collective-permute-start.4 = (bf16[3,16,128,128]{3,2,1,0:T(8,128)(2,1)}, bf16[3,16,128,128]{3,2,1,0:T(8,128)(2,1)}, u32[]{:S(2)}, u32[]{:S(2)}) collective-permute-start(bf16[3,16,128,128]{3,2,1,0:T(8,128)(2,1)} %collective-permute-done.2.refs_3_), channel_id=1, source_target_pairs={{0,16},{17,1},{2,18},{19,3},{4,20},{21,5},{6,22},{23,7},{8,24},{25... | collective-permute-start | bytes 4718600 | tf_op jit(solution)/shard_map/ppermute | solution.py:58
  78.6 0.0 collective-permute-done.3.refs_4_
  78.6 2.2 %collective-permute-done.4.refs_5_ = bf16[3,16,128,128]{3,2,1,0:T(8,128)(2,1)} collective-permute-done((bf16[3,16,128,128]{3,2,1,0:T(8,128)(2,1)}, bf16[3,16,128,128]{3,2,1,0:T(8,128)(2,1)}, u32[]{:S(2)}, u32[]{:S(2)}) %collective-permute-start.4) | collective-permute-done | bytes 1572896 | tf_op jit(solution)/shard_map/ppermute | solution.py:58
  80.8 13.9 %all-to-all-done.2 = bf16[16,32,2048]{2,1,0:T(8,128)(2,1)S(1)} async-done(((bf16[16,32,2048]{2,1,0:T(8,128)(2,1)}), bf16[16,32,2048]{2,1,0:T(8,128)(2,1)S(1)}, u32[]{:S(2)}, u32[]{:S(2)}) %all-to-all-start.2) | async-done | bytes 2097184 | tf_op jit(solution)/shard_map/all_to_all | solution.py:41
  94.7 5.4 %shard_map.123 = bf16[512,2048]{1,0:T(8,128)(2,1)S(1)} custom-call(s32[1]{0:T(128)} %bitcast.kept_ref, bf16[512,2048]{1,0:T(8,128)(2,1)S(1)} %bitcast.16, bf16[3,16,128,128]{3,2,1,0:T(8,128)(2,1)} %get-tuple-element.13.refs_0_, bf16[3,16,128,128]{3,2,1,0:T(8,128)(2,1)} %get-tuple-element.14.refs_1_, ...), custom_call_target="tpu_custom_call" | custom-call | flops 3221225472 | bytes 10485760 | tf_op jit(solution)/shard_map/pallas_call | solution.py:420
  100.2 26.6 %all_to_all.26.parts_ref = bf16[16,32,2048]{2,1,0:T(8,128)(2,1)S(1)} all-to-all(bf16[16,32,2048]{2,1,0:T(8,128)(2,1)S(1)} %bitcast.17), channel_id=1, replica_groups=mesh['z3'=2,'z2'=2,'z1'=2,'z0'=2,'core'=2,'y1'=2,'y0'=2,'x1'=2,'x0'=2] {..., dimensions={0} | all-to-all | bytes 4194304 | tf_op jit(solution)/shard_map/all_to_all | solution.py:41
  126.7 0.0 copy-start.6
  126.7 1.2 shard_map.124
  127.9 16.0 %all-to-all-start.4 = ((bf16[16,8,1024]{2,1,0:T(8,128)(2,1)}), bf16[16,8,1024]{2,1,0:T(8,128)(2,1)S(1)}, u32[]{:S(2)}, u32[]{:S(2)}) async-start(bf16[16,8,1024]{2,1,0:T(8,128)(2,1)} %bitcast.13), calls=%async_computation.4 | async-start | bytes 524288 | tf_op jit(solution)/shard_map/all_to_all | solution.py:41
  143.9 0.0 copy-done.6
  143.9 0.1 constant_dynamic-slice_fusion
  144.0 0.1 copy.15.in_ref
  144.1 16.3 %all-to-all-done.4 = bf16[16,8,1024]{2,1,0:T(8,128)(2,1)S(1)} async-done(((bf16[16,8,1024]{2,1,0:T(8,128)(2,1)}), bf16[16,8,1024]{2,1,0:T(8,128)(2,1)S(1)}, u32[]{:S(2)}, u32[]{:S(2)}) %all-to-all-start.4) | async-done | bytes 262176 | tf_op jit(solution)/shard_map/all_to_all | solution.py:41
  160.4 0.8 shard_map.126
  (4 shorter events, 0.0 us)
Async XLA Ops:
  0.0 25.9 %copy-start = (s32[256,2]{0,1:T(2,128)S(1)}, s32[256,2]{0,1:T(2,128)}, u32[]{:S(2)}) copy-start(s32[256,2]{0,1:T(2,128)} %param.19) | copy-start | bytes 6148
  1.5 2.6 %collective-permute-start = (bf16[128,128]{1,0:T(8,128)(2,1)S(1)}, bf16[128,128]{1,0:T(8,128)(2,1)S(1)}, u32[]{:S(2)}, u32[]{:S(2)}) collective-permute-start(bf16[128,128]{1,0:T(8,128)(2,1)S(1)} %pad_maximum_fusion), channel_id=1, source_target_pairs={{0,16},{16,32},{32,48},{48,64},{64,80},{80,96},{96,112},{112,128},... | collective-permute-start | bytes 98312 | tf_op jit(solution)/shard_map/ppermute | solution.py:37
  4.0 12.5 %copy-start.1 = (bf16[1,2048,256]{2,1,0:T(8,128)(2,1)S(1)}, bf16[1,2048,256]{2,1,0:T(8,128)(2,1)}, u32[]{:S(2)}) copy-start(bf16[1,2048,256]{2,1,0:T(8,128)(2,1)} %param.21) | copy-start | bytes 3145732
  4.0 12.5 %copy-start.2 = (bf16[1,2048,256]{2,1,0:T(8,128)(2,1)S(1)}, bf16[1,2048,256]{2,1,0:T(8,128)(2,1)}, u32[]{:S(2)}) copy-start(bf16[1,2048,256]{2,1,0:T(8,128)(2,1)} %param.22) | copy-start | bytes 3145732
  7.7 26.6 %all-to-all-start = ((bf16[16,16,2048]{2,1,0:T(8,128)(2,1)}), bf16[16,16,2048]{2,1,0:T(8,128)(2,1)S(1)}, u32[]{:S(2)}, u32[]{:S(2)}) async-start(bf16[16,16,2048]{2,1,0:T(8,128)(2,1)} %shard_map.118), calls=%async_computation | async-start | bytes 2097152 | tf_op jit(solution)/shard_map/all_to_all | solution.py:41
  16.5 1.2 copy-start.3
  17.8 16.6 %copy-start.4 = (bf16[16,2048]{1,0:T(8,128)(2,1)S(1)}, bf16[16,2048]{1,0:T(8,128)(2,1)}, u32[]{:S(2)}) copy-start(bf16[16,2048]{1,0:T(8,128)(2,1)} %residual_ref.1) | copy-start | bytes 196612
  17.8 16.6 %copy-start.5 = (f32[2048]{0:T(1024)S(1)}, f32[2048]{0:T(1024)}, u32[]{:S(2)}) copy-start(f32[2048]{0:T(1024)} %param.18) | copy-start | bytes 24580
  20.5 53.1 %collective-permute-start.1 = (bf16[3,16,128,128]{3,2,1,0:T(8,128)(2,1)}, bf16[3,16,128,128]{3,2,1,0:T(8,128)(2,1)}, u32[]{:S(2)}, u32[]{:S(2)}) collective-permute-start(bf16[3,16,128,128]{3,2,1,0:T(8,128)(2,1)} %get-tuple-element.13.refs_0_), channel_id=1, source_target_pairs={{0,16},{16,17},{17,1},{1,0},{2,18},{18,19},{19,3},{3,2},{4,20},{20... | collective-permute-start | bytes 4718600 | tf_op jit(solution)/shard_map/ppermute | solution.py:54
  22.8 53.3 %collective-permute-start.2 = (bf16[3,16,128,128]{3,2,1,0:T(8,128)(2,1)}, bf16[3,16,128,128]{3,2,1,0:T(8,128)(2,1)}, u32[]{:S(2)}, u32[]{:S(2)}) collective-permute-start(bf16[3,16,128,128]{3,2,1,0:T(8,128)(2,1)} %get-tuple-element.14.refs_1_), channel_id=1, source_target_pairs={{0,16},{16,19},{17,1},{1,2},{2,18},{18,17},{19,3},{3,0},{4,20},{20... | collective-permute-start | bytes 4718600 | tf_op jit(solution)/shard_map/ppermute | solution.py:54
  68.6 26.2 %all-to-all-start.2 = ((bf16[16,32,2048]{2,1,0:T(8,128)(2,1)}), bf16[16,32,2048]{2,1,0:T(8,128)(2,1)S(1)}, u32[]{:S(2)}, u32[]{:S(2)}) async-start(bf16[16,32,2048]{2,1,0:T(8,128)(2,1)} %shard_map.121), calls=%async_computation.2 | async-start | bytes 4194304 | tf_op jit(solution)/shard_map/all_to_all | solution.py:41
  73.6 5.0 %collective-permute-start.3 = (bf16[3,16,128,128]{3,2,1,0:T(8,128)(2,1)}, bf16[3,16,128,128]{3,2,1,0:T(8,128)(2,1)}, u32[]{:S(2)}, u32[]{:S(2)}) collective-permute-start(bf16[3,16,128,128]{3,2,1,0:T(8,128)(2,1)} %collective-permute-done.1.refs_2_), channel_id=1, source_target_pairs={{0,16},{17,1},{2,18},{19,3},{4,20},{21,5},{6,22},{23,7},{8,24},{25... | collective-permute-start | bytes 4718600 | tf_op jit(solution)/shard_map/ppermute | solution.py:58
  76.1 4.6 %collective-permute-start.4 = (bf16[3,16,128,128]{3,2,1,0:T(8,128)(2,1)}, bf16[3,16,128,128]{3,2,1,0:T(8,128)(2,1)}, u32[]{:S(2)}, u32[]{:S(2)}) collective-permute-start(bf16[3,16,128,128]{3,2,1,0:T(8,128)(2,1)} %collective-permute-done.2.refs_3_), channel_id=1, source_target_pairs={{0,16},{17,1},{2,18},{19,3},{4,20},{21,5},{6,22},{23,7},{8,24},{25... | collective-permute-start | bytes 4718600 | tf_op jit(solution)/shard_map/ppermute | solution.py:58
  126.7 17.2 %copy-start.6 = (f32[256,2]{0,1:T(2,128)S(1)}, f32[256,2]{0,1:T(2,128)}, u32[]{:S(2)}) copy-start(f32[256,2]{0,1:T(2,128)} %param.20) | copy-start | bytes 6148
  127.9 32.4 %all-to-all-start.4 = ((bf16[16,8,1024]{2,1,0:T(8,128)(2,1)}), bf16[16,8,1024]{2,1,0:T(8,128)(2,1)S(1)}, u32[]{:S(2)}, u32[]{:S(2)}) async-start(bf16[16,8,1024]{2,1,0:T(8,128)(2,1)} %bitcast.13), calls=%async_computation.4 | async-start | bytes 524288 | tf_op jit(solution)/shard_map/all_to_all | solution.py:41

commit v5 on v4

--- a/solution.py
+++ b/solution.py
@@ -13,22 +13,17 @@
 norm_epsilon = 1e-06
 
 
-SP = ("z3", "z2", "z1", "z0", "core")
-TP = ("y1", "y0", "x1", "x0")
-ROUTE = ("z3", "z2", "z1", "z0")
-CHIPS = ("x1", "x0", "y1", "y0")
-OWNERS = ("x1", "x0", "y1", "y0")
-
-
-def place(index, axes, order):
-    return sum(
-        ((index >> (len(axes) - 1 - axes.index(name))) & 1) << (len(order) - 1 - at)
-        for at, name in enumerate(order)
-    )
-
-
-def column_parity(block):
-    return place(block, CHIPS, TP) % 2
+SP = ("z", "core")
+TP = ("y", "x")
+SIZES = (16, 2, 4, 4)
+HEIGHT, WIDTH = SIZES[2:]
+COLUMNS = [y * WIDTH + x for x in range(WIDTH) for y in range(HEIGHT)]
+ORDERS = (COLUMNS, COLUMNS[::-1])
+GROUPS = [[core * HEIGHT * WIDTH + chip for chip in order] for core, order in enumerate(ORDERS)]
+
+
+def column_parity(block, core):
+    return ORDERS[core][block] % WIDTH % 2
 
 
 def from_behind(block, axis, distance):
@@ -37,8 +32,14 @@
     return lax.ppermute(block, axis, route)
 
 
-def exchange(blocks, axis):
-    return lax.all_to_all(blocks, axis, 0, 0, tiled=True)
+def in_plane(blocks):
+    return lax.all_to_all(
+        blocks, ("core",) + TP, 0, 0, axis_index_groups=GROUPS, tiled=True
+    )
+
+
+def along_z(blocks):
+    return lax.all_to_all(blocks, "z", 0, 0, tiled=True)
 
 
 def turn(pack, side):
@@ -51,11 +52,12 @@
             (here * columns + x, (1 - here) * columns + x),
             ((1 - here) * columns + x, (1 - here) * columns + beside),
         ]
-    return lax.ppermute(pack, ("core", "x1", "x0"), route)
+    return lax.ppermute(pack, ("core", "x"), route)
 
 
 def pass_on(pack):
-    return lax.ppermute(pack, ("core", "x0"), [(0, 2), (3, 1)])
+    route = [((x % 2) * WIDTH + x, (1 - x % 2) * WIDTH + x) for x in range(WIDTH)]
+    return lax.ppermute(pack, ("core", "x"), route)
 
 
 IN_VMEM = pl.BlockSpec(memory_space=pltpu.VMEM)
@@ -71,6 +73,10 @@
 
 def near(array):
     return pltpu.with_memory_space_constraint(array, pltpu.VMEM)
+
+
+def far(array):
+    return pltpu.with_memory_space_constraint(array, pltpu.HBM)
 
 
 def iota(shape, dim):
@@ -106,7 +112,7 @@
 
 
 def attend_kernel(
-    edge_ref, sink_ref, query_ref, key_ref, value_ref, rim_ref, *refs
+    core_ref, edge_ref, sink_ref, query_ref, key_ref, value_ref, rim_ref, *refs
 ):
     count = query_ref.shape[0]
     cosine_ref, sine_ref, weight_ref, out_ref = refs
@@ -143,23 +149,50 @@
         share = over_rows(attended, weight_ref[...]).astype(jnp.bfloat16)
         rows = out_ref.shape[1]
         for k in range(WINDOW // rows):
-            to = place(at // rows + k, TP, OWNERS)
+            owner = at // rows + k
+            to = jnp.where(core_ref[0] == 0, *(order.index(owner) for order in ORDERS))
             out_ref[to] = share[k * rows : (k + 1) * rows]
 
 
-def attention_share(edge, sinks, queries, keys_t, values_t, rim, angles, weight, chips):
+def attention_share(core, edge, sinks, queries, keys_t, values_t, rim, angles, weight, chips):
     count, width = queries.shape[0], weight.shape[1]
     return pl.pallas_call(
         attend_kernel,
         out_shape=jax.ShapeDtypeStruct((chips, count // chips, width), jnp.bfloat16),
-        in_specs=[IN_SMEM] * 2 + [IN_VMEM] * 7,
+        in_specs=[IN_SMEM] * 3 + [IN_VMEM] * 7,
         out_specs=IN_VMEM,
         cost_estimate=pl.CostEstimate(
             flops=2 * count * 128 * (width + 1024),
             bytes_accessed=2 * (count + 128) * width,
             transcendentals=2 * count * 256,
         ),
-    )(edge, sinks, queries, keys_t, values_t, *map(near, (rim, *angles)), weight)
+    )(core, edge, sinks, queries, keys_t, values_t, *map(near, (rim, *angles)), weight)
+
+
+def rim_kernel(key_ref, value_ref, out_ref, sems):
+    copies = [
+        pltpu.make_async_copy(
+            ref.at[:, pl.ds(ref.shape[1] - WINDOW, WINDOW)],
+            out_ref.at[pl.ds(k * HEAD, HEAD)],
+            sems.at[k],
+        )
+        for k, ref in enumerate((key_ref, value_ref))
+    ]
+    for copy in copies:
+        copy.start()
+    for copy in copies:
+        copy.wait()
+
+
+def rim_of(keys_t, values_t):
+    return pl.pallas_call(
+        rim_kernel,
+        out_shape=pltpu.VMEM((2 * HEAD, WINDOW), keys_t.dtype),
+        in_specs=[IN_HBM] * 2,
+        out_specs=IN_VMEM,
+        scratch_shapes=[pltpu.SemaphoreType.DMA((2,))],
+        cost_estimate=price(10**5, 2**16),
+    )(far(keys_t), far(values_t))
 
 
 def plan_kernel(ids_ref, ids_row_ref, spread_ref, collect_ref):
@@ -178,8 +211,8 @@
             before = jnp.where((other_col == row) & (below < right), 1, 0)
             rank_row = rank_row + jnp.sum(before, 0, keepdims=True)
         for half in range(2):
-            line_col = place(col >> 1, SP[:-1], ROUTE) * LINES + half * SLOTS + (col & 1) * RANKS + rank_col
-            line_row = place(row >> 1, SP[:-1], ROUTE) * LINES + half * SLOTS + (row & 1) * RANKS + rank_row
+            line_col = (col >> 1) * LINES + half * SLOTS + (col & 1) * RANKS + rank_col
+            line_row = (row >> 1) * LINES + half * SLOTS + (row & 1) * RANKS + rank_row
             collect_ref[half, k * rows : (k + 1) * rows, :] = one_hot(
                 iota((rows, lines), 1) == line_col
             )
@@ -235,9 +268,8 @@
         in_specs=[IN_HBM] * 3,
         out_specs=[IN_VMEM] * 2,
         scratch_shapes=[pltpu.SemaphoreType.DMA((2, 2 + blocks))],
-        compiler_params=room(16),
         cost_estimate=price(10**6, 12 * units * width),
-    )(gate.reshape(blocks, 128, units), up.reshape(blocks, 128, units), down)
+    )(*map(far, (gate.reshape(blocks, 128, units), up.reshape(blocks, 128, units), down)))
 
 
 def hold_kernel(in_ref, out_ref):
@@ -291,52 +323,71 @@
     return iota(shape, 1) == plane * LINES + half * SLOTS + slot
 
 
-def fan_kernel(lines_ref, out_ref):
+def for_each_core(core_ref, body):
+    for core in range(2):
+
+        @pl.when(core_ref[0] == core)
+        def _():
+            body(core)
+
+
+def fan_kernel(core_ref, lines_ref, out_ref):
     half = lines_ref.shape[1]
     count = out_ref.shape[1]
     for h in range(2):
         rows = dot(one_hot(lines_of(h)), lines_ref[...]).astype(jnp.bfloat16)
-        for to in range(out_ref.shape[0]):
-            at = column_parity(to) * count
-            out_ref[to, :, h * half : (h + 1) * half] = rows[at : at + count]
-
-
-def fan(lines, chips):
+
+        def hand_out(core):
+            for to in range(out_ref.shape[0]):
+                at = column_parity(to, core) * count
+                out_ref[to, :, h * half : (h + 1) * half] = rows[at : at + count]
+
+        for_each_core(core_ref, hand_out)
+
+
+def fan(core, lines, chips):
     rows, width = PLANES * RANKS, 2 * lines.shape[1]
     return pl.pallas_call(
         fan_kernel,
-        out_shape=pltpu.VMEM((chips, rows, width), jnp.bfloat16),
-        in_specs=[IN_VMEM],
+        out_shape=jax.ShapeDtypeStruct((chips, rows, width), jnp.bfloat16),
+        in_specs=[IN_SMEM, IN_VMEM],
         out_specs=IN_VMEM,
         compiler_params=room(16),
         cost_estimate=price(8 * rows * lines.size, 2 * chips * rows * width),
-    )(near(lines))
-
-
-def fold_kernel(parts_ref, out_ref):
+    )(core, near(lines))
+
+
+def fold_kernel(core_ref, parts_ref, out_ref, rows_ref):
     half = out_ref.shape[1]
+    count = parts_ref.shape[1]
+
+    def add_up(core):
+        totals = [0.0] * PAIR
+        for chip in range(parts_ref.shape[0]):
+            expert = column_parity(chip, core)
+            totals[expert] = totals[expert] + parts_ref[chip].astype(jnp.float32)
+        for expert, total in enumerate(totals):
+            rows_ref[expert * count : (expert + 1) * count] = total.astype(jnp.bfloat16)
+
+    for_each_core(core_ref, add_up)
     lines = 0.0
-    totals = [0.0] * PAIR
-    for chip in range(parts_ref.shape[0]):
-        expert = column_parity(chip)
-        totals[expert] = totals[expert] + parts_ref[chip].astype(jnp.float32)
-    rows = jnp.concatenate(totals, 0).astype(jnp.bfloat16)
     for h in range(2):
-        lines = lines + over_rows(one_hot(lines_of(h)), rows[:, h * half : (h + 1) * half])
+        lines = lines + over_rows(one_hot(lines_of(h)), rows_ref[:, h * half : (h + 1) * half])
     out_ref[...] = lines.astype(jnp.bfloat16)
 
 
-def fold(parts):
-    width = parts.shape[-1]
+def fold(core, parts):
+    _, rows, width = parts.shape
     lines = PLANES * LINES
     return pl.pallas_call(
         fold_kernel,
         out_shape=jax.ShapeDtypeStruct((lines, width // 2), jnp.bfloat16),
-        in_specs=[IN_VMEM],
-        out_specs=IN_VMEM,
+        in_specs=[IN_SMEM, IN_VMEM],
+        out_specs=IN_VMEM,
+        scratch_shapes=[pltpu.VMEM((PAIR * rows, width), jnp.bfloat16)],
         compiler_params=room(24),
-        cost_estimate=price(2 * lines * PAIR * parts.shape[1] * width, 2 * parts.size),
-    )(near(parts))
+        cost_estimate=price(2 * lines * PAIR * rows * width, 2 * parts.size),
+    )(core, near(parts))
 
 
 def finish_kernel(lines_ref, collect_ref, share_ref, middle_ref, out_ref):
@@ -434,7 +485,7 @@
             bytes_accessed=4 * count * width + 24 * half * width,
             transcendentals=4 * count * half,
         ),
-    )(kept, near(rows), *own, *turned, *passed)
+    )(kept, near(rows), *map(far, (*own, *turned, *passed)))
 
 
 def per_device(
@@ -453,10 +504,11 @@
 ):
     local_len = queries.shape[0]
     span = lax.axis_index(SP)
+    core = lax.axis_index("core")
+    core_at = core.astype(jnp.int32).reshape(1)
     chips = lax.axis_size(TP)
     keys_t, values_t = key_rows.T, values.T
-    rim = jnp.concatenate([keys_t[:, -WINDOW:], values_t[:, -WINDOW:]], 0)
-    rim = from_behind(rim, SP, 1)
+    rim = from_behind(rim_of(keys_t, values_t), SP, 1)
     half = HEAD // 2
     frequency = 10000.0 ** (-jnp.arange(half, dtype=jnp.float32) * 2.0 / HEAD)
     positions = span * local_len - WINDOW + jnp.arange(local_len + WINDOW, dtype=jnp.int32)
@@ -464,36 +516,36 @@
     angles = (jnp.cos(angles), jnp.sin(angles))
     edge = jnp.where(span == 0, WINDOW, 0).astype(jnp.int32).reshape(1)
     shares = attention_share(
-        edge, sink_logits, queries, keys_t, values_t, rim, angles, out_weight, chips
+        core_at, edge, sink_logits, queries, keys_t, values_t, rim, angles, out_weight, chips
     )
     tok_rows, width = residual.shape
     first = lax.axis_index(TP) * tok_rows
     own_ids = lax.dynamic_slice_in_dim(expert_ids, first, tok_rows, 0)
     own_weights = lax.dynamic_slice_in_dim(route_weight, first, tok_rows, 0)
-    shares = exchange(shares, OWNERS)
+    shares = in_plane(shares)
     own = pack(gate_proj[0], up_proj[0], down_proj[0])
     right = turn(own[0], 1)
     left = turn(own[1], -1)
     spread, collect = plan(own_ids)
     middle, lines = settle(shares, residual, norm_gain.reshape(1, -1), spread)
-    lines = exchange(lines.reshape(PLANES, LINES, width // 2), ROUTE)
-    fanned = fan(lines.reshape(PLANES * LINES, width // 2), chips)
-    gathered = exchange(fanned, CHIPS)
+    lines = along_z(lines.reshape(PLANES, LINES, width // 2))
+    fanned = fan(core_at, lines.reshape(PLANES * LINES, width // 2), chips)
+    gathered = in_plane(fanned)
     right_too = pass_on(right)
     left_too = pass_on(left)
-    kept = (lax.axis_index("core") == lax.axis_index("x0")).astype(jnp.int32).reshape(1)
+    kept = (core == lax.axis_index("x") % 2).astype(jnp.int32).reshape(1)
     own_weights = hold(own_weights)
     parts = expert_part(
         kept, gathered.reshape(-1, width), own, (right, left), (right_too, left_too)
     )
-    parts = exchange(parts.reshape(chips, -1, width), CHIPS)
-    lines = fold(parts)
-    lines = exchange(lines.reshape(PLANES, LINES, width // 2), ROUTE)
+    parts = in_plane(parts.reshape(chips, -1, width))
+    lines = fold(core_at, parts)
+    lines = along_z(lines.reshape(PLANES, LINES, width // 2))
     return finish(lines.reshape(PLANES * LINES, width // 2), collect, own_weights, middle)
 
 
 def solution(mesh):
-    fine = jax.sharding.Mesh(mesh.devices.reshape([2] * len(SP + TP)), SP + TP)
+    fine = jax.sharding.Mesh(mesh.devices.reshape(SIZES), SP + TP)
     return jax.shard_map(
         per_device,
         mesh=fine,

time: 162 us -> 159 us (0.981)
  the two profiles are of different devices: /device:TPU:8 before, /device:TPU:10 now
where the time goes in v5:
time: 159 us; the launch traced here: 158 us
  blocking collectives  57.3 us (36%)
  waiting for transfers between devices  41 us (26%)
  starting transfers between devices  40.5 us (25%)
  Pallas kernels  18.2 us (11%)
    all_to_all x1, blocking collectives, along_z(): return lax.all_to_all(blocks, 'z', 0, 0, tiled=True)  32.8 us
    all_to_all x1, blocking collectives, in_plane(): lax.all_to_all(blocks, ('core',) + TP, 0, 0, axis_index_groups=GROUPS, ti...  24.5 us
    all_to_all x1, waiting for transfers between devices, along_z(): return lax.all_to_all(blocks, 'z', 0, 0, tiled=True)  18.2 us
    all_to_all x2, waiting for transfers between devices, in_plane(): lax.all_to_all(blocks, ('core',) + TP, 0, 0, axis_index_groups=GROUPS, ti...  16.7 us
    all_to_all x2, starting transfers between devices, in_plane(): lax.all_to_all(blocks, ('core',) + TP, 0, 0, axis_index_groups=GROUPS, ti...  15.4 us
    all_to_all x1, starting transfers between devices, along_z(): return lax.all_to_all(blocks, 'z', 0, 0, tiled=True)  15.2 us
    ppermute x2, starting transfers between devices, turn(): return lax.ppermute(pack, ('core', 'x'), route)  5.57 us
    ppermute x2, waiting for transfers between devices, pass_on(): return lax.ppermute(pack, ('core', 'x'), route)  5.52 us
  transfers between devices with their start and end apart: 8, of which 6 were waited for; matrix products, arithmetic and copies ran while one was open for 0% of the time, Pallas kernels for 4%

profile of v5, /device:TPU:10, one launch (start us, length us, event | category | flops | bytes accessed | tf_op | source)
XLA Modules:
  0.0 158.0 jit_solution(8469791611581723197)
XLA Ops:
  0.0 0.0 copy-start
  0.0 0.8 shard_map.118
  0.8 1.7 %collective-permute-start = (bf16[128,128]{1,0:T(8,128)(2,1)S(1)}, bf16[128,128]{1,0:T(8,128)(2,1)S(1)}, u32[]{:S(2)}, u32[]{:S(2)}) collective-permute-start(bf16[128,128]{1,0:T(8,128)(2,1)S(1)} %shard_map.118), channel_id=1, source_target_pairs={{0,16},{16,32},{32,48},{48,64},{64,80},{80,96},{96,112},{112,128},... | collective-permute-start | bytes 98312 | tf_op jit(solution)/shard_map/ppermute | solution.py:32
  2.6 0.3 multiply_sine_fusion
  2.8 0.5 collective-permute-done.rim_ref
  3.4 3.5 %shard_map.119 = bf16[16,16,2048]{2,1,0:T(8,128)(2,1)} custom-call(s32[1]{0:T(128)} %bitcast.core_ref, s32[1]{0:T(128)} %bitcast.2.edge_ref, f32[2]{0:T(128)} %sink_ref.1, bf16[256,128]{1,0:T(8,128)(2,1)} %query_ref.1, bf16[64,256]{1,0:T(8,128)(2,1)} %bitcast.27, bf16[64,256]{1,0:T(8,128)(2,1)} %bitcast.29, ...), custom_call_target="tpu_custom_call" | custom-call | flops 201326592 | bytes 1572864 | tf_op jit(solution)/shard_map/pallas_call | solution.py:159
  6.9 8.8 %all-to-all-start = ((bf16[16,16,2048]{2,1,0:T(8,128)(2,1)}), bf16[16,16,2048]{2,1,0:T(8,128)(2,1)S(1)}, u32[]{:S(2)}, u32[]{:S(2)}) async-start(bf16[16,16,2048]{2,1,0:T(8,128)(2,1)} %shard_map.119), calls=%async_computation | async-start | bytes 2097152 | tf_op jit(solution)/shard_map/all_to_all | solution.py:36
  15.7 0.0 copy-start.1
  15.7 0.0 copy-start.2
  15.7 3.8 %shard_map.123 = (bf16[3,16,128,128]{3,2,1,0:T(8,128)(2,1)}, bf16[3,16,128,128]{3,2,1,0:T(8,128)(2,1)}) custom-call(bf16[16,128,256]{2,1,0:T(8,128)(2,1)} %bitcast.23, bf16[16,128,256]{2,1,0:T(8,128)(2,1)} %bitcast.24, bf16[256,2048]{1,0:T(8,128)(2,1)} %bitcast.25), custom_call_target="tpu_custom_call" | custom-call | flops 1000000 | bytes 6291456 | tf_op jit(solution)/shard_map/pallas_call | solution.py:265
  19.5 2.4 %collective-permute-start.1 = (bf16[3,16,128,128]{3,2,1,0:T(8,128)(2,1)}, bf16[3,16,128,128]{3,2,1,0:T(8,128)(2,1)}, u32[]{:S(2)}, u32[]{:S(2)}) collective-permute-start(bf16[3,16,128,128]{3,2,1,0:T(8,128)(2,1)} %get-tuple-element.13.refs_0_), channel_id=1, source_target_pairs={{0,16},{16,17},{17,1},{1,0},{2,18},{18,19},{19,3},{3,2},{4,20},{20... | collective-permute-start | bytes 4718600 | tf_op jit(solution)/shard_map/ppermute | solution.py:55
  21.9 3.1 %collective-permute-start.2 = (bf16[3,16,128,128]{3,2,1,0:T(8,128)(2,1)}, bf16[3,16,128,128]{3,2,1,0:T(8,128)(2,1)}, u32[]{:S(2)}, u32[]{:S(2)}) collective-permute-start(bf16[3,16,128,128]{3,2,1,0:T(8,128)(2,1)} %get-tuple-element.14.refs_1_), channel_id=1, source_target_pairs={{0,16},{16,19},{17,1},{1,2},{2,18},{18,17},{19,3},{3,0},{4,20},{20... | collective-permute-start | bytes 4718600 | tf_op jit(solution)/shard_map/ppermute | solution.py:55
  25.1 0.0 copy-done
  25.1 0.1 constant_dynamic-slice_fusion.1
  25.2 0.1 copy.13.ids_ref
  25.2 0.1 fusion.ids_row_ref
  25.3 0.2 shard_map.120
  25.6 5.1 %all-to-all-done.shares_ref = bf16[16,16,2048]{2,1,0:T(8,128)(2,1)S(1)} async-done(((bf16[16,16,2048]{2,1,0:T(8,128)(2,1)}), bf16[16,16,2048]{2,1,0:T(8,128)(2,1)S(1)}, u32[]{:S(2)}, u32[]{:S(2)}) %all-to-all-start) | async-done | bytes 1048608 | tf_op jit(solution)/shard_map/all_to_all | solution.py:36
  30.7 0.0 copy-done.1
  30.7 0.0 copy-done.2
  30.7 0.5 shard_map.121
  31.2 32.8 %all_to_all.25 = bf16[16,8,1024]{2,1,0:T(8,128)(2,1)S(1)} all-to-all(bf16[16,8,1024]{2,1,0:T(8,128)(2,1)S(1)} %bitcast.21), channel_id=1, replica_groups=mesh['z'=16,'core'=2,'y'=4,'x'=4] {'z'}, dimensions={0} | all-to-all | bytes 524288 | tf_op jit(solution)/shard_map/all_to_all | solution.py:42
  64.1 1.8 %shard_map.122 = bf16[16,32,2048]{2,1,0:T(8,128)(2,1)} custom-call(s32[1]{0:T(128)} %bitcast.core_ref, bf16[128,1024]{1,0:T(8,128)(2,1)S(1)} %bitcast.19), custom_call_target="tpu_custom_call" | custom-call | flops 33554432 | bytes 2097152 | tf_op jit(solution)/shard_map/pallas_call | solution.py:350
  65.9 6.6 %all-to-all-start.2 = ((bf16[16,32,2048]{2,1,0:T(8,128)(2,1)}), bf16[16,32,2048]{2,1,0:T(8,128)(2,1)S(1)}, u32[]{:S(2)}, u32[]{:S(2)}) async-start(bf16[16,32,2048]{2,1,0:T(8,128)(2,1)} %shard_map.122), calls=%async_computation.2 | async-start | bytes 4194304 | tf_op jit(solution)/shard_map/all_to_all | solution.py:36
  72.5 0.0 collective-permute-done.1.refs_2_
  72.5 1.3 collective-permute-start.3
  73.8 0.0 collective-permute-done.2.refs_3_
  73.8 1.3 collective-permute-start.4
  75.2 3.0 %collective-permute-done.3.refs_4_ = bf16[3,16,128,128]{3,2,1,0:T(8,128)(2,1)} collective-permute-done((bf16[3,16,128,128]{3,2,1,0:T(8,128)(2,1)}, bf16[3,16,128,128]{3,2,1,0:T(8,128)(2,1)}, u32[]{:S(2)}, u32[]{:S(2)}) %collective-permute-start.3) | collective-permute-done | bytes 1572896 | tf_op jit(solution)/shard_map/ppermute | solution.py:60
  78.2 2.5 %collective-permute-done.4.refs_5_ = bf16[3,16,128,128]{3,2,1,0:T(8,128)(2,1)} collective-permute-done((bf16[3,16,128,128]{3,2,1,0:T(8,128)(2,1)}, bf16[3,16,128,128]{3,2,1,0:T(8,128)(2,1)}, u32[]{:S(2)}, u32[]{:S(2)}) %collective-permute-start.4) | collective-permute-done | bytes 1572896 | tf_op jit(solution)/shard_map/ppermute | solution.py:60
  80.7 11.6 %all-to-all-done.2 = bf16[16,32,2048]{2,1,0:T(8,128)(2,1)S(1)} async-done(((bf16[16,32,2048]{2,1,0:T(8,128)(2,1)}), bf16[16,32,2048]{2,1,0:T(8,128)(2,1)S(1)}, u32[]{:S(2)}, u32[]{:S(2)}) %all-to-all-start.2) | async-done | bytes 2097184 | tf_op jit(solution)/shard_map/all_to_all | solution.py:36
  92.2 5.4 %shard_map.124 = bf16[512,2048]{1,0:T(8,128)(2,1)S(1)} custom-call(s32[1]{0:T(128)} %bitcast.1.kept_ref, bf16[512,2048]{1,0:T(8,128)(2,1)S(1)} %bitcast.17, bf16[3,16,128,128]{3,2,1,0:T(8,128)(2,1)} %get-tuple-element.13.refs_0_, bf16[3,16,128,128]{3,2,1,0:T(8,128)(2,1)} %get-tuple-element.14.refs_1_, ...), custom_call_target="tpu_custom_call" | custom-call | flops 3221225472 | bytes 10485760 | tf_op jit(solution)/shard_map/pallas_call | solution.py:471
  97.7 24.5 %all_to_all.26.parts_ref = bf16[16,32,2048]{2,1,0:T(8,128)(2,1)S(1)} all-to-all(bf16[16,32,2048]{2,1,0:T(8,128)(2,1)S(1)} %bitcast.18), channel_id=1, replica_groups={{0,4,8,12,1,5,9,13,2,6,10,14,3,7,11,15},{31,27,23,19,30,26,22,18,29,25,..., dimensions={0} | all-to-all | bytes 4194304 | tf_op jit(solution)/shard_map/all_to_all | solution.py:36
  122.2 0.0 copy-start.3
  122.2 1.3 shard_map.125
  123.5 15.2 %all-to-all-start.4 = ((bf16[16,8,1024]{2,1,0:T(8,128)(2,1)}), bf16[16,8,1024]{2,1,0:T(8,128)(2,1)S(1)}, u32[]{:S(2)}, u32[]{:S(2)}) async-start(bf16[16,8,1024]{2,1,0:T(8,128)(2,1)} %bitcast.14), calls=%async_computation.4 | async-start | bytes 524288 | tf_op jit(solution)/shard_map/all_to_all | solution.py:42
  138.7 0.0 copy-done.3
  138.7 0.1 constant_dynamic-slice_fusion
  138.8 0.1 copy.15.in_ref
  138.9 18.2 %all-to-all-done.4 = bf16[16,8,1024]{2,1,0:T(8,128)(2,1)S(1)} async-done(((bf16[16,8,1024]{2,1,0:T(8,128)(2,1)}), bf16[16,8,1024]{2,1,0:T(8,128)(2,1)S(1)}, u32[]{:S(2)}, u32[]{:S(2)}) %all-to-all-start.4) | async-done | bytes 262176 | tf_op jit(solution)/shard_map/all_to_all | solution.py:42
  157.1 0.8 shard_map.127
  (3 shorter events, 0.0 us)
Async XLA Ops:
  0.0 25.1 %copy-start = (s32[256,2]{0,1:T(2,128)S(1)}, s32[256,2]{0,1:T(2,128)}, u32[]{:S(2)}) copy-start(s32[256,2]{0,1:T(2,128)} %param.19) | copy-start | bytes 6148
  0.8 2.6 %collective-permute-start = (bf16[128,128]{1,0:T(8,128)(2,1)S(1)}, bf16[128,128]{1,0:T(8,128)(2,1)S(1)}, u32[]{:S(2)}, u32[]{:S(2)}) collective-permute-start(bf16[128,128]{1,0:T(8,128)(2,1)S(1)} %shard_map.118), channel_id=1, source_target_pairs={{0,16},{16,32},{32,48},{48,64},{64,80},{80,96},{96,112},{112,128},... | collective-permute-start | bytes 98312 | tf_op jit(solution)/shard_map/ppermute | solution.py:32
  6.9 23.8 %all-to-all-start = ((bf16[16,16,2048]{2,1,0:T(8,128)(2,1)}), bf16[16,16,2048]{2,1,0:T(8,128)(2,1)S(1)}, u32[]{:S(2)}, u32[]{:S(2)}) async-start(bf16[16,16,2048]{2,1,0:T(8,128)(2,1)} %shard_map.119), calls=%async_computation | async-start | bytes 2097152 | tf_op jit(solution)/shard_map/all_to_all | solution.py:36
  15.7 15.0 %copy-start.1 = (bf16[16,2048]{1,0:T(8,128)(2,1)S(1)}, bf16[16,2048]{1,0:T(8,128)(2,1)}, u32[]{:S(2)}) copy-start(bf16[16,2048]{1,0:T(8,128)(2,1)} %residual_ref.1) | copy-start | bytes 196612
  15.7 15.0 %copy-start.2 = (f32[2048]{0:T(1024)S(1)}, f32[2048]{0:T(1024)}, u32[]{:S(2)}) copy-start(f32[2048]{0:T(1024)} %param.18) | copy-start | bytes 24580
  19.5 53.0 %collective-permute-start.1 = (bf16[3,16,128,128]{3,2,1,0:T(8,128)(2,1)}, bf16[3,16,128,128]{3,2,1,0:T(8,128)(2,1)}, u32[]{:S(2)}, u32[]{:S(2)}) collective-permute-start(bf16[3,16,128,128]{3,2,1,0:T(8,128)(2,1)} %get-tuple-element.13.refs_0_), channel_id=1, source_target_pairs={{0,16},{16,17},{17,1},{1,0},{2,18},{18,19},{19,3},{3,2},{4,20},{20... | collective-permute-start | bytes 4718600 | tf_op jit(solution)/shard_map/ppermute | solution.py:55
  21.9 51.9 %collective-permute-start.2 = (bf16[3,16,128,128]{3,2,1,0:T(8,128)(2,1)}, bf16[3,16,128,128]{3,2,1,0:T(8,128)(2,1)}, u32[]{:S(2)}, u32[]{:S(2)}) collective-permute-start(bf16[3,16,128,128]{3,2,1,0:T(8,128)(2,1)} %get-tuple-element.14.refs_1_), channel_id=1, source_target_pairs={{0,16},{16,19},{17,1},{1,2},{2,18},{18,17},{19,3},{3,0},{4,20},{20... | collective-permute-start | bytes 4718600 | tf_op jit(solution)/shard_map/ppermute | solution.py:55
  65.9 26.3 %all-to-all-start.2 = ((bf16[16,32,2048]{2,1,0:T(8,128)(2,1)}), bf16[16,32,2048]{2,1,0:T(8,128)(2,1)S(1)}, u32[]{:S(2)}, u32[]{:S(2)}) async-start(bf16[16,32,2048]{2,1,0:T(8,128)(2,1)} %shard_map.122), calls=%async_computation.2 | async-start | bytes 4194304 | tf_op jit(solution)/shard_map/all_to_all | solution.py:36
  72.5 5.6 %collective-permute-start.3 = (bf16[3,16,128,128]{3,2,1,0:T(8,128)(2,1)}, bf16[3,16,128,128]{3,2,1,0:T(8,128)(2,1)}, u32[]{:S(2)}, u32[]{:S(2)}) collective-permute-start(bf16[3,16,128,128]{3,2,1,0:T(8,128)(2,1)} %collective-permute-done.1.refs_2_), channel_id=1, source_target_pairs={{0,16},{17,1},{2,18},{19,3},{4,20},{21,5},{6,22},{23,7},{8,24},{25... | collective-permute-start | bytes 4718600 | tf_op jit(solution)/shard_map/ppermute | solution.py:60
  73.8 6.8 %collective-permute-start.4 = (bf16[3,16,128,128]{3,2,1,0:T(8,128)(2,1)}, bf16[3,16,128,128]{3,2,1,0:T(8,128)(2,1)}, u32[]{:S(2)}, u32[]{:S(2)}) collective-permute-start(bf16[3,16,128,128]{3,2,1,0:T(8,128)(2,1)} %collective-permute-done.2.refs_3_), channel_id=1, source_target_pairs={{0,16},{17,1},{2,18},{19,3},{4,20},{21,5},{6,22},{23,7},{8,24},{25... | collective-permute-start | bytes 4718600 | tf_op jit(solution)/shard_map/ppermute | solution.py:60
  122.2 16.6 %copy-start.3 = (f32[256,2]{0,1:T(2,128)S(1)}, f32[256,2]{0,1:T(2,128)}, u32[]{:S(2)}) copy-start(f32[256,2]{0,1:T(2,128)} %param.20) | copy-start | bytes 6148
  123.5 33.6 %all-to-all-start.4 = ((bf16[16,8,1024]{2,1,0:T(8,128)(2,1)}), bf16[16,8,1024]{2,1,0:T(8,128)(2,1)S(1)}, u32[]{:S(2)}, u32[]{:S(2)}) async-start(bf16[16,8,1024]{2,1,0:T(8,128)(2,1)} %bitcast.14), calls=%async_computation.4 | async-start | bytes 524288 | tf_op jit(solution)/shard_map/all_to_all | solution.py:42

commit v6 on v5

--- a/solution.py
+++ b/solution.py
@@ -115,7 +115,9 @@
     core_ref, edge_ref, sink_ref, query_ref, key_ref, value_ref, rim_ref, *refs
 ):
     count = query_ref.shape[0]
-    cosine_ref, sine_ref, weight_ref, out_ref = refs
+    cosine_ref, sine_ref, weight_hbm, out_ref, weight_ref, fetched = refs
+    fetch = pltpu.make_async_copy(weight_hbm, weight_ref, fetched)
+    fetch.start()
     cosine, sine = cosine_ref[...], sine_ref[...]
     keys = jnp.concatenate([rim_ref[:HEAD], key_ref[...]], 1).astype(jnp.float32)
     keys = turned(keys, cosine, sine)
@@ -146,6 +148,8 @@
         )
         attended = (weighted / denominator).astype(jnp.bfloat16)
         attended = jnp.concatenate([attended[:, :WINDOW], attended[:, WINDOW:]], 0)
+        if at == 0:
+            fetch.wait()
         share = over_rows(attended, weight_ref[...]).astype(jnp.bfloat16)
         rows = out_ref.shape[1]
         for k in range(WINDOW // rows):
@@ -159,14 +163,15 @@
     return pl.pallas_call(
         attend_kernel,
         out_shape=jax.ShapeDtypeStruct((chips, count // chips, width), jnp.bfloat16),
-        in_specs=[IN_SMEM] * 3 + [IN_VMEM] * 7,
-        out_specs=IN_VMEM,
+        in_specs=[IN_SMEM] * 3 + [IN_VMEM] * 6 + [IN_HBM],
+        out_specs=IN_VMEM,
+        scratch_shapes=[pltpu.VMEM(weight.shape, weight.dtype), pltpu.SemaphoreType.DMA],
         cost_estimate=pl.CostEstimate(
             flops=2 * count * 128 * (width + 1024),
             bytes_accessed=2 * (count + 128) * width,
             transcendentals=2 * count * 256,
         ),
-    )(core, edge, sinks, queries, keys_t, values_t, *map(near, (rim, *angles)), weight)
+    )(core, edge, sinks, queries, keys_t, values_t, *map(near, (rim, *angles)), far(weight))
 
 
 def rim_kernel(key_ref, value_ref, out_ref, sems):

time: 159 us -> 159 us (level)
  no operation moved by 1% of the time
where the time goes in v6:
time: 159 us
  blocking collectives  57.4 us (36%)
  waiting for transfers between devices  41.1 us (26%)
  starting transfers between devices  40.5 us (25%)
  Pallas kernels  18.9 us (12%)
    all_to_all x1, blocking collectives, along_z(): return lax.all_to_all(blocks, 'z', 0, 0, tiled=True)  32.8 us
    all_to_all x1, blocking collectives, in_plane(): lax.all_to_all(blocks, ('core',) + TP, 0, 0, axis_index_groups=GROUPS, ti...  24.5 us
    all_to_all x1, waiting for transfers between devices, along_z(): return lax.all_to_all(blocks, 'z', 0, 0, tiled=True)  18.3 us
    all_to_all x2, waiting for transfers between devices, in_plane(): lax.all_to_all(blocks, ('core',) + TP, 0, 0, axis_index_groups=GROUPS, ti...  16.7 us
    all_to_all x2, starting transfers between devices, in_plane(): lax.all_to_all(blocks, ('core',) + TP, 0, 0, axis_index_groups=GROUPS, ti...  15.4 us
    all_to_all x1, starting transfers between devices, along_z(): return lax.all_to_all(blocks, 'z', 0, 0, tiled=True)  15.2 us
    ppermute x2, starting transfers between devices, turn(): return lax.ppermute(pack, ('core', 'x'), route)  5.57 us
    ppermute x2, waiting for transfers between devices, pass_on(): return lax.ppermute(pack, ('core', 'x'), route)  5.52 us
  transfers between devices with their start and end apart: 8, of which 6 were waited for; matrix products, arithmetic and copies ran while one was open for 0% of the time, Pallas kernels for 4%

profile of v6, /device:TPU:10, one launch (start us, length us, event | category | flops | bytes accessed | tf_op | source)
XLA Modules:
  0.0 158.8 jit_solution(8693128322929425578)
XLA Ops:
  0.0 0.0 copy-start
  0.0 0.8 shard_map.118
  0.8 1.7 %collective-permute-start = (bf16[128,128]{1,0:T(8,128)(2,1)S(1)}, bf16[128,128]{1,0:T(8,128)(2,1)S(1)}, u32[]{:S(2)}, u32[]{:S(2)}) collective-permute-start(bf16[128,128]{1,0:T(8,128)(2,1)S(1)} %shard_map.118), channel_id=1, source_target_pairs={{0,16},{16,32},{32,48},{48,64},{64,80},{80,96},{96,112},{112,128},... | collective-permute-start | bytes 98312 | tf_op jit(solution)/shard_map/ppermute | solution.py:32
  2.6 0.3 multiply_sine_fusion
  2.8 0.5 collective-permute-done.rim_ref
  3.4 4.2 %shard_map.119 = bf16[16,16,2048]{2,1,0:T(8,128)(2,1)} custom-call(s32[1]{0:T(128)} %bitcast.core_ref, s32[1]{0:T(128)} %bitcast.2.edge_ref, f32[2]{0:T(128)} %sink_ref.1, bf16[256,128]{1,0:T(8,128)(2,1)} %query_ref.1, bf16[64,256]{1,0:T(8,128)(2,1)} %bitcast.27, bf16[64,256]{1,0:T(8,128)(2,1)} %bitcast.29, ...), custom_call_target="tpu_custom_call" | custom-call | flops 201326592 | bytes 1572864 | tf_op jit(solution)/shard_map/pallas_call | solution.py:163
  7.6 8.8 %all-to-all-start = ((bf16[16,16,2048]{2,1,0:T(8,128)(2,1)}), bf16[16,16,2048]{2,1,0:T(8,128)(2,1)S(1)}, u32[]{:S(2)}, u32[]{:S(2)}) async-start(bf16[16,16,2048]{2,1,0:T(8,128)(2,1)} %shard_map.119), calls=%async_computation | async-start | bytes 2097152 | tf_op jit(solution)/shard_map/all_to_all | solution.py:36
  16.4 0.0 copy-start.1
  16.4 0.0 copy-start.2
  16.4 3.8 %shard_map.123 = (bf16[3,16,128,128]{3,2,1,0:T(8,128)(2,1)}, bf16[3,16,128,128]{3,2,1,0:T(8,128)(2,1)}) custom-call(bf16[16,128,256]{2,1,0:T(8,128)(2,1)} %bitcast.23, bf16[16,128,256]{2,1,0:T(8,128)(2,1)} %bitcast.24, bf16[256,2048]{1,0:T(8,128)(2,1)} %bitcast.25), custom_call_target="tpu_custom_call" | custom-call | flops 1000000 | bytes 6291456 | tf_op jit(solution)/shard_map/pallas_call | solution.py:270
  20.2 2.4 %collective-permute-start.1 = (bf16[3,16,128,128]{3,2,1,0:T(8,128)(2,1)}, bf16[3,16,128,128]{3,2,1,0:T(8,128)(2,1)}, u32[]{:S(2)}, u32[]{:S(2)}) collective-permute-start(bf16[3,16,128,128]{3,2,1,0:T(8,128)(2,1)} %get-tuple-element.13.refs_0_), channel_id=1, source_target_pairs={{0,16},{16,17},{17,1},{1,0},{2,18},{18,19},{19,3},{3,2},{4,20},{20... | collective-permute-start | bytes 4718600 | tf_op jit(solution)/shard_map/ppermute | solution.py:55
  22.6 3.1 %collective-permute-start.2 = (bf16[3,16,128,128]{3,2,1,0:T(8,128)(2,1)}, bf16[3,16,128,128]{3,2,1,0:T(8,128)(2,1)}, u32[]{:S(2)}, u32[]{:S(2)}) collective-permute-start(bf16[3,16,128,128]{3,2,1,0:T(8,128)(2,1)} %get-tuple-element.14.refs_1_), channel_id=1, source_target_pairs={{0,16},{16,19},{17,1},{1,2},{2,18},{18,17},{19,3},{3,0},{4,20},{20... | collective-permute-start | bytes 4718600 | tf_op jit(solution)/shard_map/ppermute | solution.py:55
  25.7 0.0 copy-done
  25.8 0.1 constant_dynamic-slice_fusion.1
  25.8 0.1 copy.13.ids_ref
  25.9 0.1 fusion.ids_row_ref
  26.0 0.2 shard_map.120
  26.2 5.1 %all-to-all-done.shares_ref = bf16[16,16,2048]{2,1,0:T(8,128)(2,1)S(1)} async-done(((bf16[16,16,2048]{2,1,0:T(8,128)(2,1)}), bf16[16,16,2048]{2,1,0:T(8,128)(2,1)S(1)}, u32[]{:S(2)}, u32[]{:S(2)}) %all-to-all-start) | async-done | bytes 1048608 | tf_op jit(solution)/shard_map/all_to_all | solution.py:36
  31.4 0.0 copy-done.1
  31.4 0.0 copy-done.2
  31.4 0.5 shard_map.121
  31.9 32.8 %all_to_all.25 = bf16[16,8,1024]{2,1,0:T(8,128)(2,1)S(1)} all-to-all(bf16[16,8,1024]{2,1,0:T(8,128)(2,1)S(1)} %bitcast.21), channel_id=1, replica_groups=mesh['z'=16,'core'=2,'y'=4,'x'=4] {'z'}, dimensions={0} | all-to-all | bytes 524288 | tf_op jit(solution)/shard_map/all_to_all | solution.py:42
  64.7 1.8 %shard_map.122 = bf16[16,32,2048]{2,1,0:T(8,128)(2,1)} custom-call(s32[1]{0:T(128)} %bitcast.core_ref, bf16[128,1024]{1,0:T(8,128)(2,1)S(1)} %bitcast.19), custom_call_target="tpu_custom_call" | custom-call | flops 33554432 | bytes 2097152 | tf_op jit(solution)/shard_map/pallas_call | solution.py:355
  66.6 6.6 %all-to-all-start.2 = ((bf16[16,32,2048]{2,1,0:T(8,128)(2,1)}), bf16[16,32,2048]{2,1,0:T(8,128)(2,1)S(1)}, u32[]{:S(2)}, u32[]{:S(2)}) async-start(bf16[16,32,2048]{2,1,0:T(8,128)(2,1)} %shard_map.122), calls=%async_computation.2 | async-start | bytes 4194304 | tf_op jit(solution)/shard_map/all_to_all | solution.py:36
  73.2 0.0 collective-permute-done.1.refs_2_
  73.2 1.3 collective-permute-start.3
  74.5 0.0 collective-permute-done.2.refs_3_
  74.5 1.3 collective-permute-start.4
  75.8 3.0 %collective-permute-done.3.refs_4_ = bf16[3,16,128,128]{3,2,1,0:T(8,128)(2,1)} collective-permute-done((bf16[3,16,128,128]{3,2,1,0:T(8,128)(2,1)}, bf16[3,16,128,128]{3,2,1,0:T(8,128)(2,1)}, u32[]{:S(2)}, u32[]{:S(2)}) %collective-permute-start.3) | collective-permute-done | bytes 1572896 | tf_op jit(solution)/shard_map/ppermute | solution.py:60
  78.8 2.5 %collective-permute-done.4.refs_5_ = bf16[3,16,128,128]{3,2,1,0:T(8,128)(2,1)} collective-permute-done((bf16[3,16,128,128]{3,2,1,0:T(8,128)(2,1)}, bf16[3,16,128,128]{3,2,1,0:T(8,128)(2,1)}, u32[]{:S(2)}, u32[]{:S(2)}) %collective-permute-start.4) | collective-permute-done | bytes 1572896 | tf_op jit(solution)/shard_map/ppermute | solution.py:60
  81.3 11.6 %all-to-all-done.2 = bf16[16,32,2048]{2,1,0:T(8,128)(2,1)S(1)} async-done(((bf16[16,32,2048]{2,1,0:T(8,128)(2,1)}), bf16[16,32,2048]{2,1,0:T(8,128)(2,1)S(1)}, u32[]{:S(2)}, u32[]{:S(2)}) %all-to-all-start.2) | async-done | bytes 2097184 | tf_op jit(solution)/shard_map/all_to_all | solution.py:36
  92.9 5.4 %shard_map.124 = bf16[512,2048]{1,0:T(8,128)(2,1)S(1)} custom-call(s32[1]{0:T(128)} %bitcast.1.kept_ref, bf16[512,2048]{1,0:T(8,128)(2,1)S(1)} %bitcast.17, bf16[3,16,128,128]{3,2,1,0:T(8,128)(2,1)} %get-tuple-element.13.refs_0_, bf16[3,16,128,128]{3,2,1,0:T(8,128)(2,1)} %get-tuple-element.14.refs_1_, ...), custom_call_target="tpu_custom_call" | custom-call | flops 3221225472 | bytes 10485760 | tf_op jit(solution)/shard_map/pallas_call | solution.py:476
  98.3 24.5 %all_to_all.26.parts_ref = bf16[16,32,2048]{2,1,0:T(8,128)(2,1)S(1)} all-to-all(bf16[16,32,2048]{2,1,0:T(8,128)(2,1)S(1)} %bitcast.18), channel_id=1, replica_groups={{0,4,8,12,1,5,9,13,2,6,10,14,3,7,11,15},{31,27,23,19,30,26,22,18,29,25,..., dimensions={0} | all-to-all | bytes 4194304 | tf_op jit(solution)/shard_map/all_to_all | solution.py:36
  122.9 0.0 copy-start.3
  122.9 1.3 shard_map.125
  124.2 15.2 %all-to-all-start.4 = ((bf16[16,8,1024]{2,1,0:T(8,128)(2,1)}), bf16[16,8,1024]{2,1,0:T(8,128)(2,1)S(1)}, u32[]{:S(2)}, u32[]{:S(2)}) async-start(bf16[16,8,1024]{2,1,0:T(8,128)(2,1)} %bitcast.14), calls=%async_computation.4 | async-start | bytes 524288 | tf_op jit(solution)/shard_map/all_to_all | solution.py:42
  139.4 0.0 copy-done.3
  139.4 0.1 constant_dynamic-slice_fusion
  139.5 0.1 copy.15.in_ref
  139.6 18.3 %all-to-all-done.4 = bf16[16,8,1024]{2,1,0:T(8,128)(2,1)S(1)} async-done(((bf16[16,8,1024]{2,1,0:T(8,128)(2,1)}), bf16[16,8,1024]{2,1,0:T(8,128)(2,1)S(1)}, u32[]{:S(2)}, u32[]{:S(2)}) %all-to-all-start.4) | async-done | bytes 262176 | tf_op jit(solution)/shard_map/all_to_all | solution.py:42
  157.9 0.8 shard_map.127
  (3 shorter events, 0.0 us)
Async XLA Ops:
  0.0 25.8 %copy-start = (s32[256,2]{0,1:T(2,128)S(1)}, s32[256,2]{0,1:T(2,128)}, u32[]{:S(2)}) copy-start(s32[256,2]{0,1:T(2,128)} %param.19) | copy-start | bytes 6148
  0.8 2.6 %collective-permute-start = (bf16[128,128]{1,0:T(8,128)(2,1)S(1)}, bf16[128,128]{1,0:T(8,128)(2,1)S(1)}, u32[]{:S(2)}, u32[]{:S(2)}) collective-permute-start(bf16[128,128]{1,0:T(8,128)(2,1)S(1)} %shard_map.118), channel_id=1, source_target_pairs={{0,16},{16,32},{32,48},{48,64},{64,80},{80,96},{96,112},{112,128},... | collective-permute-start | bytes 98312 | tf_op jit(solution)/shard_map/ppermute | solution.py:32
  7.6 23.8 %all-to-all-start = ((bf16[16,16,2048]{2,1,0:T(8,128)(2,1)}), bf16[16,16,2048]{2,1,0:T(8,128)(2,1)S(1)}, u32[]{:S(2)}, u32[]{:S(2)}) async-start(bf16[16,16,2048]{2,1,0:T(8,128)(2,1)} %shard_map.119), calls=%async_computation | async-start | bytes 2097152 | tf_op jit(solution)/shard_map/all_to_all | solution.py:36
  16.4 15.0 %copy-start.1 = (bf16[16,2048]{1,0:T(8,128)(2,1)S(1)}, bf16[16,2048]{1,0:T(8,128)(2,1)}, u32[]{:S(2)}) copy-start(bf16[16,2048]{1,0:T(8,128)(2,1)} %residual_ref.1) | copy-start | bytes 196612
  16.4 15.0 %copy-start.2 = (f32[2048]{0:T(1024)S(1)}, f32[2048]{0:T(1024)}, u32[]{:S(2)}) copy-start(f32[2048]{0:T(1024)} %param.18) | copy-start | bytes 24580
  20.2 53.0 %collective-permute-start.1 = (bf16[3,16,128,128]{3,2,1,0:T(8,128)(2,1)}, bf16[3,16,128,128]{3,2,1,0:T(8,128)(2,1)}, u32[]{:S(2)}, u32[]{:S(2)}) collective-permute-start(bf16[3,16,128,128]{3,2,1,0:T(8,128)(2,1)} %get-tuple-element.13.refs_0_), channel_id=1, source_target_pairs={{0,16},{16,17},{17,1},{1,0},{2,18},{18,19},{19,3},{3,2},{4,20},{20... | collective-permute-start | bytes 4718600 | tf_op jit(solution)/shard_map/ppermute | solution.py:55
  22.6 51.9 %collective-permute-start.2 = (bf16[3,16,128,128]{3,2,1,0:T(8,128)(2,1)}, bf16[3,16,128,128]{3,2,1,0:T(8,128)(2,1)}, u32[]{:S(2)}, u32[]{:S(2)}) collective-permute-start(bf16[3,16,128,128]{3,2,1,0:T(8,128)(2,1)} %get-tuple-element.14.refs_1_), channel_id=1, source_target_pairs={{0,16},{16,19},{17,1},{1,2},{2,18},{18,17},{19,3},{3,0},{4,20},{20... | collective-permute-start | bytes 4718600 | tf_op jit(solution)/shard_map/ppermute | solution.py:55
  66.6 26.3 %all-to-all-start.2 = ((bf16[16,32,2048]{2,1,0:T(8,128)(2,1)}), bf16[16,32,2048]{2,1,0:T(8,128)(2,1)S(1)}, u32[]{:S(2)}, u32[]{:S(2)}) async-start(bf16[16,32,2048]{2,1,0:T(8,128)(2,1)} %shard_map.122), calls=%async_computation.2 | async-start | bytes 4194304 | tf_op jit(solution)/shard_map/all_to_all | solution.py:36
  73.2 5.6 %collective-permute-start.3 = (bf16[3,16,128,128]{3,2,1,0:T(8,128)(2,1)}, bf16[3,16,128,128]{3,2,1,0:T(8,128)(2,1)}, u32[]{:S(2)}, u32[]{:S(2)}) collective-permute-start(bf16[3,16,128,128]{3,2,1,0:T(8,128)(2,1)} %collective-permute-done.1.refs_2_), channel_id=1, source_target_pairs={{0,16},{17,1},{2,18},{19,3},{4,20},{21,5},{6,22},{23,7},{8,24},{25... | collective-permute-start | bytes 4718600 | tf_op jit(solution)/shard_map/ppermute | solution.py:60
  74.5 6.8 %collective-permute-start.4 = (bf16[3,16,128,128]{3,2,1,0:T(8,128)(2,1)}, bf16[3,16,128,128]{3,2,1,0:T(8,128)(2,1)}, u32[]{:S(2)}, u32[]{:S(2)}) collective-permute-start(bf16[3,16,128,128]{3,2,1,0:T(8,128)(2,1)} %collective-permute-done.2.refs_3_), channel_id=1, source_target_pairs={{0,16},{17,1},{2,18},{19,3},{4,20},{21,5},{6,22},{23,7},{8,24},{25... | collective-permute-start | bytes 4718600 | tf_op jit(solution)/shard_map/ppermute | solution.py:60
  122.9 16.5 %copy-start.3 = (f32[256,2]{0,1:T(2,128)S(1)}, f32[256,2]{0,1:T(2,128)}, u32[]{:S(2)}) copy-start(f32[256,2]{0,1:T(2,128)} %param.20) | copy-start | bytes 6148
  124.2 33.7 %all-to-all-start.4 = ((bf16[16,8,1024]{2,1,0:T(8,128)(2,1)}), bf16[16,8,1024]{2,1,0:T(8,128)(2,1)S(1)}, u32[]{:S(2)}, u32[]{:S(2)}) async-start(bf16[16,8,1024]{2,1,0:T(8,128)(2,1)} %bitcast.14), calls=%async_computation.4 | async-start | bytes 524288 | tf_op jit(solution)/shard_map/all_to_all | solution.py:42
